TPU v7x, 512 devices: a whole 4x4x16 slice. The times are simulated.
512 devices in a mesh: kv: 32 (over z, core), tp: 16 (over y, x).
Axes of the slice: x: 4, y: 4, z: 16, core: 2. Of those that a mesh axis runs over, the one named last changes fastest.
Arguments:
- tokens: bfloat16 [256, 4096], P(None, ('kv', 'tp')), may hold values from -3 to 3
- lengths: int32 [64], replicated, may hold values from 1 to 4, 128 in all
- states: float32 [64, 16, 128, 128], P('kv', 'tp'), may hold values from -3 to 3
- gain_pre: float32 [4096], P('kv'), may hold values from 0.1 to 1.9
- pre_gate: bfloat16 [4096, 11264], P('kv', 'tp'), may hold values from -0.09375 to 0.09375
- pre_up: bfloat16 [4096, 11264], P('kv', 'tp'), may hold values from -0.09375 to 0.09375
- pre_down: bfloat16 [11264, 4096], P('tp', 'kv'), may hold values from -1 to 1
- gain_mix: float32 [4096], P('kv'), may hold values from 0.1 to 1.9
- query_weight: bfloat16 [4096, 2048], P('kv', 'tp'), may hold values from -0.09375 to 0.09375
- forget_weight: bfloat16 [4096, 2048], P('kv', 'tp'), may hold values from -0.09375 to 0.09375
- input_weight: bfloat16 [4096, 2048], P('kv', 'tp'), may hold values from -0.09375 to 0.09375
- outgate_weight: bfloat16 [4096, 2048], P('kv', 'tp'), may hold values from -0.09375 to 0.09375
- forget_floor: float32 [2048], P('tp'), may hold values from 0 to 0.9
- head_gain: float32 [128], replicated, may hold values from 0.1 to 1.9
- mix_weight: bfloat16 [2048, 4096], P('tp', 'kv'), may hold values from -1 to 1
- gain_post: float32 [4096], P('kv'), may hold values from 0.1 to 1.9
- post_gate: bfloat16 [4096, 11264], P('kv', 'tp'), may hold values from -0.09375 to 0.09375
- post_up: bfloat16 [4096, 11264], P('kv', 'tp'), may hold values from -0.09375 to 0.09375
- post_down: bfloat16 [11264, 4096], P('tp', 'kv'), may hold values from -0.0546875 to 0.0546875
Outputs:
- out_tokens: bfloat16 [256, 4096], P(None, ('kv', 'tp'))
- new_states: float32 [64, 16, 128, 128], P('kv', 'tp')
Inputs may be any that keep to these rules, and one draw needn't show every extreme that they name: `lengths`: each of the 64 sequences has 1 to 4 new tokens, 128 in all, and at least one has exactly 4.
All inputs are finite; a program needn't handle non-finite values.
Results may differ from a plain program's by a relative error of at most 0.011.
Values may be sent and summed in bfloat16 or wider, within the bound.
No kernel may reach another device: no remote copies, remote signals or barrier semaphores. Data moves between devices by JAX's collectives and lax.ppermute only.
A program may use at most 64 MiB of HBM per device.

v0:
```python
import jax
import jax.numpy as jnp
from jax import lax
from jax.sharding import PartitionSpec as P

D = 4096
DK = 128
W = 4


EPSILON = 1e-06


def sent_to_all(value, axis):
    copies = jnp.broadcast_to(value, (lax.axis_size(axis), *value.shape))
    return lax.all_to_all(copies, axis, split_axis=0, concat_axis=0, tiled=True)


def joined_along(pieces, dim):
    pieces = jnp.moveaxis(pieces, 0, dim)
    dims = pieces.shape
    return pieces.reshape(*dims[:dim], dims[dim] * dims[dim + 1], *dims[dim + 2 :])


def gathered_copies(value, axis, dim):
    pieces = sent_to_all(value, axis)
    return joined_along(pieces, dim)


def taken_together(value, axis):
    return sent_to_all(value, axis).sum(axis=0)


def cut_along(value, dim, count):
    before, after = (value.shape[:dim], value.shape[dim + 1 :])
    return jnp.moveaxis(value.reshape(*before, count, -1, *after), dim, 0)


def sent_and_summed(value, axis, dim):
    count = lax.axis_size(axis)
    pieces = lax.all_to_all(cut_along(value, dim, count), axis, 0, 0, tiled=True)
    return jnp.sum(pieces, axis=0)


def gathered_norm(shard, gain_block):
    gathered = gathered_copies(shard, "tp", 1)
    block_squares = jnp.sum(jnp.square(gathered.astype(jnp.float32)), axis=1)
    totals = taken_together(block_squares, "kv")
    scale = lax.rsqrt(totals[:, None] / D + EPSILON)
    return (gathered.astype(jnp.float32) * scale * gain_block).astype(jnp.bfloat16)


def half_mixer(shard, gain_block, gate_weight, up_weight, down_weight):
    normed = gathered_norm(shard, gain_block)
    half_cols = gate_weight.shape[1]
    owned = sent_and_summed(
        jnp.concatenate(
            [
                jnp.dot(normed, gate_weight, preferred_element_type=jnp.float32),
                jnp.dot(normed, up_weight, preferred_element_type=jnp.float32),
            ],
            axis=1,
        ),
        "kv",
        0,
    )
    hidden = (jax.nn.silu(owned[:, :half_cols]) * owned[:, half_cols:]).astype(jnp.bfloat16)
    partial_out = jnp.dot(
        gathered_copies(hidden, "kv", 0), down_weight, preferred_element_type=jnp.float32
    )
    return sent_and_summed(partial_out, "tp", 1)


def packing_table(lengths, slot_count):
    seq_count = lengths.shape[0]
    starts = jnp.cumsum(lengths) - lengths
    slots = jnp.arange(slot_count, dtype=jnp.int32)
    seq_of = slots // W
    within = slots % W
    owner_len = jnp.sum(
        jnp.where(
            seq_of[:, None] == jnp.arange(seq_count, dtype=jnp.int32)[None, :], lengths[None, :], 0
        ),
        axis=1,
    )
    owner_start = jnp.sum(
        jnp.where(
            seq_of[:, None] == jnp.arange(seq_count, dtype=jnp.int32)[None, :], starts[None, :], 0
        ),
        axis=1,
    )
    target = jnp.where(within < owner_len, owner_start + within, -1)
    packed_count = slot_count // 2
    return (jnp.arange(packed_count, dtype=jnp.int32)[:, None] == target[None, :]).astype(
        jnp.float32
    )


def local(
    tokens,
    lengths,
    states,
    gain_pre,
    pre_gate,
    pre_up,
    pre_down,
    gain_mix,
    query_weight,
    forget_weight,
    input_weight,
    outgate_weight,
    forget_floor,
    head_gain,
    mix_weight,
    gain_post,
    post_gate,
    post_up,
    post_down,
):
    slot_count = tokens.shape[0]
    table = packing_table(lengths, slot_count)
    table_half = table.astype(jnp.bfloat16)
    spread_half = jnp.transpose(table).astype(jnp.bfloat16)
    entry = jnp.dot(table_half, tokens, preferred_element_type=jnp.float32).astype(jnp.bfloat16)
    resid_one = (
        entry.astype(jnp.float32) + 0.5 * half_mixer(entry, gain_pre, pre_gate, pre_up, pre_down)
    ).astype(jnp.bfloat16)
    normed = gathered_norm(resid_one, gain_mix)
    normed = jnp.dot(spread_half, normed, preferred_element_type=jnp.float32).astype(jnp.bfloat16)
    head_cols = query_weight.shape[1]
    seq_local = states.shape[0]
    heads_local = states.shape[1]
    owned = sent_and_summed(
        jnp.concatenate(
            [
                jnp.dot(normed, query_weight, preferred_element_type=jnp.float32),
                jnp.dot(normed, forget_weight, preferred_element_type=jnp.float32),
                jnp.dot(normed, input_weight, preferred_element_type=jnp.float32),
                jnp.dot(normed, outgate_weight, preferred_element_type=jnp.float32),
            ],
            axis=1,
        ),
        "kv",
        0,
    )
    shape_four = (seq_local, W, heads_local, DK)
    queries = jax.nn.silu(owned[:, :head_cols]).reshape(shape_four)
    forget_raw = owned[:, head_cols : 2 * head_cols].reshape(shape_four)
    fresh_values = owned[:, 2 * head_cols : 3 * head_cols].reshape(shape_four)
    gating = owned[:, 3 * head_cols :].reshape(shape_four)
    local_lengths = lax.dynamic_slice_in_dim(lengths, lax.axis_index("kv") * seq_local, seq_local)
    live_mask = jnp.arange(W, dtype=jnp.int32)[None, :] < local_lengths[:, None]
    live_four = live_mask[:, :, None, None]
    floors = forget_floor.reshape(heads_local, DK)
    forgets = jnp.where(
        live_four, floors + (1.0 - floors) * jax.nn.sigmoid(forget_raw), jnp.float32(1.0)
    )
    write_rate = 1.0 - forgets
    carried = states
    readings = []
    for offset in range(W):
        carried = (
            forgets[:, offset, :, :, None] * carried
            + write_rate[:, offset, :, :, None] * fresh_values[:, offset, :, None, :]
        )
        readings.append(
            jnp.einsum(
                "bhk,bhkv->bhv", queries[:, offset], carried, precision=lax.Precision.HIGHEST
            )
        )
    read_out = jnp.stack(readings, axis=1)
    meansq = jnp.mean(read_out * read_out, axis=3, keepdims=True)
    head_out = (
        (
            read_out
            * lax.rsqrt(meansq + EPSILON)
            * head_gain
            * jax.nn.silu(gating)
            * live_four.astype(jnp.float32)
        )
        .astype(jnp.bfloat16)
        .reshape(seq_local * W, heads_local * DK)
    )
    mixed_part = jnp.dot(
        gathered_copies(head_out, "kv", 0), mix_weight, preferred_element_type=jnp.float32
    )
    mixed_part = jnp.dot(
        table, mixed_part, preferred_element_type=jnp.float32, precision=lax.Precision.HIGHEST
    )
    mixed = sent_and_summed(mixed_part, "tp", 1)
    resid_two = (resid_one.astype(jnp.float32) + mixed).astype(jnp.bfloat16)
    finished = resid_two.astype(jnp.float32) + 0.5 * half_mixer(
        resid_two, gain_post, post_gate, post_up, post_down
    )
    outcome = jnp.dot(
        spread_half, finished.astype(jnp.bfloat16), preferred_element_type=jnp.float32
    ).astype(jnp.bfloat16)
    return (outcome, carried)


def solution(mesh):
    placed = (
        P(None, ("kv", "tp")),
        P(),
        P("kv", "tp", None, None),
        P("kv"),
        P("kv", "tp"),
        P("kv", "tp"),
        P("tp", "kv"),
        P("kv"),
        P("kv", "tp"),
        P("kv", "tp"),
        P("kv", "tp"),
        P("kv", "tp"),
        P("tp"),
        P(),
        P("tp", "kv"),
        P("kv"),
        P("kv", "tp"),
        P("kv", "tp"),
        P("tp", "kv"),
    )
    return jax.shard_map(
        local,
        mesh=mesh,
        in_specs=placed,
        out_specs=(P(None, ("kv", "tp")), P("kv", "tp", None, None)),
        check_vma=False,
    )
```

profile of v0, /device:TPU:1, one launch (start us, length us, event | category | flops | bytes accessed | tf_op | source)
XLA Modules:
  0.0 338.8 jit_solution(1746809235819680676)
XLA Ops:
  0.7 0.7 copy-done.15
  1.5 0.1 reduce.10
  1.8 0.7 copy-done.18
  2.5 0.1 convolution_convert_fusion.2
  2.6 13.8 %all_to_all.78 = bf16[16,128,8]{1,2,0:T(8,128)(2,1)S(1)} all-to-all(bf16[16,128,8]{1,2,0:T(8,128)(2,1)S(1)} %broadcast_in_dim.80), channel_id=1, replica_groups=mesh['kv'=32,'tp'=16] {'tp'}, dimensions={0} | all-to-all | bytes 65536 | tf_op jit(solution)/shard_map/all_to_all | solution.py:16
  16.5 29.0 %all_to_all.79 = f32[32,1,128]{2,1,0:T(1,128)S(1)} all-to-all(f32[32,1,128]{2,1,0:T(1,128)S(1)} %broadcast_in_dim.81), channel_id=1, replica_groups=mesh['kv'=32,'tp'=16] {'kv'}, dimensions={0} | all-to-all | bytes 32768 | tf_op jit(solution)/shard_map/all_to_all | solution.py:16
  45.5 0.6 copy-done.13
  46.1 0.2 fusion.43
  46.4 0.7 copy-done.5
  47.1 0.3 fusion.45
  47.4 0.3 copy.62
  47.6 0.2 reshape.457
  47.8 45.4 %all_to_all.80 = f32[32,4,1408]{2,1,0:T(4,128)S(1)} all-to-all(f32[32,4,1408]{2,1,0:T(4,128)S(1)} %reshape.457), channel_id=1, replica_groups=mesh['kv'=32,'tp'=16] {'kv'}, dimensions={0} | all-to-all | bytes 1441792 | tf_op jit(solution)/shard_map/all_to_all | solution.py:41
  93.2 0.1 reduce_sum.139
  93.4 0.7 broadcast_in_dim.82
  94.2 4.6 %all-to-all-start.3 = ((bf16[32,4,704]{2,1,0:T(4,128)(2,1)}), bf16[32,4,704]{2,1,0:T(4,128)(2,1)S(1)}, u32[]{:S(2)}, u32[]{:S(2)}) async-start(bf16[32,4,704]{2,1,0:T(4,128)(2,1)} %broadcast_in_dim.82), calls=%async_computation.3 | async-start | bytes 393216 | tf_op jit(solution)/shard_map/all_to_all | solution.py:16
  98.8 0.1 copy.63
  98.9 18.8 %all-to-all-done.3 = bf16[32,4,704]{2,1,0:T(4,128)(2,1)S(1)} async-done(((bf16[32,4,704]{2,1,0:T(4,128)(2,1)}), bf16[32,4,704]{2,1,0:T(4,128)(2,1)S(1)}, u32[]{:S(2)}, u32[]{:S(2)}) %all-to-all-start.3) | async-done | bytes 180256 | tf_op jit(solution)/shard_map/all_to_all | solution.py:16
  117.8 0.2 convolution_bitcast_fusion.2
  118.1 9.3 %all_to_all.81 = f32[16,128,8]{1,2,0:T(8,128)S(1)} all-to-all(f32[16,128,8]{1,2,0:T(8,128)S(1)} %copy.66), channel_id=1, replica_groups=mesh['kv'=32,'tp'=16] {'tp'}, dimensions={0} | all-to-all | bytes 131072 | tf_op jit(solution)/shard_map/all_to_all | solution.py:41
  127.4 9.6 %all_to_all.82 = bf16[16,128,8]{1,2,0:T(8,128)(2,1)S(1)} all-to-all(bf16[16,128,8]{1,2,0:T(8,128)(2,1)S(1)} %broadcast_in_dim.83), channel_id=1, replica_groups=mesh['kv'=32,'tp'=16] {'tp'}, dimensions={0} | all-to-all | bytes 65536 | tf_op jit(solution)/shard_map/all_to_all | solution.py:16
  137.1 18.5 %all_to_all.83 = f32[32,1,128]{2,1,0:T(1,128)S(1)} all-to-all(f32[32,1,128]{2,1,0:T(1,128)S(1)} %broadcast_in_dim.84), channel_id=1, replica_groups=mesh['kv'=32,'tp'=16] {'kv'}, dimensions={0} | all-to-all | bytes 32768 | tf_op jit(solution)/shard_map/all_to_all | solution.py:16
  155.5 0.6 copy-done.19
  156.2 0.2 convolution_convert_fusion
  156.4 0.5 copy-done.8
  156.9 0.2 fusion.57
  157.2 0.5 copy-done.9
  157.7 0.2 fusion.58
  157.9 0.5 copy-done.10
  158.5 0.2 fusion.59
  158.7 0.5 copy-done.11
  159.2 0.2 fusion.60
  159.5 1.0 copy.68
  160.5 4.4 %all-to-all-start.7 = ((f32[32,8,512]{2,1,0:T(8,128)}), f32[32,8,512]{2,1,0:T(8,128)S(1)}, u32[]{:S(2)}, u32[]{:S(2)}) async-start(f32[32,8,512]{2,1,0:T(8,128)} %bitcast.11), calls=%async_computation.7 | async-start | bytes 1048576 | tf_op jit(solution)/shard_map/all_to_all | solution.py:41
  165.1 0.6 copy-done.16
  165.7 32.7 %all-to-all-done.7 = f32[32,8,512]{2,1,0:T(8,128)S(1)} async-done(((f32[32,8,512]{2,1,0:T(8,128)}), f32[32,8,512]{2,1,0:T(8,128)S(1)}, u32[]{:S(2)}, u32[]{:S(2)}) %all-to-all-start.7) | async-done | bytes 524320 | tf_op jit(solution)/shard_map/all_to_all | solution.py:41
  198.6 0.3 convolution_bitcast_fusion.6
  198.9 0.4 convolution_bitcast_fusion.5
  199.3 0.5 convolution_bitcast_fusion.4
  199.8 0.3 multiply_add_fusion
  200.2 0.2 convolution_bitcast_fusion.3
  200.4 0.1 multiply_reduce_fusion
  200.6 0.7 copy-done.17
  201.4 16.4 %all_to_all.84 = bf16[32,8,128]{2,1,0:T(8,128)(2,1)S(1)} all-to-all(bf16[32,8,128]{2,1,0:T(8,128)(2,1)S(1)} %broadcast_in_dim.86), channel_id=1, replica_groups=mesh['kv'=32,'tp'=16] {'kv'}, dimensions={0} | all-to-all | bytes 131072 | tf_op jit(solution)/shard_map/all_to_all | solution.py:16
  217.8 0.1 fusion.20
  217.9 0.3 convolution_bitcast_fusion
  218.2 9.5 %all_to_all.85 = f32[16,128,8]{1,2,0:T(8,128)S(1)} all-to-all(f32[16,128,8]{1,2,0:T(8,128)S(1)} %convolution_bitcast_fusion), channel_id=1, replica_groups=mesh['kv'=32,'tp'=16] {'tp'}, dimensions={0} | all-to-all | bytes 131072 | tf_op jit(solution)/shard_map/all_to_all | solution.py:41
  227.8 9.6 %all_to_all.86 = bf16[16,128,8]{1,2,0:T(8,128)(2,1)S(1)} all-to-all(bf16[16,128,8]{1,2,0:T(8,128)(2,1)S(1)} %broadcast_in_dim.87), channel_id=1, replica_groups=mesh['kv'=32,'tp'=16] {'tp'}, dimensions={0} | all-to-all | bytes 65536 | tf_op jit(solution)/shard_map/all_to_all | solution.py:16
  237.4 18.8 %all_to_all.87 = f32[32,1,128]{2,1,0:T(1,128)S(1)} all-to-all(f32[32,1,128]{2,1,0:T(1,128)S(1)} %broadcast_in_dim.88), channel_id=1, replica_groups=mesh['kv'=32,'tp'=16] {'kv'}, dimensions={0} | all-to-all | bytes 32768 | tf_op jit(solution)/shard_map/all_to_all | solution.py:16
  256.2 0.6 copy-done.14
  256.8 0.3 fusion.39
  257.1 0.7 copy-done.7
  257.7 0.3 fusion.41
  258.0 0.3 copy.70
  258.3 0.2 reshape.472
  258.5 45.3 %all_to_all.88 = f32[32,4,1408]{2,1,0:T(4,128)S(1)} all-to-all(f32[32,4,1408]{2,1,0:T(4,128)S(1)} %reshape.472), channel_id=1, replica_groups=mesh['kv'=32,'tp'=16] {'kv'}, dimensions={0} | all-to-all | bytes 1441792 | tf_op jit(solution)/shard_map/all_to_all | solution.py:41
  303.9 0.1 reduce_sum.148
  304.1 0.7 broadcast_in_dim.89
  304.8 4.6 %all-to-all-start.13 = ((bf16[32,4,704]{2,1,0:T(4,128)(2,1)}), bf16[32,4,704]{2,1,0:T(4,128)(2,1)S(1)}, u32[]{:S(2)}, u32[]{:S(2)}) async-start(bf16[32,4,704]{2,1,0:T(4,128)(2,1)} %broadcast_in_dim.89), calls=%async_computation.13 | async-start | bytes 393216 | tf_op jit(solution)/shard_map/all_to_all | solution.py:16
  309.4 0.1 copy.71
  309.6 18.8 %all-to-all-done.13 = bf16[32,4,704]{2,1,0:T(4,128)(2,1)S(1)} async-done(((bf16[32,4,704]{2,1,0:T(4,128)(2,1)}), bf16[32,4,704]{2,1,0:T(4,128)(2,1)S(1)}, u32[]{:S(2)}, u32[]{:S(2)}) %all-to-all-start.13) | async-done | bytes 180256 | tf_op jit(solution)/shard_map/all_to_all | solution.py:16
  328.5 0.2 convolution_bitcast_fusion.1
  328.7 9.3 %all_to_all.89 = f32[16,128,8]{1,2,0:T(8,128)S(1)} all-to-all(f32[16,128,8]{1,2,0:T(8,128)S(1)} %copy.74), channel_id=1, replica_groups=mesh['kv'=32,'tp'=16] {'tp'}, dimensions={0} | all-to-all | bytes 131072 | tf_op jit(solution)/shard_map/all_to_all | solution.py:41
  338.0 0.8 convolution_convert_fusion.1
  (75 shorter events, 1.7 us)
Async XLA Ops:
  0.6 44.9 %copy-start = (bf16[128,704]{0,1:T(8,128)(2,1)S(1)}, bf16[128,704]{0,1:T(8,128)(2,1)}, u32[]{:S(2)}) copy-start(bf16[128,704]{0,1:T(8,128)(2,1)} %param.23) | copy-start | bytes 540676
  0.7 0.7 copy-start.15
  1.8 0.7 copy-start.18
  45.5 0.7 copy-start.13
  46.1 0.9 copy-start.5
  94.2 4.6 %copy-start.3 = (bf16[704,128]{1,0:T(8,128)(2,1)S(1)}, bf16[704,128]{1,0:T(8,128)(2,1)}, u32[]{:S(2)}) copy-start(bf16[704,128]{1,0:T(8,128)(2,1)} %param.25) | copy-start | bytes 540676
  94.2 23.6 %all-to-all-start.3 = ((bf16[32,4,704]{2,1,0:T(4,128)(2,1)}), bf16[32,4,704]{2,1,0:T(4,128)(2,1)S(1)}, u32[]{:S(2)}, u32[]{:S(2)}) async-start(bf16[32,4,704]{2,1,0:T(4,128)(2,1)} %broadcast_in_dim.82), calls=%async_computation.3 | async-start | bytes 393216 | tf_op jit(solution)/shard_map/all_to_all | solution.py:16
  155.5 0.7 copy-start.19
  156.2 0.8 copy-start.8
  156.9 0.8 copy-start.9
  157.7 0.8 copy-start.10
  158.5 0.8 copy-start.11
  160.5 38.0 %all-to-all-start.7 = ((f32[32,8,512]{2,1,0:T(8,128)}), f32[32,8,512]{2,1,0:T(8,128)S(1)}, u32[]{:S(2)}, u32[]{:S(2)}) async-start(f32[32,8,512]{2,1,0:T(8,128)} %bitcast.11), calls=%async_computation.7 | async-start | bytes 1048576 | tf_op jit(solution)/shard_map/all_to_all | solution.py:41
  165.1 0.7 copy-start.16
  165.7 32.9 %copy-start.1 = (f32[2,1,128,128]{3,2,1,0:T(8,128)S(1)}, f32[2,1,128,128]{3,2,1,0:T(8,128)}, u32[]{:S(2)}) copy-start(f32[2,1,128,128]{3,2,1,0:T(8,128)} %param.21) | copy-start | bytes 393220
  200.2 17.6 %copy-start.2 = (f32[2,1,128,128]{3,2,1,0:T(8,128)}, f32[2,1,128,128]{3,2,1,0:T(8,128)S(1)}, u32[]{:S(2)}) copy-start(f32[2,1,128,128]{3,2,1,0:T(8,128)S(1)} %multiply_add_fusion) | copy-start | bytes 393220
  200.6 0.7 copy-start.17
  201.3 16.5 %copy-start.12 = (bf16[128,128]{1,0:T(8,128)(2,1)S(1)}, bf16[128,128]{1,0:T(8,128)(2,1)}, u32[]{:S(2)}) copy-start(bf16[128,128]{1,0:T(8,128)(2,1)} %param.33) | copy-start | bytes 98308
  218.2 37.9 %copy-start.6 = (bf16[128,704]{0,1:T(8,128)(2,1)S(1)}, bf16[128,704]{0,1:T(8,128)(2,1)}, u32[]{:S(2)}) copy-start(bf16[128,704]{0,1:T(8,128)(2,1)} %param.35) | copy-start | bytes 540676
  256.1 0.7 copy-start.14
  256.8 0.9 copy-start.7
  304.8 4.6 %copy-start.4 = (bf16[704,128]{1,0:T(8,128)(2,1)S(1)}, bf16[704,128]{1,0:T(8,128)(2,1)}, u32[]{:S(2)}) copy-start(bf16[704,128]{1,0:T(8,128)(2,1)} %param.37) | copy-start | bytes 540676
  304.8 23.6 %all-to-all-start.13 = ((bf16[32,4,704]{2,1,0:T(4,128)(2,1)}), bf16[32,4,704]{2,1,0:T(4,128)(2,1)S(1)}, u32[]{:S(2)}, u32[]{:S(2)}) async-start(bf16[32,4,704]{2,1,0:T(4,128)(2,1)} %broadcast_in_dim.89), calls=%async_computation.13 | async-start | bytes 393216 | tf_op jit(solution)/shard_map/all_to_all | solution.py:16
where the time goes:
time: 340 us; the launch traced here: 339 us
  blocking collectives  234 us (69%)
  waiting for transfers between devices  70.3 us (21%)
  starting transfers between devices  13.6 us (4%)
  local copies, waits for them, and re-layouts  12.3 us (4%)
  matrix products  5.29 us (2%)
    all_to_all x5, blocking collectives, sent_and_summed(): lax.all_to_all(cut_along(value, dim, count), axis, 0, 0, tiled=True)  119 us
    all_to_all x7, blocking collectives, sent_to_all(): return lax.all_to_all(copies, axis, split_axis=0, concat_axis=0, tiled=True)  116 us
    all_to_all x2, waiting for transfers between devices, sent_to_all(): return lax.all_to_all(copies, axis, split_axis=0, concat_axis=0, tiled=True)  37.6 us
    all_to_all x1, waiting for transfers between devices, sent_and_summed(): lax.all_to_all(cut_along(value, dim, count), axis, 0, 0, tiled=True)  32.7 us
    all_to_all x2, starting transfers between devices, sent_to_all(): return lax.all_to_all(copies, axis, split_axis=0, concat_axis=0, tiled=True)  9.21 us
    unnamed x42, local copies, waits for them, and re-layouts  8.32 us
  transfers between devices with their start and end apart: 3, of which 3 were waited for; matrix products, arithmetic and copies ran while one was open for 0% of the time, Pallas kernels for 0%

commit v1 on v0

v1 whole, which is shorter than its diff:
```python
import jax
import jax.numpy as jnp
from jax import lax
from jax.sharding import Mesh
from jax.sharding import PartitionSpec as P

D = 4096
DK = 128
W = 4
EPSILON = 1e-06
LANES = 128

f32 = jnp.float32
bf16 = jnp.bfloat16


def exchanged(value, axis):
    return lax.all_to_all(value, axis, split_axis=0, concat_axis=0, tiled=True)


def sent_to_all(value, axis):
    return exchanged(jnp.broadcast_to(value, (lax.axis_size(axis), *value.shape)), axis)


def matmul(a, b):
    return jnp.dot(a, b, preferred_element_type=f32)


def split_three(values):
    high = lax.reduce_precision(values, 8, 7)
    rest = values - high
    mid = lax.reduce_precision(rest, 8, 7)
    return high, mid, rest - mid


def lane_padded(value, width):
    return jnp.pad(value, ((0, 0), (0, width - value.shape[1])))


def squares_of(rows):
    wide = rows.astype(f32)
    total = jnp.sum(wide * wide, axis=1, keepdims=True)
    high = lax.reduce_precision(total, 8, 7)
    return high, total - high


def slot_targets(lengths, slot_count):
    seq_count = lengths.shape[0]
    seqs = jnp.arange(seq_count, dtype=jnp.int32)
    slots = jnp.arange(slot_count, dtype=jnp.int32)
    seq_of = slots // W
    within = slots % W
    before = jnp.sum(jnp.where(seqs[None, :] < seq_of[:, None], lengths[None, :], 0), axis=1)
    own = jnp.sum(jnp.where(seqs[None, :] == seq_of[:, None], lengths[None, :], 0), axis=1)
    return jnp.where(within < own, before + within, -1)


def local(
    tokens,
    lengths,
    states,
    gain_pre,
    pre_gate,
    pre_up,
    pre_down,
    gain_mix,
    query_weight,
    forget_weight,
    input_weight,
    outgate_weight,
    forget_floor,
    head_gain,
    mix_weight,
    gain_post,
    post_gate,
    post_up,
    post_down,
):
    core = lax.axis_index("c")
    z_count = lax.axis_size("z")
    tp_count = lax.axis_size("tp")
    slot_count = tokens.shape[0]
    packed = slot_count // 2
    half = packed // 2
    per_z = half // z_count
    own_cols = gain_pre.shape[0]
    hidden = pre_gate.shape[1]
    wide = -(-hidden // LANES) * LANES
    head_cols = query_weight.shape[1]
    seq_local, heads_local = states.shape[:2]

    downs = jnp.concatenate([pre_down, post_down], axis=0)
    down_blocks = 2 * hidden // own_cols
    gain_rows = jnp.stack(
        [piece for gain in (gain_pre, gain_mix, gain_post) for piece in split_three(gain)]
    ).astype(bf16)
    gain_block = jnp.pad(gain_rows, ((0, own_cols - gain_rows.shape[0]), (0, 0)))
    mine = jnp.concatenate(
        [
            lane_padded(pre_gate, wide),
            lane_padded(pre_up, wide),
            lane_padded(post_gate, wide),
            lane_padded(post_up, wide),
            query_weight,
            forget_weight,
            input_weight,
            outgate_weight,
            mix_weight,
            gain_block,
        ]
        + [downs[i * own_cols : (i + 1) * own_cols] for i in range(down_blocks)],
        axis=1,
    )
    theirs = lax.ppermute(mine, "c", [(0, 1), (1, 0)])

    def unpacked(bundle):
        at = 4 * wide
        both_ff = (bundle[:, : 2 * wide], bundle[:, 2 * wide : at])
        heads = bundle[:, at : at + 4 * head_cols]
        at += 4 * head_cols
        mix = bundle[:, at : at + own_cols]
        at += own_cols
        gains = bundle[:9, at : at + own_cols].astype(f32)
        gains = [gains[3 * i] + gains[3 * i + 1] + gains[3 * i + 2] for i in range(3)]
        at += own_cols
        down = jnp.concatenate(
            [bundle[:, at + i * own_cols : at + (i + 1) * own_cols] for i in range(down_blocks)],
            axis=0,
        )
        return both_ff, heads, mix, gains, (down[:hidden], down[hidden:])

    ff_mine, heads_mine, mix_mine, _, _ = unpacked(mine)
    gains_mine = (gain_pre, gain_mix, gain_post)
    down_mine = (pre_down, post_down)
    ff_other, heads_other, mix_other, gains_other, down_other = unpacked(theirs)

    def both_gains(i):
        return jnp.concatenate([gains_mine[i], gains_other[i]])[None, :]

    targets = slot_targets(lengths, slot_count)
    rows = jnp.arange(packed, dtype=jnp.int32)
    table = rows[:, None] == targets[None, :]
    table_half = table.astype(bf16)

    entry = lax.dot_general(
        tokens, table_half, (((0,), (1,)), ((), ())), preferred_element_type=f32
    ).astype(bf16)
    pieces = jnp.stack([entry[:, :half], entry[:, half:]])
    pieces = jnp.broadcast_to(pieces[:, None], (2, tp_count, *pieces.shape[1:]))
    gathered = exchanged(pieces.reshape(2 * tp_count, *pieces.shape[2:]), ("c", "tp"))
    gathered = gathered.reshape(2, own_cols, half)
    gathered = jnp.where(core == 0, gathered, gathered[::-1])
    resid = gathered.reshape(2 * own_cols, half).T

    def ff_hidden(resid, which):
        scaled = (resid.astype(f32) * both_gains(0 if which == 0 else 2)).astype(bf16)
        product = matmul(scaled[:, :own_cols], ff_mine[which]) + matmul(
            scaled[:, own_cols:], ff_other[which]
        )
        high, low = squares_of(resid)
        lanes = jnp.arange(2 * wide, dtype=jnp.int32)[None, :]
        product = jnp.where(lanes == hidden, high, jnp.where(lanes == hidden + 1, low, product))
        sent = product.astype(bf16).reshape(z_count, per_z, 2 * wide)
        owned = jnp.sum(exchanged(sent, "z").astype(f32), axis=0)
        total = owned[:, hidden : hidden + 1] + owned[:, hidden + 1 : hidden + 2]
        scale = lax.rsqrt(total / D + EPSILON)
        gate = owned[:, :hidden] * scale
        up = owned[:, wide : wide + hidden] * scale
        act = (jax.nn.silu(gate) * up).astype(bf16)
        return sent_to_all(act, "z").reshape(half, hidden)

    def tp_summed(partial):
        return jnp.sum(sent_to_all(partial.astype(bf16), "tp").astype(f32), axis=0)

    act = ff_hidden(resid, 0)
    partial = jnp.concatenate([matmul(act, down_mine[0]), matmul(act, down_other[0])], axis=1)
    resid_one = (resid.astype(f32) + 0.5 * tp_summed(partial)).astype(bf16)

    turned = jnp.concatenate([resid_one[:, own_cols:], resid_one[:, :own_cols]], axis=1)
    all_rows = jnp.concatenate([resid_one, lax.ppermute(turned, "c", [(0, 1), (1, 0)])], axis=0)
    row_ids = jnp.where(core == 0, rows, (rows + half) % packed)
    by_owner = targets.reshape(z_count, 2, seq_local * W)
    own_targets = jnp.where(core == 0, by_owner[:, 0], by_owner[:, 1]).reshape(packed)
    spread = (own_targets[:, None] == row_ids[None, :]).astype(bf16)
    slot_rows = matmul(spread, all_rows).astype(bf16)
    scaled = (slot_rows.astype(f32) * both_gains(1)).astype(bf16)
    product = matmul(scaled[:, :own_cols], heads_mine) + matmul(scaled[:, own_cols:], heads_other)
    high, low = squares_of(slot_rows)
    lanes = jnp.arange(LANES, dtype=jnp.int32)[None, :]
    stats = jnp.where(lanes == 0, high, jnp.where(lanes == 1, low, 0.0))
    sent = jnp.concatenate([product, stats], axis=1).astype(bf16)
    sent = sent.reshape(z_count, seq_local * W, 4 * head_cols + LANES)
    owned = jnp.sum(exchanged(sent, "z").astype(f32), axis=0)
    at = 4 * head_cols
    total = owned[:, at : at + 1] + owned[:, at + 1 : at + 2]
    owned = owned[:, :at] * lax.rsqrt(total / D + EPSILON)

    shape_four = (seq_local, W, heads_local, DK)
    queries = jax.nn.silu(owned[:, :head_cols]).reshape(shape_four)
    forget_raw = owned[:, head_cols : 2 * head_cols].reshape(shape_four)
    fresh_values = owned[:, 2 * head_cols : 3 * head_cols].reshape(shape_four)
    gating = owned[:, 3 * head_cols :].reshape(shape_four)
    first_seq = (lax.axis_index("z") * 2 + core) * seq_local
    local_lengths = lax.dynamic_slice_in_dim(lengths, first_seq, seq_local)
    live_mask = jnp.arange(W, dtype=jnp.int32)[None, :] < local_lengths[:, None]
    live_four = live_mask[:, :, None, None]
    floors = forget_floor.reshape(heads_local, DK)
    forgets = jnp.where(
        live_four, floors + (1.0 - floors) * jax.nn.sigmoid(forget_raw), jnp.float32(1.0)
    )
    write_rate = 1.0 - forgets
    carried = states
    readings = []
    for offset in range(W):
        carried = (
            forgets[:, offset, :, :, None] * carried
            + write_rate[:, offset, :, :, None] * fresh_values[:, offset, :, None, :]
        )
        readings.append(jnp.sum(queries[:, offset, :, :, None] * carried, axis=2))
    read_out = jnp.stack(readings, axis=1)
    meansq = jnp.mean(read_out * read_out, axis=3, keepdims=True)
    head_out = (
        (
            read_out
            * lax.rsqrt(meansq + EPSILON)
            * head_gain
            * jax.nn.silu(gating)
            * live_four.astype(f32)
        )
        .astype(bf16)
        .reshape(seq_local * W, heads_local * DK)
    )
    all_heads = sent_to_all(head_out, ("z", "c")).reshape(slot_count, heads_local * DK)
    my_table = jnp.where(core == 0, table_half[:half], table_half[half:])
    head_rows = matmul(my_table, all_heads).astype(bf16)
    partial = jnp.concatenate([matmul(head_rows, mix_mine), matmul(head_rows, mix_other)], axis=1)
    resid_two = (resid_one.astype(f32) + tp_summed(partial)).astype(bf16)

    act = ff_hidden(resid_two, 1)
    contract = (((0,), (1,)), ((), ()))
    finish = jnp.stack(
        [
            lax.dot_general(down, act, contract, preferred_element_type=f32)
            for down in (down_mine[1], down_other[1])
        ]
    )
    first = (lax.axis_index("tp") == 0).astype(f32)
    residual = resid_two.astype(f32).T.reshape(2, own_cols, half)
    finish = 0.5 * finish + first * residual
    finish = jnp.where(core == 0, finish, finish[::-1])
    finish = finish.reshape(2 * tp_count, own_cols // tp_count, half)
    finished = jnp.sum(exchanged(finish, ("c", "tp")).reshape(2, tp_count, -1, half), axis=1)
    finished = jnp.concatenate([finished[0], finished[1]], axis=1).astype(bf16)
    outcome = lax.dot_general(
        table_half, finished, (((0,), (1,)), ((), ())), preferred_element_type=f32
    ).astype(bf16)
    return (outcome, carried)


def solution(mesh):
    kv = mesh.shape["kv"]
    tp = mesh.shape["tp"]
    cut = Mesh(mesh.devices.reshape(kv // 2, 2, tp), ("z", "c", "tp"))
    kv_axes = ("z", "c")
    placed = (
        P(None, ("z", "c", "tp")),
        P(),
        P(kv_axes, "tp", None, None),
        P(kv_axes),
        P(kv_axes, "tp"),
        P(kv_axes, "tp"),
        P("tp", kv_axes),
        P(kv_axes),
        P(kv_axes, "tp"),
        P(kv_axes, "tp"),
        P(kv_axes, "tp"),
        P(kv_axes, "tp"),
        P("tp"),
        P(),
        P("tp", kv_axes),
        P(kv_axes),
        P(kv_axes, "tp"),
        P(kv_axes, "tp"),
        P("tp", kv_axes),
    )
    return jax.shard_map(
        local,
        mesh=cut,
        in_specs=placed,
        out_specs=(P(None, ("z", "c", "tp")), P(kv_axes, "tp", None, None)),
        check_vma=False,
    )
```

time: 340 us -> 227 us (0.67)
  blocking collectives: 234 us -> 30.1 us
  starting transfers between devices: 13.6 us -> 68.3 us
  waiting for transfers between devices: 70.3 us -> 87.4 us
  local copies, waits for them, and re-layouts: 12.3 us -> 27.3 us
  other arithmetic: 1.84 us -> 7.49 us
    all_to_all x12 -> x2, blocking collectives: 234 us -> 30.1 us  [exchanged(): return lax.all_to_all(value, axis, split_axis=0, concat_axis=0, tiled=True)]
    all_to_all x3 -> x8, starting transfers between devices: 13.6 us -> 53.9 us  [exchanged(): return lax.all_to_all(value, axis, split_axis=0, concat_axis=0, tiled=True)]
    all_to_all x3 -> x8, waiting for transfers between devices: 70.3 us -> 86.6 us  [exchanged(): return lax.all_to_all(value, axis, split_axis=0, concat_axis=0, tiled=True)]
    ppermute x0 -> x2, starting transfers between devices: none -> 14.5 us  [the longest x1 8.73 us: local(): theirs = lax.ppermute(mine, 'c', [(0, 1), (1, 0)])]
    unnamed x42 -> x74, local copies, waits for them, and re-layouts: 8.32 us -> 18.5 us
  transfers between devices with their start and end apart: 3 -> 10, of which waited for: 3 -> 9; matrix products, arithmetic and copies ran while one was open for 0% -> 1% of each run, Pallas kernels for 0% -> 0%
where the time goes in v1:
time: 227 us; the launch traced here: 226 us
  waiting for transfers between devices  87.4 us (39%)
  starting transfers between devices  68.3 us (30%)
  blocking collectives  30.1 us (13%)
  local copies, waits for them, and re-layouts  27.3 us (12%)
  other arithmetic  7.49 us (3%)
  matrix products  3.78 us (2%)
    all_to_all x8, waiting for transfers between devices, exchanged(): return lax.all_to_all(value, axis, split_axis=0, concat_axis=0, tiled=True)  86.6 us
    all_to_all x8, starting transfers between devices, exchanged(): return lax.all_to_all(value, axis, split_axis=0, concat_axis=0, tiled=True)  53.9 us
    all_to_all x2, blocking collectives, exchanged(): return lax.all_to_all(value, axis, split_axis=0, concat_axis=0, tiled=True)  30.1 us
    unnamed x74, local copies, waits for them, and re-layouts  18.5 us
    ppermute x1, starting transfers between devices, local(): theirs = lax.ppermute(mine, 'c', [(0, 1), (1, 0)])  8.73 us
    ppermute x1, starting transfers between devices, local(): lax.ppermute(turned, 'c', [(0, 1), (1, 0)])  5.72 us
  transfers between devices with their start and end apart: 10, of which 9 were waited for; matrix products, arithmetic and copies ran while one was open for 1% of the time, Pallas kernels for 0%

profile of v1, /device:TPU:1, one launch (start us, length us, event | category | flops | bytes accessed | tf_op | source)
XLA Modules:
  0.0 225.9 jit_solution(4390293936203612636)
XLA Ops:
  0.6 0.7 fusion.99
  1.3 0.7 fusion.91
  2.2 1.7 constant_dynamic-update-slice_fusion.20
  3.9 0.9 copy.157
  4.8 0.9 copy.158
  5.7 0.9 copy.159
  6.5 0.9 copy.160
  7.4 0.9 copy.161
  8.3 1.0 fusion.109
  10.7 0.7 constant_dynamic-update-slice_fusion.19
  11.4 0.7 fusion.107
  12.1 0.7 fusion.108
  12.8 0.6 constant_dynamic-update-slice_fusion.16
  13.4 0.6 constant_dynamic-update-slice_fusion.15
  14.0 0.6 constant_dynamic-update-slice_fusion.14
  14.6 0.6 constant_dynamic-update-slice_fusion.13
  15.2 0.6 constant_dynamic-update-slice_fusion.12
  15.8 0.6 constant_dynamic-update-slice_fusion.11
  16.4 0.6 constant_dynamic-update-slice_fusion.10
  17.0 0.6 constant_dynamic-update-slice_fusion.9
  17.7 0.6 constant_dynamic-update-slice_fusion.8
  18.3 0.6 constant_dynamic-update-slice_fusion.7
  18.9 0.6 constant_dynamic-update-slice_fusion.6
  19.5 0.6 constant_dynamic-update-slice_fusion.5
  20.1 0.6 constant_dynamic-update-slice_fusion.4
  20.7 0.6 constant_dynamic-update-slice_fusion.3
  21.3 0.6 constant_dynamic-update-slice_fusion.2
  21.9 0.6 constant_dynamic-update-slice_fusion.1
  22.5 0.6 constant_dynamic-update-slice_fusion
  23.1 8.7 %collective-permute-start = (bf16[128,5248]{0,1:T(8,128)(2,1)}, bf16[128,5248]{0,1:T(8,128)(2,1)S(1)}, u32[]{:S(2)}, u32[]{:S(2)}) collective-permute-start(bf16[128,5248]{0,1:T(8,128)(2,1)} %constant_dynamic-update-slice_fusion), channel_id=1, source_target_pairs={{0,16},{16,0},{1,17},{17,1},{2,18},{18,2},{3,19},{19,3},{4,20},{20... | collective-permute-start | bytes 4030472 | tf_op jit(solution)/shard_map/ppermute | solution.py:114
  32.2 0.7 reshape.509
  33.0 3.6 %all-to-all-start = ((bf16[32,2,256]{2,1,0:T(2,128)(2,1)}), bf16[32,2,256]{2,1,0:T(2,128)(2,1)S(1)}, u32[]{:S(2)}, u32[]{:S(2)}) async-start(bf16[32,2,256]{2,1,0:T(2,128)(2,1)} %reshape.509), calls=%async_computation | async-start | bytes 65536 | tf_op jit(solution)/shard_map/all_to_all | solution.py:18
  36.8 6.7 %all-to-all-done = bf16[32,2,256]{2,1,0:T(2,128)(2,1)S(1)} async-done(((bf16[32,2,256]{2,1,0:T(2,128)(2,1)}), bf16[32,2,256]{2,1,0:T(2,128)(2,1)S(1)}, u32[]{:S(2)}, u32[]{:S(2)}) %all-to-all-start) | async-done | bytes 32800 | tf_op jit(solution)/shard_map/all_to_all | solution.py:18
  43.8 0.3 fusion.41
  44.8 0.7 reshape.484
  45.5 13.2 %all-to-all-start.1 = ((bf16[16,4,1536]{2,1,0:T(4,128)(2,1)}), bf16[16,4,1536]{2,1,0:T(4,128)(2,1)S(1)}, u32[]{:S(2)}, u32[]{:S(2)}) async-start(bf16[16,4,1536]{2,1,0:T(4,128)(2,1)} %reshape.484), calls=%async_computation.1 | async-start | bytes 393216 | tf_op jit(solution)/shard_map/all_to_all | solution.py:18
  58.8 12.4 %all-to-all-done.1 = bf16[16,4,1536]{2,1,0:T(4,128)(2,1)S(1)} async-done(((bf16[16,4,1536]{2,1,0:T(4,128)(2,1)}), bf16[16,4,1536]{2,1,0:T(4,128)(2,1)S(1)}, u32[]{:S(2)}, u32[]{:S(2)}) %all-to-all-start.1) | async-done | bytes 196640 | tf_op jit(solution)/shard_map/all_to_all | solution.py:18
  71.6 0.7 broadcast_in_dim.164
  72.3 8.9 %all-to-all-start.2 = ((bf16[16,4,704]{2,1,0:T(4,128)(2,1)}), bf16[16,4,704]{2,1,0:T(4,128)(2,1)S(1)}, u32[]{:S(2)}, u32[]{:S(2)}) async-start(bf16[16,4,704]{2,1,0:T(4,128)(2,1)} %broadcast_in_dim.164), calls=%async_computation.2 | async-start | bytes 196608 | tf_op jit(solution)/shard_map/all_to_all | solution.py:18
  81.2 11.8 %all-to-all-done.2 = bf16[16,4,704]{2,1,0:T(4,128)(2,1)S(1)} async-done(((bf16[16,4,704]{2,1,0:T(4,128)(2,1)}), bf16[16,4,704]{2,1,0:T(4,128)(2,1)S(1)}, u32[]{:S(2)}, u32[]{:S(2)}) %all-to-all-start.2) | async-done | bytes 90144 | tf_op jit(solution)/shard_map/all_to_all | solution.py:18
  93.5 0.8 broadcast_in_dim.165
  94.4 3.6 %all-to-all-start.3 = ((bf16[16,64,256]{2,1,0:T(8,128)(2,1)}), bf16[16,64,256]{2,1,0:T(8,128)(2,1)S(1)}, u32[]{:S(2)}, u32[]{:S(2)}) async-start(bf16[16,64,256]{2,1,0:T(8,128)(2,1)} %broadcast_in_dim.165), calls=%async_computation.3 | async-start | bytes 1048576 | tf_op jit(solution)/shard_map/all_to_all | solution.py:18
  98.1 8.8 %all-to-all-done.3 = bf16[16,64,256]{2,1,0:T(8,128)(2,1)S(1)} async-done(((bf16[16,64,256]{2,1,0:T(8,128)(2,1)}), bf16[16,64,256]{2,1,0:T(8,128)(2,1)S(1)}, u32[]{:S(2)}, u32[]{:S(2)}) %all-to-all-start.3) | async-done | bytes 524320 | tf_op jit(solution)/shard_map/all_to_all | solution.py:18
  107.1 5.7 %collective-permute-start.1 = (bf16[64,256]{1,0:T(8,128)(2,1)S(1)}, bf16[64,256]{1,0:T(8,128)(2,1)S(1)}, u32[]{:S(2)}, u32[]{:S(2)}) collective-permute-start(bf16[64,256]{1,0:T(8,128)(2,1)S(1)} %pad_maximum_fusion.3), channel_id=1, source_target_pairs={{0,16},{16,0},{1,17},{17,1},{2,18},{18,2},{3,19},{19,3},{4,20},{20... | collective-permute-start | bytes 98312 | tf_op jit(solution)/shard_map/ppermute | solution.py:180
  112.9 0.8 collective-permute-done.1
  113.7 0.3 multiply_convert_fusion
  114.6 0.7 pad_maximum_fusion
  115.3 4.4 %all-to-all-start.4 = ((bf16[16,8,640]{2,1,0:T(8,128)(2,1)}), bf16[16,8,640]{2,1,0:T(8,128)(2,1)S(1)}, u32[]{:S(2)}, u32[]{:S(2)}) async-start(bf16[16,8,640]{2,1,0:T(8,128)(2,1)} %pad_maximum_fusion), calls=%async_computation.4 | async-start | bytes 327680 | tf_op jit(solution)/shard_map/all_to_all | solution.py:18
  120.0 12.0 %all-to-all-done.4 = bf16[16,8,640]{2,1,0:T(8,128)(2,1)S(1)} async-done(((bf16[16,8,640]{2,1,0:T(8,128)(2,1)}), bf16[16,8,640]{2,1,0:T(8,128)(2,1)S(1)}, u32[]{:S(2)}, u32[]{:S(2)}) %all-to-all-start.4) | async-done | bytes 163872 | tf_op jit(solution)/shard_map/all_to_all | solution.py:18
  132.5 1.1 multiply_reduce_fusion.2
  133.9 0.6 broadcast_in_dim.173
  134.6 8.7 %all-to-all-start.5 = ((bf16[32,8,128]{2,1,0:T(8,128)(2,1)}), bf16[32,8,128]{2,1,0:T(8,128)(2,1)S(1)}, u32[]{:S(2)}, u32[]{:S(2)}) async-start(bf16[32,8,128]{2,1,0:T(8,128)(2,1)} %broadcast_in_dim.173), calls=%async_computation.5 | async-start | bytes 131072 | tf_op jit(solution)/shard_map/all_to_all | solution.py:18
  143.3 13.0 %all-to-all-done.5 = bf16[32,8,128]{2,1,0:T(8,128)(2,1)S(1)} async-done(((bf16[32,8,128]{2,1,0:T(8,128)(2,1)}), bf16[32,8,128]{2,1,0:T(8,128)(2,1)S(1)}, u32[]{:S(2)}, u32[]{:S(2)}) %all-to-all-start.5) | async-done | bytes 65568 | tf_op jit(solution)/shard_map/all_to_all | solution.py:18
  156.7 0.9 broadcast_in_dim.174
  157.6 3.6 %all-to-all-start.6 = ((bf16[16,64,256]{2,1,0:T(8,128)(2,1)}), bf16[16,64,256]{2,1,0:T(8,128)(2,1)S(1)}, u32[]{:S(2)}, u32[]{:S(2)}) async-start(bf16[16,64,256]{2,1,0:T(8,128)(2,1)} %broadcast_in_dim.174), calls=%async_computation.6 | async-start | bytes 1048576 | tf_op jit(solution)/shard_map/all_to_all | solution.py:18
  161.2 10.1 %all-to-all-done.6 = bf16[16,64,256]{2,1,0:T(8,128)(2,1)S(1)} async-done(((bf16[16,64,256]{2,1,0:T(8,128)(2,1)}), bf16[16,64,256]{2,1,0:T(8,128)(2,1)S(1)}, u32[]{:S(2)}, u32[]{:S(2)}) %all-to-all-start.6) | async-done | bytes 524320 | tf_op jit(solution)/shard_map/all_to_all | solution.py:18
  172.0 15.7 %all_to_all.50 = bf16[16,4,1536]{2,1,0:T(4,128)(2,1)S(1)} all-to-all(bf16[16,4,1536]{2,1,0:T(4,128)(2,1)S(1)} %reshape.489), channel_id=1, replica_groups=mesh['z'=16,'c'=2,'tp'=16] {'z'}, dimensions={0} | all-to-all | bytes 393216 | tf_op jit(solution)/shard_map/all_to_all | solution.py:18
  188.1 0.7 broadcast_in_dim.177
  188.8 7.9 %all-to-all-start.8 = ((bf16[16,4,704]{2,1,0:T(4,128)(2,1)}), bf16[16,4,704]{2,1,0:T(4,128)(2,1)S(1)}, u32[]{:S(2)}, u32[]{:S(2)}) async-start(bf16[16,4,704]{2,1,0:T(4,128)(2,1)} %broadcast_in_dim.177), calls=%async_computation.8 | async-start | bytes 196608 | tf_op jit(solution)/shard_map/all_to_all | solution.py:18
  196.7 11.8 %all-to-all-done.8 = bf16[16,4,704]{2,1,0:T(4,128)(2,1)S(1)} async-done(((bf16[16,4,704]{2,1,0:T(4,128)(2,1)}), bf16[16,4,704]{2,1,0:T(4,128)(2,1)S(1)}, u32[]{:S(2)}, u32[]{:S(2)}) %all-to-all-start.8) | async-done | bytes 90144 | tf_op jit(solution)/shard_map/all_to_all | solution.py:18
  209.3 14.4 %all_to_all.51 = f32[32,1,512]{2,1,0:T(1,128)S(1)} all-to-all(f32[32,1,512]{2,1,0:T(1,128)S(1)} %reshape.511), channel_id=1, replica_groups=mesh['z'=16,'c'=2,'tp'=16] {'c','tp'}, dimensions={0} | all-to-all | bytes 131072 | tf_op jit(solution)/shard_map/all_to_all | solution.py:18
  223.7 0.5 broadcast.469
  224.2 0.8 reduce.21
  225.1 0.8 convolution_convert_fusion.6
  (140 shorter events, 8.1 us)
Async XLA Ops:
  0.6 31.4 %copy-start = (bf16[256,8]{0,1:T(8,128)(2,1)S(1)}, bf16[256,8]{0,1:T(8,128)(2,1)}, u32[]{:S(2)}) copy-start(bf16[256,8]{0,1:T(8,128)(2,1)} %param.19) | copy-start | bytes 12292
  2.2 8.5 %copy-start.3 = (bf16[128,704]{0,1:T(8,128)(2,1)S(1)}, bf16[128,704]{0,1:T(8,128)(2,1)}, u32[]{:S(2)}) copy-start(bf16[128,704]{0,1:T(8,128)(2,1)} %param.24) | copy-start | bytes 540676
  3.9 7.5 %copy-start.4 = (bf16[128,704]{0,1:T(8,128)(2,1)S(1)}, bf16[128,704]{0,1:T(8,128)(2,1)}, u32[]{:S(2)}) copy-start(bf16[128,704]{0,1:T(8,128)(2,1)} %param.35) | copy-start | bytes 540676
  8.3 3.8 %copy-start.5 = (bf16[128,704]{0,1:T(8,128)(2,1)S(1)}, bf16[128,704]{0,1:T(8,128)(2,1)}, u32[]{:S(2)}) copy-start(bf16[128,704]{0,1:T(8,128)(2,1)} %param.36) | copy-start | bytes 540676
  10.7 21.2 %copy-start.16 = (s32[64]{0:T(128)S(1)}, s32[64]{0:T(128)}, u32[]{:S(2)}) copy-start(s32[64]{0:T(128)} %param.20) | copy-start | bytes 772
  12.1 32.0 %copy-start.13 = (f32[128]{0:T(128)S(1)}, f32[128]{0:T(128)}, u32[]{:S(2)}) copy-start(f32[128]{0:T(128)} %param.22) | copy-start | bytes 1540
  23.1 20.7 %collective-permute-start = (bf16[128,5248]{0,1:T(8,128)(2,1)}, bf16[128,5248]{0,1:T(8,128)(2,1)S(1)}, u32[]{:S(2)}, u32[]{:S(2)}) collective-permute-start(bf16[128,5248]{0,1:T(8,128)(2,1)} %constant_dynamic-update-slice_fusion), channel_id=1, source_target_pairs={{0,16},{16,0},{1,17},{17,1},{2,18},{18,2},{3,19},{19,3},{4,20},{20... | collective-permute-start | bytes 4030472 | tf_op jit(solution)/shard_map/ppermute | solution.py:114
  33.0 10.6 %all-to-all-start = ((bf16[32,2,256]{2,1,0:T(2,128)(2,1)}), bf16[32,2,256]{2,1,0:T(2,128)(2,1)S(1)}, u32[]{:S(2)}, u32[]{:S(2)}) async-start(bf16[32,2,256]{2,1,0:T(2,128)(2,1)} %reshape.509), calls=%async_computation | async-start | bytes 65536 | tf_op jit(solution)/shard_map/all_to_all | solution.py:18
  44.8 48.2 %copy-start.1 = (bf16[704,128]{1,0:T(8,128)(2,1)S(1)}, bf16[704,128]{1,0:T(8,128)(2,1)}, u32[]{:S(2)}) copy-start(bf16[704,128]{1,0:T(8,128)(2,1)} %param.25) | copy-start | bytes 540676
  45.5 25.7 %all-to-all-start.1 = ((bf16[16,4,1536]{2,1,0:T(4,128)(2,1)}), bf16[16,4,1536]{2,1,0:T(4,128)(2,1)S(1)}, u32[]{:S(2)}, u32[]{:S(2)}) async-start(bf16[16,4,1536]{2,1,0:T(4,128)(2,1)} %reshape.484), calls=%async_computation.1 | async-start | bytes 393216 | tf_op jit(solution)/shard_map/all_to_all | solution.py:18
  72.3 20.7 %all-to-all-start.2 = ((bf16[16,4,704]{2,1,0:T(4,128)(2,1)}), bf16[16,4,704]{2,1,0:T(4,128)(2,1)S(1)}, u32[]{:S(2)}, u32[]{:S(2)}) async-start(bf16[16,4,704]{2,1,0:T(4,128)(2,1)} %broadcast_in_dim.164), calls=%async_computation.2 | async-start | bytes 196608 | tf_op jit(solution)/shard_map/all_to_all | solution.py:18
  93.4 19.4 %copy-start.14 = (f32[128]{0:T(128)S(1)}, f32[128]{0:T(128)}, u32[]{:S(2)}) copy-start(f32[128]{0:T(128)} %param.26) | copy-start | bytes 1540
  93.5 20.5 %copy-start.8 = (bf16[128,128]{1,0:T(8,128)(2,1)S(1)}, bf16[128,128]{1,0:T(8,128)(2,1)}, u32[]{:S(2)}) copy-start(bf16[128,128]{1,0:T(8,128)(2,1)} %param.27) | copy-start | bytes 98308
  93.5 20.5 %copy-start.9 = (bf16[128,128]{1,0:T(8,128)(2,1)S(1)}, bf16[128,128]{1,0:T(8,128)(2,1)}, u32[]{:S(2)}) copy-start(bf16[128,128]{1,0:T(8,128)(2,1)} %param.28) | copy-start | bytes 98308
  93.5 20.5 %copy-start.10 = (bf16[128,128]{1,0:T(8,128)(2,1)S(1)}, bf16[128,128]{1,0:T(8,128)(2,1)}, u32[]{:S(2)}) copy-start(bf16[128,128]{1,0:T(8,128)(2,1)} %param.29) | copy-start | bytes 98308
  93.5 20.5 %copy-start.11 = (bf16[128,128]{1,0:T(8,128)(2,1)S(1)}, bf16[128,128]{1,0:T(8,128)(2,1)}, u32[]{:S(2)}) copy-start(bf16[128,128]{1,0:T(8,128)(2,1)} %param.30) | copy-start | bytes 98308
  94.4 12.6 %all-to-all-start.3 = ((bf16[16,64,256]{2,1,0:T(8,128)(2,1)}), bf16[16,64,256]{2,1,0:T(8,128)(2,1)S(1)}, u32[]{:S(2)}, u32[]{:S(2)}) async-start(bf16[16,64,256]{2,1,0:T(8,128)(2,1)} %broadcast_in_dim.165), calls=%async_computation.3 | async-start | bytes 1048576 | tf_op jit(solution)/shard_map/all_to_all | solution.py:18
  98.1 21.9 %copy-start.15 = (f32[128]{0:T(128)S(1)}, f32[128]{0:T(128)}, u32[]{:S(2)}) copy-start(f32[128]{0:T(128)} %param.31) | copy-start | bytes 1540
  107.1 25.4 %copy-start.6 = (f32[2,1,128,128]{3,2,1,0:T(8,128)S(1)}, f32[2,1,128,128]{3,2,1,0:T(8,128)}, u32[]{:S(2)}) copy-start(f32[2,1,128,128]{3,2,1,0:T(8,128)} %param.21) | copy-start | bytes 393220
  107.1 6.6 %collective-permute-start.1 = (bf16[64,256]{1,0:T(8,128)(2,1)S(1)}, bf16[64,256]{1,0:T(8,128)(2,1)S(1)}, u32[]{:S(2)}, u32[]{:S(2)}) collective-permute-start(bf16[64,256]{1,0:T(8,128)(2,1)S(1)} %pad_maximum_fusion.3), channel_id=1, source_target_pairs={{0,16},{16,0},{1,17},{17,1},{2,18},{18,2},{3,19},{19,3},{4,20},{20... | collective-permute-start | bytes 98312 | tf_op jit(solution)/shard_map/ppermute | solution.py:180
  112.9 21.0 %copy-start.17 = (f32[128]{0:T(128)S(1)}, f32[128]{0:T(128)}, u32[]{:S(2)}) copy-start(f32[128]{0:T(128)} %param.32) | copy-start | bytes 1540
  114.0 42.4 %copy-start.7 = (bf16[128,128]{1,0:T(8,128)(2,1)S(1)}, bf16[128,128]{1,0:T(8,128)(2,1)}, u32[]{:S(2)}) copy-start(bf16[128,128]{1,0:T(8,128)(2,1)} %param.33) | copy-start | bytes 98308
  115.3 16.7 %all-to-all-start.4 = ((bf16[16,8,640]{2,1,0:T(8,128)(2,1)}), bf16[16,8,640]{2,1,0:T(8,128)(2,1)S(1)}, u32[]{:S(2)}, u32[]{:S(2)}) async-start(bf16[16,8,640]{2,1,0:T(8,128)(2,1)} %pad_maximum_fusion), calls=%async_computation.4 | async-start | bytes 327680 | tf_op jit(solution)/shard_map/all_to_all | solution.py:18
  132.3 28.9 %copy-start.12 = (f32[128]{0:T(128)S(1)}, f32[128]{0:T(128)}, u32[]{:S(2)}) copy-start(f32[128]{0:T(128)} %param.34) | copy-start | bytes 1540
  134.6 21.7 %all-to-all-start.5 = ((bf16[32,8,128]{2,1,0:T(8,128)(2,1)}), bf16[32,8,128]{2,1,0:T(8,128)(2,1)S(1)}, u32[]{:S(2)}, u32[]{:S(2)}) async-start(bf16[32,8,128]{2,1,0:T(8,128)(2,1)} %broadcast_in_dim.173), calls=%async_computation.5 | async-start | bytes 131072 | tf_op jit(solution)/shard_map/all_to_all | solution.py:18
  157.6 13.7 %all-to-all-start.6 = ((bf16[16,64,256]{2,1,0:T(8,128)(2,1)}), bf16[16,64,256]{2,1,0:T(8,128)(2,1)S(1)}, u32[]{:S(2)}, u32[]{:S(2)}) async-start(bf16[16,64,256]{2,1,0:T(8,128)(2,1)} %broadcast_in_dim.174), calls=%async_computation.6 | async-start | bytes 1048576 | tf_op jit(solution)/shard_map/all_to_all | solution.py:18
  171.7 36.9 %copy-start.2 = (bf16[704,128]{1,0:T(8,128)(2,1)S(1)}, bf16[704,128]{1,0:T(8,128)(2,1)}, u32[]{:S(2)}) copy-start(bf16[704,128]{1,0:T(8,128)(2,1)} %param.37) | copy-start | bytes 540676
  188.8 19.8 %all-to-all-start.8 = ((bf16[16,4,704]{2,1,0:T(4,128)(2,1)}), bf16[16,4,704]{2,1,0:T(4,128)(2,1)S(1)}, u32[]{:S(2)}, u32[]{:S(2)}) async-start(bf16[16,4,704]{2,1,0:T(4,128)(2,1)} %broadcast_in_dim.177), calls=%async_computation.8 | async-start | bytes 196608 | tf_op jit(solution)/shard_map/all_to_all | solution.py:18

commit v2 on v1

v2 whole, which is shorter than its diff:
```python
import jax
import jax.numpy as jnp
from jax import lax
from jax.experimental import pallas as pl
from jax.experimental.pallas import tpu as pltpu
from jax.sharding import Mesh
from jax.sharding import PartitionSpec as P

D = 4096
DK = 128
W = 4
EPSILON = 1e-06
LANES = 128
GAIN_ROWS = 16

f32 = jnp.float32
bf16 = jnp.bfloat16
barrier = lax.optimization_barrier


def matmul(a, b):
    return jnp.dot(a, b, preferred_element_type=f32)


def matmul_t(a, b):
    return lax.dot_general(a, b, (((1,), (1,)), ((), ())), preferred_element_type=f32)


def pack_kernel(*refs):
    weights, gains, out, sems = refs[:-5], refs[-5:-2], refs[-2], refs[-1]
    copies = []
    at = 0
    for i, ref in enumerate(weights):
        count = ref.shape[0]
        copies.append(pltpu.make_async_copy(ref, out.at[pl.ds(at, count)], sems.at[i]))
        copies[-1].start()
        at += count
    pieces = []
    for ref in gains:
        value = ref[...]
        high = value.astype(bf16).astype(f32)
        rest = value - high
        mid = rest.astype(bf16).astype(f32)
        pieces += [high, mid, rest - mid]
    pieces.append(jnp.zeros((GAIN_ROWS - len(pieces), LANES), f32))
    out[at:, :] = jnp.concatenate(pieces, axis=0).astype(bf16)
    for copy in copies:
        copy.wait()


def packed_weights(weights, gains):
    rows = sum(w.shape[0] for w in weights) + GAIN_ROWS
    return pl.pallas_call(
        pack_kernel,
        in_specs=[pl.BlockSpec(memory_space=pl.ANY)] * len(weights)
        + [pl.BlockSpec(memory_space=pltpu.VMEM)] * len(gains),
        out_specs=pl.BlockSpec(memory_space=pltpu.VMEM),
        out_shape=jax.ShapeDtypeStruct((rows, weights[0].shape[1]), bf16),
        scratch_shapes=[pltpu.SemaphoreType.DMA((len(weights),))],
    )(*weights, *[gain[None, :] for gain in gains])


def squares_of(rows, width):
    wide = rows.astype(f32)
    total = jnp.sum(wide * wide, axis=1, keepdims=True)
    high = lax.reduce_precision(total, 8, 7)
    lanes = lax.broadcasted_iota(jnp.int32, (1, width), 1)
    return jnp.where(lanes == 0, high, jnp.where(lanes == 1, total - high, 0.0))


def slot_targets(lengths, slot_count):
    seq_count = lengths.shape[0]
    seqs = jnp.arange(seq_count, dtype=jnp.int32)
    slots = jnp.arange(slot_count, dtype=jnp.int32)
    seq_of = slots // W
    within = slots % W
    before = jnp.sum(jnp.where(seqs[None, :] < seq_of[:, None], lengths[None, :], 0), axis=1)
    own = jnp.sum(jnp.where(seqs[None, :] == seq_of[:, None], lengths[None, :], 0), axis=1)
    return jnp.where(within < own, before + within, -1)


def products(rows, gain, exact, own, other, product):
    cols = rows.shape[1] // 2
    wide = rows.astype(f32) * gain
    parts = [wide.astype(bf16)]
    if exact:
        parts.append((wide - lax.reduce_precision(wide, 8, 7)).astype(bf16))
    return [
        sum(product(p[:, :cols], a) + product(p[:, cols:], b) for p in parts)
        for a, b in zip(own, other, strict=True)
    ]


def local(
    tokens,
    lengths,
    states,
    gain_pre,
    pre_gate,
    pre_up,
    pre_down,
    gain_mix,
    query_weight,
    forget_weight,
    input_weight,
    outgate_weight,
    forget_floor,
    head_gain,
    mix_weight,
    gain_post,
    post_gate,
    post_up,
    post_down,
):
    core = lax.axis_index("c")
    z_count = lax.axis_size("z")
    tp_count = lax.axis_size("tp")
    slot_count = tokens.shape[0]
    packed = slot_count // 2
    half = packed // 2
    per_z = half // z_count
    own_cols = gain_pre.shape[0]
    hidden = pre_gate.shape[1]
    wide = -(-hidden // LANES) * LANES
    head_cols = query_weight.shape[1]
    seq_local, heads_local = states.shape[:2]
    swap = [(0, 1), (1, 0)]

    side = {}

    def exchanged(value, axis):
        value, tied = barrier((value, dict(side)))
        value = lax.all_to_all(value, axis, split_axis=0, concat_axis=0, tiled=True)
        value, tied = barrier((value, tied))
        side.update(tied)
        return value

    def sent_to_all(value, axis):
        return exchanged(jnp.broadcast_to(value, (lax.axis_size(axis), *value.shape)), axis)

    ff_names = ("pre_gate", "pre_up", "post_gate", "post_up")
    head_names = ("query", "forget", "input", "outgate")
    names = (*ff_names, *head_names, "mix", "pre_down", "post_down")
    mine = (pre_gate.T, pre_up.T, post_gate.T, post_up.T)
    mine += (query_weight, forget_weight, input_weight, outgate_weight)
    mine += (mix_weight, pre_down, post_down)
    gains = (gain_pre, gain_mix, gain_post)
    bundle = lax.ppermute(packed_weights(mine, gains), "c", swap)

    targets = slot_targets(lengths, slot_count)
    rows = jnp.arange(packed, dtype=jnp.int32)
    table = (rows[:, None] == targets[None, :]).astype(bf16)
    row_ids = jnp.where(core == 0, rows, (rows + half) % packed)
    by_owner = targets.reshape(z_count, 2, seq_local * W)
    own_targets = jnp.where(core == 0, by_owner[:, 0], by_owner[:, 1]).reshape(packed)
    first_seq = (lax.axis_index("z") * 2 + core) * seq_local
    local_lengths = lax.dynamic_slice_in_dim(lengths, first_seq, seq_local)
    live = jnp.arange(W, dtype=jnp.int32)[None, :] < local_lengths[:, None]
    side["table"] = table
    side["my_table"] = jnp.where(core == 0, table[:half], table[half:])
    side["spread"] = (own_targets[:, None] == row_ids[None, :]).astype(bf16)
    side["live"] = live[:, :, None, None].astype(f32)
    side["floors"] = forget_floor.reshape(heads_local, DK)
    side["rises"] = 1.0 - side["floors"]

    entry = lax.dot_general(
        tokens, table, (((0,), (1,)), ((), ())), preferred_element_type=f32
    ).astype(bf16)
    pieces = jnp.stack([entry[:, :half], entry[:, half:]])
    pieces = jnp.broadcast_to(pieces[:, None], (2, tp_count, *pieces.shape[1:]))
    gathered = exchanged(pieces.reshape(2 * tp_count, *pieces.shape[2:]), ("c", "tp"))
    gathered = gathered.reshape(2, own_cols, half)
    gathered = jnp.where(core == 0, gathered, gathered[::-1])
    side["resid"] = gathered.reshape(2 * own_cols, half).T

    at = 0
    for name, weight in zip(names, mine, strict=True):
        side[name] = (weight, bundle[at : at + weight.shape[0]])
        at += weight.shape[0]
    parts = bundle[at : at + 3 * len(gains)].astype(f32)
    for i, gain in enumerate(gains):
        other = jnp.sum(parts[3 * i : 3 * i + 3], axis=0)
        side[f"gain{i}"] = jnp.concatenate([gain, other])[None, :]

    def ff_hidden(gain, names, exact):
        resid = side["resid"]
        own, other = zip(*[side[name] for name in names], strict=True)
        gate, up = products(resid, side[gain], exact, own, other, matmul_t)
        blank = jnp.zeros((half, wide - hidden), f32)
        sent = jnp.concatenate([gate, squares_of(resid, wide - hidden), up, blank], axis=1)
        sent = sent.astype(bf16).reshape(z_count, per_z, 2 * wide)
        owned = jnp.sum(exchanged(sent, "z").astype(f32), axis=0)
        total = owned[:, hidden : hidden + 1] + owned[:, hidden + 1 : hidden + 2]
        scale = lax.rsqrt(total / D + EPSILON)
        gate = owned[:, :hidden] * scale
        up = owned[:, wide : wide + hidden] * scale
        act = (jax.nn.silu(gate) * up).astype(bf16)
        return sent_to_all(act, "z").reshape(half, hidden)

    def tp_summed(value, name):
        own, other = side[name]
        partial = jnp.concatenate([matmul(value, own), matmul(value, other)], axis=1)
        return jnp.sum(sent_to_all(partial.astype(bf16), "tp").astype(f32), axis=0)

    act = ff_hidden("gain0", ff_names[:2], True)
    summed = tp_summed(act, "pre_down")
    resid = (side["resid"].astype(f32) + 0.5 * summed).astype(bf16)
    side["resid"] = resid

    turned = jnp.concatenate([resid[:, own_cols:], resid[:, :own_cols]], axis=1)
    all_rows = jnp.concatenate([resid, lax.ppermute(turned, "c", swap)], axis=0)
    slot_rows = matmul(side["spread"], all_rows).astype(bf16)
    own, other = zip(*[side[name] for name in head_names], strict=True)
    product = products(slot_rows, side["gain1"], True, own, other, matmul)
    sent = jnp.concatenate([*product, squares_of(slot_rows, LANES)], axis=1).astype(bf16)
    sent = sent.reshape(z_count, seq_local * W, 4 * head_cols + LANES)
    side["states"] = states
    owned = jnp.sum(exchanged(sent, "z").astype(f32), axis=0)
    at = 4 * head_cols
    total = owned[:, at : at + 1] + owned[:, at + 1 : at + 2]
    owned = owned[:, :at] * lax.rsqrt(total / D + EPSILON)

    shape_four = (seq_local, W, heads_local, DK)
    queries = jax.nn.silu(owned[:, :head_cols]).reshape(shape_four)
    forget_raw = owned[:, head_cols : 2 * head_cols].reshape(shape_four)
    fresh_values = owned[:, 2 * head_cols : 3 * head_cols].reshape(shape_four)
    gating = owned[:, 3 * head_cols :].reshape(shape_four)
    live = side["live"]
    forgets = jnp.where(
        live > 0, side["floors"] + side["rises"] * jax.nn.sigmoid(forget_raw), jnp.float32(1.0)
    )
    write_rate = 1.0 - forgets
    carried = side["states"]
    readings = []
    for offset in range(W):
        carried = (
            forgets[:, offset, :, :, None] * carried
            + write_rate[:, offset, :, :, None] * fresh_values[:, offset, :, None, :]
        )
        readings.append(jnp.sum(queries[:, offset, :, :, None] * carried, axis=2))
    side["states"] = carried
    read_out = jnp.stack(readings, axis=1)
    meansq = jnp.mean(read_out * read_out, axis=3, keepdims=True)
    head_out = (
        read_out * lax.rsqrt(meansq + EPSILON) * head_gain * jax.nn.silu(gating) * live
    ).astype(bf16)
    head_out = head_out.reshape(seq_local * W, heads_local * DK)
    all_heads = sent_to_all(head_out, ("z", "c")).reshape(slot_count, heads_local * DK)
    head_rows = matmul(side["my_table"], all_heads).astype(bf16)
    summed = tp_summed(head_rows, "mix")
    side["resid"] = (side["resid"].astype(f32) + summed).astype(bf16)

    act = ff_hidden("gain2", ff_names[2:], False)
    contract = (((0,), (1,)), ((), ()))
    finish = jnp.stack(
        [
            lax.dot_general(down, act, contract, preferred_element_type=f32)
            for down in side["post_down"]
        ]
    )
    first = (lax.axis_index("tp") == 0).astype(f32)
    residual = side["resid"].astype(f32).T.reshape(2, own_cols, half)
    finish = 0.5 * finish + first * residual
    finish = jnp.where(core == 0, finish, finish[::-1])
    finish = finish.reshape(2 * tp_count, own_cols // tp_count, half)
    finished = jnp.sum(exchanged(finish, ("c", "tp")).reshape(2, tp_count, -1, half), axis=1)
    finished = jnp.concatenate([finished[0], finished[1]], axis=1).astype(bf16)
    outcome = lax.dot_general(
        side["table"], finished, (((0,), (1,)), ((), ())), preferred_element_type=f32
    ).astype(bf16)
    return (outcome, side["states"])


def solution(mesh):
    kv = mesh.shape["kv"]
    tp = mesh.shape["tp"]
    cut = Mesh(mesh.devices.reshape(kv // 2, 2, tp), ("z", "c", "tp"))
    kv_axes = ("z", "c")
    placed = (
        P(None, ("z", "c", "tp")),
        P(),
        P(kv_axes, "tp", None, None),
        P(kv_axes),
        P(kv_axes, "tp"),
        P(kv_axes, "tp"),
        P("tp", kv_axes),
        P(kv_axes),
        P(kv_axes, "tp"),
        P(kv_axes, "tp"),
        P(kv_axes, "tp"),
        P(kv_axes, "tp"),
        P("tp"),
        P(),
        P("tp", kv_axes),
        P(kv_axes),
        P(kv_axes, "tp"),
        P(kv_axes, "tp"),
        P("tp", kv_axes),
    )
    return jax.shard_map(
        local,
        mesh=cut,
        in_specs=placed,
        out_specs=(P(None, ("z", "c", "tp")), P(kv_axes, "tp", None, None)),
        check_vma=False,
    )
```

time: 227 us -> 206 us (0.907)
  blocking collectives: 30.1 us -> 139 us
  waiting for transfers between devices: 87.4 us -> 19.6 us
  starting transfers between devices: 68.3 us -> 26.5 us
  local copies, waits for them, and re-layouts: 27.3 us -> 4.4 us
  Pallas kernels: 0 us -> 3.26 us
  matrix products: 3.78 us -> 6.84 us
  other arithmetic: 7.49 us -> 4.48 us
    all_to_all x2 -> x8, blocking collectives: 30.1 us -> 139 us  [exchanged(): value = lax.all_to_all(value, axis, split_axis=0, concat_axis=0, tiled=True)]
    all_to_all x8 -> x2, waiting for transfers between devices: 86.6 us -> 18.8 us  [exchanged(): value = lax.all_to_all(value, axis, split_axis=0, concat_axis=0, tiled=True)]
    all_to_all x8 -> x2, starting transfers between devices: 53.9 us -> 11.5 us  [exchanged(): value = lax.all_to_all(value, axis, split_axis=0, concat_axis=0, tiled=True)]
    unnamed x74 -> x40, local copies, waits for them, and re-layouts: 18.5 us -> 0.95 us
    pallas_call x0 -> x1, Pallas kernels: none -> 3.26 us  [packed_weights(): pl.pallas_call(pack_kernel, in_specs=[pl.BlockSpec(memory_space=pl.ANY)]...]
    broadcast_in_dim x5, local copies, waits for them, and re-layouts: 3.66 us -> 0.8 us  [sent_to_all(): jnp.broadcast_to(value, (lax.axis_size(axis), *value.shape))]
    dot_general x2 -> x14, matrix products: 0.92 us -> 3.27 us  [the longest x12 2.34 us: matmul_t(): lax.dot_general(a, b, (((1,), (1,)), ((), ())), preferred_element_type=f32)]
  transfers between devices with their start and end apart: 10 -> 4, of which waited for: 9 -> 3; matrix products, arithmetic and copies ran while one was open for 1% -> 1% of each run, Pallas kernels for 0% -> 0%
where the time goes in v2:
time: 206 us; the launch traced here: 205 us
  blocking collectives  139 us (67%)
  starting transfers between devices  26.5 us (13%)
  waiting for transfers between devices  19.6 us (10%)
  matrix products  6.84 us (3%)
  other arithmetic  4.48 us (2%)
  local copies, waits for them, and re-layouts  4.4 us (2%)
  Pallas kernels  3.26 us (2%)
    all_to_all x8, blocking collectives, exchanged(): value = lax.all_to_all(value, axis, split_axis=0, concat_axis=0, tiled=True)  139 us
    all_to_all x2, waiting for transfers between devices, exchanged(): value = lax.all_to_all(value, axis, split_axis=0, concat_axis=0, tiled=True)  18.8 us
    all_to_all x2, starting transfers between devices, exchanged(): value = lax.all_to_all(value, axis, split_axis=0, concat_axis=0, tiled=True)  11.5 us
    ppermute x1, starting transfers between devices, local(): bundle = lax.ppermute(packed_weights(mine, gains), 'c', swap)  8.88 us
    ppermute x1, starting transfers between devices, local(): all_rows = jnp.concatenate([resid, lax.ppermute(turned, 'c', swap)], axis=0)  6.09 us
  transfers between devices with their start and end apart: 4, of which 3 were waited for; matrix products, arithmetic and copies ran while one was open for 1% of the time, Pallas kernels for 0%

profile of v2, /device:TPU:1, one launch (start us, length us, event | category | flops | bytes accessed | tf_op | source)
XLA Modules:
  0.0 205.2 jit_solution(9591487660711950049)
XLA Ops:
  0.7 3.3 %shard_map.194 = bf16[4880,128]{1,0:T(8,128)(2,1)} custom-call(bf16[704,128]{1,0:T(8,128)(2,1)} %bitcast.148, bf16[704,128]{1,0:T(8,128)(2,1)} %bitcast.149, bf16[704,128]{1,0:T(8,128)(2,1)} %bitcast.150, bf16[704,128]{1,0:T(8,128)(2,1)} %bitcast.152, bf16[128,128]{1,0:T(8,128)(2,1)} %refs_4_.1, bf16[128,128]{1,0:T(8,128)(2,1)} %refs_5_.1, ...), custom_call_target="tpu_custom_call" | custom-call | tf_op jit(solution)/shard_map/pallas_call | solution.py:53
  4.0 8.9 %collective-permute-start = (bf16[4880,128]{1,0:T(8,128)(2,1)}, bf16[4880,128]{1,0:T(8,128)(2,1)S(1)}, u32[]{:S(2)}, u32[]{:S(2)}) collective-permute-start(bf16[4880,128]{1,0:T(8,128)(2,1)} %shard_map.194), channel_id=1, source_target_pairs={{0,16},{16,0},{1,17},{17,1},{2,18},{18,2},{3,19},{19,3},{4,20},{20... | collective-permute-start | bytes 3747848 | tf_op jit(solution)/shard_map/ppermute | solution.py:148
  13.2 0.1 fusion.23
  14.0 0.7 reshape.539
  14.7 3.6 %all-to-all-start = ((bf16[32,2,256]{2,1,0:T(2,128)(2,1)}), bf16[32,2,256]{2,1,0:T(2,128)(2,1)S(1)}, u32[]{:S(2)}, u32[]{:S(2)}) async-start(bf16[32,2,256]{2,1,0:T(2,128)(2,1)} %reshape.539), calls=%async_computation | async-start | bytes 65536 | tf_op jit(solution)/shard_map/all_to_all | solution.py:133
  18.3 6.9 %all-to-all-done = bf16[32,2,256]{2,1,0:T(2,128)(2,1)S(1)} async-done(((bf16[32,2,256]{2,1,0:T(2,128)(2,1)}), bf16[32,2,256]{2,1,0:T(2,128)(2,1)S(1)}, u32[]{:S(2)}, u32[]{:S(2)}) %all-to-all-start) | async-done | bytes 32800 | tf_op jit(solution)/shard_map/all_to_all | solution.py:133
  25.7 0.2 fusion.79
  25.9 0.2 fusion.77
  26.1 0.2 fusion.73
  26.3 0.2 fusion.71
  26.5 0.2 convolution_add_fusion.5
  26.7 0.2 fusion.2
  27.1 0.2 convolution_add_fusion.3
  27.3 0.2 fusion.3
  27.7 0.2 concatenate.71
  28.0 25.6 %all_to_all.50 = bf16[16,4,1536]{2,1,0:T(4,128)(2,1)S(1)} all-to-all(bf16[16,4,1536]{2,1,0:T(4,128)(2,1)S(1)} %concatenate.71), channel_id=1, replica_groups=mesh['z'=16,'c'=2,'tp'=16] {'z'}, dimensions={0} | all-to-all | bytes 393216 | tf_op jit(solution)/shard_map/all_to_all | solution.py:133
  53.7 0.2 fusion.100
  54.0 20.5 %all_to_all.51 = bf16[16,4,704]{2,1,0:T(4,128)(2,1)S(1)} all-to-all(bf16[16,4,704]{2,1,0:T(4,128)(2,1)S(1)} %broadcast_in_dim.201), channel_id=1, replica_groups=mesh['z'=16,'c'=2,'tp'=16] {'z'}, dimensions={0} | all-to-all | bytes 180224 | tf_op jit(solution)/shard_map/all_to_all | solution.py:133
  74.6 0.2 convolution_convert_fusion.4
  74.8 0.2 convolution_convert_fusion.5
  75.1 12.1 %all_to_all.52 = bf16[16,64,256]{2,1,0:T(8,128)(2,1)S(1)} all-to-all(bf16[16,64,256]{2,1,0:T(8,128)(2,1)S(1)} %broadcast_in_dim.202), channel_id=1, replica_groups=mesh['z'=16,'c'=2,'tp'=16] {'tp'}, dimensions={0} | all-to-all | bytes 1048576 | tf_op jit(solution)/shard_map/all_to_all | solution.py:133
  87.3 6.1 %collective-permute-start.1 = (bf16[64,256]{1,0:T(8,128)(2,1)S(1)}, bf16[64,256]{1,0:T(8,128)(2,1)S(1)}, u32[]{:S(2)}, u32[]{:S(2)}) collective-permute-start(bf16[64,256]{1,0:T(8,128)(2,1)S(1)} %pad_maximum_fusion.1), channel_id=1, source_target_pairs={{0,16},{16,0},{1,17},{17,1},{2,18},{18,2},{3,19},{19,3},{4,20},{20... | collective-permute-start | bytes 98312 | tf_op jit(solution)/shard_map/ppermute | solution.py:211
  93.4 0.8 collective-permute-done.1
  94.3 0.2 fusion.24
  94.5 0.1 fusion.60
  94.6 0.1 fusion.48
  94.8 0.1 fusion.58
  94.9 0.1 fusion.46
  95.1 0.1 fusion.56
  95.2 0.1 fusion.44
  95.3 0.1 fusion.54
  95.5 0.1 fusion.42
  95.7 0.1 convolution_add_fusion.13
  95.9 0.1 fusion.22
  96.0 0.1 convolution_add_fusion.11
  96.2 0.1 convolution_add_fusion.9
  96.3 0.1 convolution_add_fusion.7
  96.4 0.2 fusion.20
  96.6 0.2 fusion.18
  96.8 0.2 fusion.16
  97.0 16.2 %all_to_all.53 = bf16[16,8,640]{2,1,0:T(8,128)(2,1)S(1)} all-to-all(bf16[16,8,640]{2,1,0:T(8,128)(2,1)S(1)} %fusion.37), channel_id=1, replica_groups=mesh['z'=16,'c'=2,'tp'=16] {'z'}, dimensions={0} | all-to-all | bytes 327680 | tf_op jit(solution)/shard_map/all_to_all | solution.py:133
  113.4 0.2 fusion.92
  113.8 1.1 multiply_reduce_fusion.2
  115.3 21.5 %all_to_all.54 = bf16[32,8,128]{2,1,0:T(8,128)(2,1)S(1)} all-to-all(bf16[32,8,128]{2,1,0:T(8,128)(2,1)S(1)} %broadcast_in_dim.210), channel_id=1, replica_groups=mesh['z'=16,'c'=2,'tp'=16] {'z','c'}, dimensions={0} | all-to-all | bytes 131072 | tf_op jit(solution)/shard_map/all_to_all | solution.py:133
  136.8 0.1 convolution_convert_fusion.3
  136.9 0.1 convolution_convert_fusion.1
  137.1 0.1 convolution_convert_fusion.2
  137.3 12.7 %all_to_all.55 = bf16[16,64,256]{2,1,0:T(8,128)(2,1)S(1)} all-to-all(bf16[16,64,256]{2,1,0:T(8,128)(2,1)S(1)} %broadcast_in_dim.211), channel_id=1, replica_groups=mesh['z'=16,'c'=2,'tp'=16] {'tp'}, dimensions={0} | all-to-all | bytes 1048576 | tf_op jit(solution)/shard_map/all_to_all | solution.py:133
  150.3 0.2 fusion.67
  150.4 0.2 fusion.4
  150.8 0.2 fusion.65
  151.0 0.2 fusion.5
  151.3 0.2 concatenate.85
  151.6 15.6 %all_to_all.56 = bf16[16,4,1536]{2,1,0:T(4,128)(2,1)S(1)} all-to-all(bf16[16,4,1536]{2,1,0:T(4,128)(2,1)S(1)} %concatenate.85), channel_id=1, replica_groups=mesh['z'=16,'c'=2,'tp'=16] {'z'}, dimensions={0} | all-to-all | bytes 393216 | tf_op jit(solution)/shard_map/all_to_all | solution.py:133
  167.3 0.2 fusion.96
  167.6 0.7 broadcast_in_dim.214
  168.3 7.9 %all-to-all-start.8 = ((bf16[16,4,704]{2,1,0:T(4,128)(2,1)}), bf16[16,4,704]{2,1,0:T(4,128)(2,1)S(1)}, u32[]{:S(2)}, u32[]{:S(2)}) async-start(bf16[16,4,704]{2,1,0:T(4,128)(2,1)} %broadcast_in_dim.214), calls=%async_computation.8 | async-start | bytes 196608 | tf_op jit(solution)/shard_map/all_to_all | solution.py:133
  176.2 11.8 %all-to-all-done.8 = bf16[16,4,704]{2,1,0:T(4,128)(2,1)S(1)} async-done(((bf16[16,4,704]{2,1,0:T(4,128)(2,1)}), bf16[16,4,704]{2,1,0:T(4,128)(2,1)S(1)}, u32[]{:S(2)}, u32[]{:S(2)}) %all-to-all-start.8) | async-done | bytes 90144 | tf_op jit(solution)/shard_map/all_to_all | solution.py:133
  188.1 0.2 convolution_bitcast_fusion
  188.3 0.2 convolution_bitcast_fusion.1
  188.7 14.3 %all_to_all.57 = f32[32,1,512]{2,1,0:T(1,128)S(1)} all-to-all(f32[32,1,512]{2,1,0:T(1,128)S(1)} %reshape.541), channel_id=1, replica_groups=mesh['z'=16,'c'=2,'tp'=16] {'c','tp'}, dimensions={0} | all-to-all | bytes 131072 | tf_op jit(solution)/shard_map/all_to_all | solution.py:133
  203.0 0.5 broadcast.491
  203.5 0.8 reduce.15
  204.4 0.8 convolution_convert_fusion.6
  (125 shorter events, 4.0 us)
Async XLA Ops:
  0.6 12.6 %copy-start = (bf16[256,8]{0,1:T(8,128)(2,1)S(1)}, bf16[256,8]{0,1:T(8,128)(2,1)}, u32[]{:S(2)}) copy-start(bf16[256,8]{0,1:T(8,128)(2,1)} %param.19) | copy-start | bytes 12292
  0.6 12.2 %copy-start.17 = (s32[64]{0:T(128)S(1)}, s32[64]{0:T(128)}, u32[]{:S(2)}) copy-start(s32[64]{0:T(128)} %param.20) | copy-start | bytes 772
  0.7 12.8 %copy-start.16 = (f32[128]{0:T(128)S(1)}, f32[128]{0:T(128)}, u32[]{:S(2)}) copy-start(f32[128]{0:T(128)} %param.31) | copy-start | bytes 1540
  0.7 24.9 %copy-start.14 = (f32[128]{0:T(128)S(1)}, f32[128]{0:T(128)}, u32[]{:S(2)}) copy-start(f32[128]{0:T(128)} %param.22) | copy-start | bytes 1540
  0.7 24.9 %copy-start.15 = (f32[128]{0:T(128)S(1)}, f32[128]{0:T(128)}, u32[]{:S(2)}) copy-start(f32[128]{0:T(128)} %param.26) | copy-start | bytes 1540
  0.7 25.0 %copy-start.1 = (bf16[128,704]{0,1:T(8,128)(2,1)S(1)}, bf16[128,704]{0,1:T(8,128)(2,1)}, u32[]{:S(2)}) copy-start(bf16[128,704]{0,1:T(8,128)(2,1)} %param.23) | copy-start | bytes 540676
  4.0 22.0 %copy-start.2 = (bf16[128,704]{0,1:T(8,128)(2,1)S(1)}, bf16[128,704]{0,1:T(8,128)(2,1)}, u32[]{:S(2)}) copy-start(bf16[128,704]{0,1:T(8,128)(2,1)} %param.24) | copy-start | bytes 540676
  4.0 21.6 %collective-permute-start = (bf16[4880,128]{1,0:T(8,128)(2,1)}, bf16[4880,128]{1,0:T(8,128)(2,1)S(1)}, u32[]{:S(2)}, u32[]{:S(2)}) collective-permute-start(bf16[4880,128]{1,0:T(8,128)(2,1)} %shard_map.194), channel_id=1, source_target_pairs={{0,16},{16,0},{1,17},{17,1},{2,18},{18,2},{3,19},{19,3},{4,20},{20... | collective-permute-start | bytes 3747848 | tf_op jit(solution)/shard_map/ppermute | solution.py:148
  14.7 10.6 %all-to-all-start = ((bf16[32,2,256]{2,1,0:T(2,128)(2,1)}), bf16[32,2,256]{2,1,0:T(2,128)(2,1)S(1)}, u32[]{:S(2)}, u32[]{:S(2)}) async-start(bf16[32,2,256]{2,1,0:T(2,128)(2,1)} %reshape.539), calls=%async_computation | async-start | bytes 65536 | tf_op jit(solution)/shard_map/all_to_all | solution.py:133
  26.7 0.8 copy-start.13
  28.0 46.8 %copy-start.3 = (bf16[704,128]{1,0:T(8,128)(2,1)S(1)}, bf16[704,128]{1,0:T(8,128)(2,1)}, u32[]{:S(2)}) copy-start(bf16[704,128]{1,0:T(8,128)(2,1)} %refs_9_.1) | copy-start | bytes 540676
  75.0 19.5 %copy-start.7 = (bf16[128,128]{1,0:T(8,128)(2,1)S(1)}, bf16[128,128]{1,0:T(8,128)(2,1)}, u32[]{:S(2)}) copy-start(bf16[128,128]{1,0:T(8,128)(2,1)} %refs_4_.1) | copy-start | bytes 98308
  75.1 19.7 %copy-start.8 = (bf16[128,128]{1,0:T(8,128)(2,1)S(1)}, bf16[128,128]{1,0:T(8,128)(2,1)}, u32[]{:S(2)}) copy-start(bf16[128,128]{1,0:T(8,128)(2,1)} %refs_5_.1) | copy-start | bytes 98308
  75.1 20.0 %copy-start.9 = (bf16[128,128]{1,0:T(8,128)(2,1)S(1)}, bf16[128,128]{1,0:T(8,128)(2,1)}, u32[]{:S(2)}) copy-start(bf16[128,128]{1,0:T(8,128)(2,1)} %refs_6_.1) | copy-start | bytes 98308
  75.1 20.3 %copy-start.10 = (bf16[128,128]{1,0:T(8,128)(2,1)S(1)}, bf16[128,128]{1,0:T(8,128)(2,1)}, u32[]{:S(2)}) copy-start(bf16[128,128]{1,0:T(8,128)(2,1)} %refs_7_.1) | copy-start | bytes 98308
  87.3 6.9 %collective-permute-start.1 = (bf16[64,256]{1,0:T(8,128)(2,1)S(1)}, bf16[64,256]{1,0:T(8,128)(2,1)S(1)}, u32[]{:S(2)}, u32[]{:S(2)}) collective-permute-start(bf16[64,256]{1,0:T(8,128)(2,1)S(1)} %pad_maximum_fusion.1), channel_id=1, source_target_pairs={{0,16},{16,0},{1,17},{17,1},{2,18},{18,2},{3,19},{19,3},{4,20},{20... | collective-permute-start | bytes 98312 | tf_op jit(solution)/shard_map/ppermute | solution.py:211
  95.6 18.2 %copy-start.12 = (f32[2,1,128,128]{3,2,1,0:T(8,128)S(1)}, f32[2,1,128,128]{3,2,1,0:T(8,128)}, u32[]{:S(2)}) copy-start(f32[2,1,128,128]{3,2,1,0:T(8,128)} %param.21) | copy-start | bytes 393220
  95.9 19.3 %copy-start.18 = (f32[128]{0:T(128)S(1)}, f32[128]{0:T(128)}, u32[]{:S(2)}) copy-start(f32[128]{0:T(128)} %param.32) | copy-start | bytes 1540
  96.2 40.9 %copy-start.11 = (bf16[128,128]{1,0:T(8,128)(2,1)S(1)}, bf16[128,128]{1,0:T(8,128)(2,1)}, u32[]{:S(2)}) copy-start(bf16[128,128]{1,0:T(8,128)(2,1)} %refs_8_.1) | copy-start | bytes 98308
  137.1 13.2 %copy-start.4 = (bf16[128,704]{0,1:T(8,128)(2,1)S(1)}, bf16[128,704]{0,1:T(8,128)(2,1)}, u32[]{:S(2)}) copy-start(bf16[128,704]{0,1:T(8,128)(2,1)} %param.35) | copy-start | bytes 540676
  137.3 13.5 %copy-start.5 = (bf16[128,704]{0,1:T(8,128)(2,1)S(1)}, bf16[128,704]{0,1:T(8,128)(2,1)}, u32[]{:S(2)}) copy-start(bf16[128,704]{0,1:T(8,128)(2,1)} %param.36) | copy-start | bytes 540676
  151.0 37.3 %copy-start.6 = (bf16[704,128]{1,0:T(8,128)(2,1)S(1)}, bf16[704,128]{1,0:T(8,128)(2,1)}, u32[]{:S(2)}) copy-start(bf16[704,128]{1,0:T(8,128)(2,1)} %refs_10_.1) | copy-start | bytes 540676
  168.3 19.8 %all-to-all-start.8 = ((bf16[16,4,704]{2,1,0:T(4,128)(2,1)}), bf16[16,4,704]{2,1,0:T(4,128)(2,1)S(1)}, u32[]{:S(2)}, u32[]{:S(2)}) async-start(bf16[16,4,704]{2,1,0:T(4,128)(2,1)} %broadcast_in_dim.214), calls=%async_computation.8 | async-start | bytes 196608 | tf_op jit(solution)/shard_map/all_to_all | solution.py:133

commit v3 on v2

--- a/solution.py
+++ b/solution.py
@@ -55,16 +55,15 @@
         in_specs=[pl.BlockSpec(memory_space=pl.ANY)] * len(weights)
         + [pl.BlockSpec(memory_space=pltpu.VMEM)] * len(gains),
         out_specs=pl.BlockSpec(memory_space=pltpu.VMEM),
-        out_shape=jax.ShapeDtypeStruct((rows, weights[0].shape[1]), bf16),
+        out_shape=pltpu.VMEM((rows, weights[0].shape[1]), bf16),
         scratch_shapes=[pltpu.SemaphoreType.DMA((len(weights),))],
     )(*weights, *[gain[None, :] for gain in gains])
 
 
-def squares_of(rows, width):
+def squares_of(rows, lanes):
     wide = rows.astype(f32)
     total = jnp.sum(wide * wide, axis=1, keepdims=True)
     high = lax.reduce_precision(total, 8, 7)
-    lanes = lax.broadcasted_iota(jnp.int32, (1, width), 1)
     return jnp.where(lanes == 0, high, jnp.where(lanes == 1, total - high, 0.0))
 
 
@@ -79,16 +78,14 @@
     return jnp.where(within < own, before + within, -1)
 
 
-def products(rows, gain, exact, own, other, product):
-    cols = rows.shape[1] // 2
+def products(rows, gain, exact, weights, product):
+    count = rows.shape[0]
     wide = rows.astype(f32) * gain
-    parts = [wide.astype(bf16)]
-    if exact:
-        parts.append((wide - lax.reduce_precision(wide, 8, 7)).astype(bf16))
-    return [
-        sum(product(p[:, :cols], a) + product(p[:, cols:], b) for p in parts)
-        for a, b in zip(own, other, strict=True)
-    ]
+    if not exact:
+        return product(wide.astype(bf16), weights)
+    rest = wide - lax.reduce_precision(wide, 8, 7)
+    both = product(jnp.concatenate([wide, rest], axis=0).astype(bf16), weights)
+    return both[:count] + both[count:]
 
 
 def local(
@@ -121,7 +118,7 @@
     per_z = half // z_count
     own_cols = gain_pre.shape[0]
     hidden = pre_gate.shape[1]
-    wide = -(-hidden // LANES) * LANES
+    ff_cols = 2 * hidden
     head_cols = query_weight.shape[1]
     seq_local, heads_local = states.shape[:2]
     swap = [(0, 1), (1, 0)]
@@ -138,9 +135,6 @@
     def sent_to_all(value, axis):
         return exchanged(jnp.broadcast_to(value, (lax.axis_size(axis), *value.shape)), axis)
 
-    ff_names = ("pre_gate", "pre_up", "post_gate", "post_up")
-    head_names = ("query", "forget", "input", "outgate")
-    names = (*ff_names, *head_names, "mix", "pre_down", "post_down")
     mine = (pre_gate.T, pre_up.T, post_gate.T, post_up.T)
     mine += (query_weight, forget_weight, input_weight, outgate_weight)
     mine += (mix_weight, pre_down, post_down)
@@ -162,6 +156,8 @@
     side["live"] = live[:, :, None, None].astype(f32)
     side["floors"] = forget_floor.reshape(heads_local, DK)
     side["rises"] = 1.0 - side["floors"]
+    side["first"] = (lax.axis_index("tp") == 0).astype(f32)
+    side["lanes"] = lax.broadcasted_iota(jnp.int32, (1, LANES), 1)
 
     entry = lax.dot_general(
         tokens, table, (((0,), (1,)), ((), ())), preferred_element_type=f32
@@ -173,27 +169,31 @@
     gathered = jnp.where(core == 0, gathered, gathered[::-1])
     side["resid"] = gathered.reshape(2 * own_cols, half).T
 
+    theirs = []
     at = 0
-    for name, weight in zip(names, mine, strict=True):
-        side[name] = (weight, bundle[at : at + weight.shape[0]])
+    for weight in mine:
+        theirs.append(bundle[at : at + weight.shape[0]])
         at += weight.shape[0]
     parts = bundle[at : at + 3 * len(gains)].astype(f32)
     for i, gain in enumerate(gains):
         other = jnp.sum(parts[3 * i : 3 * i + 3], axis=0)
         side[f"gain{i}"] = jnp.concatenate([gain, other])[None, :]
-
-    def ff_hidden(gain, names, exact):
+    for i, name in ((0, "pre_ff"), (2, "post_ff")):
+        side[name] = [[mine[i], theirs[i]], [mine[i + 1], theirs[i + 1]]]
+    side["heads"] = [list(mine[4:8]), theirs[4:8]]
+    for i, name in ((8, "mix"), (9, "pre_down"), (10, "post_down")):
+        side[name] = (mine[i], theirs[i])
+
+    def ff_hidden(gain, name, exact):
         resid = side["resid"]
-        own, other = zip(*[side[name] for name in names], strict=True)
-        gate, up = products(resid, side[gain], exact, own, other, matmul_t)
-        blank = jnp.zeros((half, wide - hidden), f32)
-        sent = jnp.concatenate([gate, squares_of(resid, wide - hidden), up, blank], axis=1)
-        sent = sent.astype(bf16).reshape(z_count, per_z, 2 * wide)
+        product = products(resid, side[gain], exact, jnp.block(side[name]), matmul_t)
+        sent = jnp.concatenate([product, squares_of(resid, side["lanes"])], axis=1)
+        sent = sent.astype(bf16).reshape(z_count, per_z, ff_cols + LANES)
         owned = jnp.sum(exchanged(sent, "z").astype(f32), axis=0)
-        total = owned[:, hidden : hidden + 1] + owned[:, hidden + 1 : hidden + 2]
+        total = owned[:, ff_cols : ff_cols + 1] + owned[:, ff_cols + 1 : ff_cols + 2]
         scale = lax.rsqrt(total / D + EPSILON)
         gate = owned[:, :hidden] * scale
-        up = owned[:, wide : wide + hidden] * scale
+        up = owned[:, hidden:ff_cols] * scale
         act = (jax.nn.silu(gate) * up).astype(bf16)
         return sent_to_all(act, "z").reshape(half, hidden)
 
@@ -202,7 +202,7 @@
         partial = jnp.concatenate([matmul(value, own), matmul(value, other)], axis=1)
         return jnp.sum(sent_to_all(partial.astype(bf16), "tp").astype(f32), axis=0)
 
-    act = ff_hidden("gain0", ff_names[:2], True)
+    act = ff_hidden("gain0", "pre_ff", True)
     summed = tp_summed(act, "pre_down")
     resid = (side["resid"].astype(f32) + 0.5 * summed).astype(bf16)
     side["resid"] = resid
@@ -210,9 +210,8 @@
     turned = jnp.concatenate([resid[:, own_cols:], resid[:, :own_cols]], axis=1)
     all_rows = jnp.concatenate([resid, lax.ppermute(turned, "c", swap)], axis=0)
     slot_rows = matmul(side["spread"], all_rows).astype(bf16)
-    own, other = zip(*[side[name] for name in head_names], strict=True)
-    product = products(slot_rows, side["gain1"], True, own, other, matmul)
-    sent = jnp.concatenate([*product, squares_of(slot_rows, LANES)], axis=1).astype(bf16)
+    product = products(slot_rows, side["gain1"], True, jnp.block(side["heads"]), matmul)
+    sent = jnp.concatenate([product, squares_of(slot_rows, side["lanes"])], axis=1).astype(bf16)
     sent = sent.reshape(z_count, seq_local * W, 4 * head_cols + LANES)
     side["states"] = states
     owned = jnp.sum(exchanged(sent, "z").astype(f32), axis=0)
@@ -250,7 +249,7 @@
     summed = tp_summed(head_rows, "mix")
     side["resid"] = (side["resid"].astype(f32) + summed).astype(bf16)
 
-    act = ff_hidden("gain2", ff_names[2:], False)
+    act = ff_hidden("gain2", "post_ff", False)
     contract = (((0,), (1,)), ((), ()))
     finish = jnp.stack(
         [
@@ -258,16 +257,15 @@
             for down in side["post_down"]
         ]
     )
-    first = (lax.axis_index("tp") == 0).astype(f32)
     residual = side["resid"].astype(f32).T.reshape(2, own_cols, half)
-    finish = 0.5 * finish + first * residual
+    finish = 0.5 * finish + side["first"] * residual
     finish = jnp.where(core == 0, finish, finish[::-1])
-    finish = finish.reshape(2 * tp_count, own_cols // tp_count, half)
-    finished = jnp.sum(exchanged(finish, ("c", "tp")).reshape(2, tp_count, -1, half), axis=1)
+    piece = own_cols // tp_count
+    finish = finish.reshape(2 * tp_count, piece * half)
+    finished = jnp.sum(exchanged(finish, ("c", "tp")).reshape(2, tp_count, -1), axis=1)
+    finished = finished.reshape(2, piece, half)
     finished = jnp.concatenate([finished[0], finished[1]], axis=1).astype(bf16)
-    outcome = lax.dot_general(
-        side["table"], finished, (((0,), (1,)), ((), ())), preferred_element_type=f32
-    ).astype(bf16)
+    outcome = matmul(finished, side["table"]).astype(bf16).T
     return (outcome, side["states"])
 
 

time: 206 us -> 200 us (0.971)
  blocking collectives: 139 us -> 168 us
  waiting for transfers between devices: 19.6 us -> 0.82 us
  starting transfers between devices: 26.5 us -> 14.8 us
  matrix products: 6.84 us -> 3.2 us
    all_to_all x8 -> x10, blocking collectives: 139 us -> 168 us  [exchanged(): value = lax.all_to_all(value, axis, split_axis=0, concat_axis=0, tiled=True)]
    all_to_all x2 -> x0, waiting for transfers between devices: 18.8 us -> none  [exchanged(): value = lax.all_to_all(value, axis, split_axis=0, concat_axis=0, tiled=True)]
    all_to_all x2 -> x0, starting transfers between devices: 11.5 us -> none  [exchanged(): value = lax.all_to_all(value, axis, split_axis=0, concat_axis=0, tiled=True)]
  transfers between devices with their start and end apart: 4 -> 2, of which waited for: 3 -> 1; matrix products, arithmetic and copies ran while one was open for 1% -> 1% of each run, Pallas kernels for 0% -> 0%
where the time goes in v3:
time: 200 us; the launch traced here: 199 us
  blocking collectives  168 us (84%)
  starting transfers between devices  14.8 us (7%)
  other arithmetic  5.63 us (3%)
  matrix products  3.2 us (2%)
  local copies, waits for them, and re-layouts  2.8 us (1%)
  Pallas kernels  2.19 us (1%)
    all_to_all x10, blocking collectives, exchanged(): value = lax.all_to_all(value, axis, split_axis=0, concat_axis=0, tiled=True)  168 us
    ppermute x1, starting transfers between devices, local(): bundle = lax.ppermute(packed_weights(mine, gains), 'c', swap)  8.75 us
    ppermute x1, starting transfers between devices, local(): all_rows = jnp.concatenate([resid, lax.ppermute(turned, 'c', swap)], axis=0)  6.09 us
  transfers between devices with their start and end apart: 2, of which 1 were waited for; matrix products, arithmetic and copies ran while one was open for 1% of the time, Pallas kernels for 0%

profile of v3, /device:TPU:1, one launch (start us, length us, event | category | flops | bytes accessed | tf_op | source)
XLA Modules:
  0.0 199.2 jit_solution(5092514074730074882)
XLA Ops:
  0.7 2.2 %shard_map.194 = bf16[4880,128]{1,0:T(8,128)(2,1)S(1)} custom-call(bf16[704,128]{1,0:T(8,128)(2,1)} %bitcast.125, bf16[704,128]{1,0:T(8,128)(2,1)} %bitcast.127, bf16[704,128]{1,0:T(8,128)(2,1)} %bitcast.129, bf16[704,128]{1,0:T(8,128)(2,1)} %bitcast.131, bf16[128,128]{1,0:T(8,128)(2,1)} %refs_4_.1, bf16[128,128]{1,0:T(8,128)(2,1)} %refs_5_.1, ...), custom_call_target="tpu_custom_call" | custom-call | tf_op jit(solution)/shard_map/pallas_call | solution.py:53
  2.9 8.7 %collective-permute-start = (bf16[4880,128]{1,0:T(8,128)(2,1)S(1)}, bf16[4880,128]{1,0:T(8,128)(2,1)S(1)}, u32[]{:S(2)}, u32[]{:S(2)}) collective-permute-start(bf16[4880,128]{1,0:T(8,128)(2,1)S(1)} %shard_map.194), channel_id=1, source_target_pairs={{0,16},{16,0},{1,17},{17,1},{2,18},{18,2},{3,19},{19,3},{4,20},{20... | collective-permute-start | bytes 3747848 | tf_op jit(solution)/shard_map/ppermute | solution.py:142
  11.7 0.1 select_reduce_fusion
  11.8 0.1 reduce_sum.184
  11.9 0.1 reduce_sum.183
  12.1 0.6 compare_convert_fusion.1
  12.7 0.1 fusion.1
  13.0 0.1 select_n.166
  13.1 0.7 compare_convert_fusion
  13.9 0.1 reshape.522
  14.0 9.7 %all_to_all.57 = bf16[32,2,256]{2,1,0:T(2,128)(2,1)S(1)} all-to-all(bf16[32,2,256]{2,1,0:T(2,128)(2,1)S(1)} %reshape.522), channel_id=1, replica_groups=mesh['z'=16,'c'=2,'tp'=16] {'c','tp'}, dimensions={0} | all-to-all | bytes 65536 | tf_op jit(solution)/shard_map/all_to_all | solution.py:130
  23.7 0.1 reshape.523
  23.9 0.1 copy.67
  24.0 0.5 compare_bitcast_fusion.6
  24.6 0.1 fusion.41
  24.7 0.1 reduce_sum.187
  24.9 0.4 fusion.2
  25.4 0.5 copy-done.20
  25.9 0.1 select_convert_fusion.2
  26.0 0.1 pad_maximum_fusion
  26.1 26.2 %all_to_all.58 = bf16[16,4,1536]{2,1,0:T(4,128)(2,1)S(1)} all-to-all(bf16[16,4,1536]{2,1,0:T(4,128)(2,1)S(1)} %pad_maximum_fusion), channel_id=1, replica_groups=mesh['z'=16,'c'=2,'tp'=16] {'z'}, dimensions={0} | all-to-all | bytes 393216 | tf_op jit(solution)/shard_map/all_to_all | solution.py:130
  52.3 0.1 convert_reduce_fusion.3
  52.4 0.2 fusion.77
  52.6 0.1 fusion.61
  52.7 20.5 %all_to_all.59 = bf16[16,4,704]{2,1,0:T(4,128)(2,1)S(1)} all-to-all(bf16[16,4,704]{2,1,0:T(4,128)(2,1)S(1)} %broadcast_in_dim.212), channel_id=1, replica_groups=mesh['z'=16,'c'=2,'tp'=16] {'z'}, dimensions={0} | all-to-all | bytes 180224 | tf_op jit(solution)/shard_map/all_to_all | solution.py:130
  73.3 0.2 convolution_convert_fusion.5
  73.5 0.2 convolution_convert_fusion.6
  73.8 12.1 %all_to_all.60 = bf16[16,64,256]{2,1,0:T(8,128)(2,1)S(1)} all-to-all(bf16[16,64,256]{2,1,0:T(8,128)(2,1)S(1)} %broadcast_in_dim.213), channel_id=1, replica_groups=mesh['z'=16,'c'=2,'tp'=16] {'tp'}, dimensions={0} | all-to-all | bytes 1048576 | tf_op jit(solution)/shard_map/all_to_all | solution.py:130
  86.0 6.1 %collective-permute-start.1 = (bf16[64,256]{1,0:T(8,128)(2,1)S(1)}, bf16[64,256]{1,0:T(8,128)(2,1)S(1)}, u32[]{:S(2)}, u32[]{:S(2)}) collective-permute-start(bf16[64,256]{1,0:T(8,128)(2,1)S(1)} %pad_maximum_fusion.4), channel_id=1, source_target_pairs={{0,16},{16,0},{1,17},{17,1},{2,18},{18,2},{3,19},{19,3},{4,20},{20... | collective-permute-start | bytes 98312 | tf_op jit(solution)/shard_map/ppermute | solution.py:211
  92.1 0.8 collective-permute-done.1
  93.0 0.2 multiply_convert_fusion
  93.2 0.1 reduce_sum.193
  93.4 0.2 fusion.19
  93.7 0.1 select_convert_fusion
  93.8 16.2 %all_to_all.61 = bf16[16,8,640]{2,1,0:T(8,128)(2,1)S(1)} all-to-all(bf16[16,8,640]{2,1,0:T(8,128)(2,1)S(1)} %pad_maximum_fusion.2), channel_id=1, replica_groups=mesh['z'=16,'c'=2,'tp'=16] {'z'}, dimensions={0} | all-to-all | bytes 327680 | tf_op jit(solution)/shard_map/all_to_all | solution.py:130
  110.0 0.1 mul.462
  110.1 0.2 fusion.69
  110.6 1.1 multiply_reduce_fusion.2
  111.7 0.1 multiply_reduce_fusion.5
  111.8 0.1 copy.70
  111.9 0.1 rsqrt.23
  112.1 21.5 %all_to_all.62 = bf16[32,8,128]{2,1,0:T(8,128)(2,1)S(1)} all-to-all(bf16[32,8,128]{2,1,0:T(8,128)(2,1)S(1)} %broadcast_in_dim.223), channel_id=1, replica_groups=mesh['z'=16,'c'=2,'tp'=16] {'z','c'}, dimensions={0} | all-to-all | bytes 131072 | tf_op jit(solution)/shard_map/all_to_all | solution.py:130
  133.6 0.1 convolution_convert_fusion.4
  133.7 0.1 convolution_convert_fusion.2
  133.9 0.1 convolution_convert_fusion.3
  134.1 12.6 %all_to_all.63 = bf16[16,64,256]{2,1,0:T(8,128)(2,1)S(1)} all-to-all(bf16[16,64,256]{2,1,0:T(8,128)(2,1)S(1)} %broadcast_in_dim.224), channel_id=1, replica_groups=mesh['z'=16,'c'=2,'tp'=16] {'tp'}, dimensions={0} | all-to-all | bytes 1048576 | tf_op jit(solution)/shard_map/all_to_all | solution.py:130
  146.7 0.1 fusion.44
  146.9 0.1 reduce_sum.202
  147.0 0.4 convolution_convert_fusion
  147.4 0.1 select_convert_fusion.1
  147.5 0.1 pad_maximum_fusion.1
  147.6 15.6 %all_to_all.64 = bf16[16,4,1536]{2,1,0:T(4,128)(2,1)S(1)} all-to-all(bf16[16,4,1536]{2,1,0:T(4,128)(2,1)S(1)} %pad_maximum_fusion.1), channel_id=1, replica_groups=mesh['z'=16,'c'=2,'tp'=16] {'z'}, dimensions={0} | all-to-all | bytes 393216 | tf_op jit(solution)/shard_map/all_to_all | solution.py:130
  163.3 0.1 convert_reduce_fusion.2
  163.4 0.2 fusion.73
  163.6 0.1 fusion.60
  163.7 19.6 %all_to_all.65 = bf16[16,4,704]{2,1,0:T(4,128)(2,1)S(1)} all-to-all(bf16[16,4,704]{2,1,0:T(4,128)(2,1)S(1)} %broadcast_in_dim.231), channel_id=1, replica_groups=mesh['z'=16,'c'=2,'tp'=16] {'z'}, dimensions={0} | all-to-all | bytes 180224 | tf_op jit(solution)/shard_map/all_to_all | solution.py:130
  183.3 0.2 convolution_bitcast_fusion.1
  183.5 0.2 convolution_bitcast_fusion
  183.7 0.1 copy.72
  183.8 0.1 reshape.508
  184.0 14.3 %all_to_all.66 = f32[32,1,512]{2,1,0:T(1,128)S(1)} all-to-all(f32[32,1,512]{2,1,0:T(1,128)S(1)} %copy.73), channel_id=1, replica_groups=mesh['z'=16,'c'=2,'tp'=16] {'c','tp'}, dimensions={0} | all-to-all | bytes 131072 | tf_op jit(solution)/shard_map/all_to_all | solution.py:130
  198.3 0.1 squeeze.10
  198.4 0.1 squeeze.11
  198.4 0.8 convolution_convert_fusion.7
  (110 shorter events, 1.7 us)
Async XLA Ops:
  0.6 12.1 %copy-start = (bf16[256,8]{0,1:T(8,128)(2,1)S(1)}, bf16[256,8]{0,1:T(8,128)(2,1)}, u32[]{:S(2)}) copy-start(bf16[256,8]{0,1:T(8,128)(2,1)} %param.19) | copy-start | bytes 12292
  0.6 11.0 %copy-start.18 = (s32[64]{0:T(128)S(1)}, s32[64]{0:T(128)}, u32[]{:S(2)}) copy-start(s32[64]{0:T(128)} %param.20) | copy-start | bytes 772
  0.7 12.1 %copy-start.17 = (f32[128]{0:T(128)S(1)}, f32[128]{0:T(128)}, u32[]{:S(2)}) copy-start(f32[128]{0:T(128)} %param.31) | copy-start | bytes 1540
  0.7 23.9 %copy-start.14 = (f32[128]{0:T(128)S(1)}, f32[128]{0:T(128)}, u32[]{:S(2)}) copy-start(f32[128]{0:T(128)} %param.34) | copy-start | bytes 1540
  0.7 23.9 %copy-start.15 = (f32[128]{0:T(128)S(1)}, f32[128]{0:T(128)}, u32[]{:S(2)}) copy-start(f32[128]{0:T(128)} %param.22) | copy-start | bytes 1540
  0.7 23.9 %copy-start.16 = (f32[128]{0:T(128)S(1)}, f32[128]{0:T(128)}, u32[]{:S(2)}) copy-start(f32[128]{0:T(128)} %param.26) | copy-start | bytes 1540
  2.9 21.6 %collective-permute-start = (bf16[4880,128]{1,0:T(8,128)(2,1)S(1)}, bf16[4880,128]{1,0:T(8,128)(2,1)S(1)}, u32[]{:S(2)}, u32[]{:S(2)}) collective-permute-start(bf16[4880,128]{1,0:T(8,128)(2,1)S(1)} %shard_map.194), channel_id=1, source_target_pairs={{0,16},{16,0},{1,17},{17,1},{2,18},{18,2},{3,19},{19,3},{4,20},{20... | collective-permute-start | bytes 3747848 | tf_op jit(solution)/shard_map/ppermute | solution.py:142
  13.9 10.1 %copy-start.22 = (s32[1,128]{1,0:T(1,128)}, s32[1,128]{1,0:T(1,128)S(1)}, u32[]{:S(2)}) copy-start(s32[1,128]{1,0:T(1,128)S(1)} %iota.80) | copy-start | bytes 1540
  23.9 1.1 copy-start.3
  23.9 1.1 copy-start.4
  25.3 0.6 copy-start.20
  25.4 48.1 %copy-start.1 = (bf16[704,128]{1,0:T(8,128)(2,1)S(1)}, bf16[704,128]{1,0:T(8,128)(2,1)}, u32[]{:S(2)}) copy-start(bf16[704,128]{1,0:T(8,128)(2,1)} %refs_9_.1) | copy-start | bytes 540676
  73.7 18.5 %copy-start.23 = (s32[1,128]{1,0:T(1,128)S(1)}, s32[1,128]{1,0:T(1,128)}, u32[]{:S(2)}) copy-start(s32[1,128]{1,0:T(1,128)} %copy-done.22) | copy-start | bytes 1540
  73.7 19.3 %copy-start.13 = (bf16[128,128]{1,0:T(8,128)(2,1)S(1)}, bf16[128,128]{1,0:T(8,128)(2,1)}, u32[]{:S(2)}) copy-start(bf16[128,128]{1,0:T(8,128)(2,1)} %compare_convert_fusion) | copy-start | bytes 98308
  73.7 19.6 %copy-start.9 = (bf16[128,128]{1,0:T(8,128)(2,1)S(1)}, bf16[128,128]{1,0:T(8,128)(2,1)}, u32[]{:S(2)}) copy-start(bf16[128,128]{1,0:T(8,128)(2,1)} %refs_4_.1) | copy-start | bytes 98308
  73.8 19.6 %copy-start.10 = (bf16[128,128]{1,0:T(8,128)(2,1)S(1)}, bf16[128,128]{1,0:T(8,128)(2,1)}, u32[]{:S(2)}) copy-start(bf16[128,128]{1,0:T(8,128)(2,1)} %refs_5_.1) | copy-start | bytes 98308
  73.8 19.6 %copy-start.11 = (bf16[128,128]{1,0:T(8,128)(2,1)S(1)}, bf16[128,128]{1,0:T(8,128)(2,1)}, u32[]{:S(2)}) copy-start(bf16[128,128]{1,0:T(8,128)(2,1)} %refs_6_.1) | copy-start | bytes 98308
  73.8 19.6 %copy-start.12 = (bf16[128,128]{1,0:T(8,128)(2,1)S(1)}, bf16[128,128]{1,0:T(8,128)(2,1)}, u32[]{:S(2)}) copy-start(bf16[128,128]{1,0:T(8,128)(2,1)} %refs_7_.1) | copy-start | bytes 98308
  86.0 6.9 %collective-permute-start.1 = (bf16[64,256]{1,0:T(8,128)(2,1)S(1)}, bf16[64,256]{1,0:T(8,128)(2,1)S(1)}, u32[]{:S(2)}, u32[]{:S(2)}) collective-permute-start(bf16[64,256]{1,0:T(8,128)(2,1)S(1)} %pad_maximum_fusion.4), channel_id=1, source_target_pairs={{0,16},{16,0},{1,17},{17,1},{2,18},{18,2},{3,19},{19,3},{4,20},{20... | collective-permute-start | bytes 98312 | tf_op jit(solution)/shard_map/ppermute | solution.py:211
  93.3 16.7 %copy-start.21 = (f32[2,4,1,1]{1,0,3,2:T(2,128)S(1)}, f32[2,4,1,1]{1,0,3,2:T(2,128)}, u32[]{:S(2)}) copy-start(f32[2,4,1,1]{1,0,3,2:T(2,128)} %compare_convert_fusion.1) | copy-start | bytes 100
  93.6 17.0 %copy-start.8 = (f32[2,1,128,128]{3,2,1,0:T(8,128)S(1)}, f32[2,1,128,128]{3,2,1,0:T(8,128)}, u32[]{:S(2)}) copy-start(f32[2,1,128,128]{3,2,1,0:T(8,128)} %param.21) | copy-start | bytes 393220
  93.6 18.4 %copy-start.19 = (f32[128]{0:T(128)S(1)}, f32[128]{0:T(128)}, u32[]{:S(2)}) copy-start(f32[128]{0:T(128)} %param.32) | copy-start | bytes 1540
  93.6 40.2 %copy-start.7 = (bf16[128,128]{1,0:T(8,128)(2,1)S(1)}, bf16[128,128]{1,0:T(8,128)(2,1)}, u32[]{:S(2)}) copy-start(bf16[128,128]{1,0:T(8,128)(2,1)} %refs_8_.1) | copy-start | bytes 98308
  133.8 13.1 %copy-start.5 = (bf16[128,704]{0,1:T(8,128)(2,1)S(1)}, bf16[128,704]{0,1:T(8,128)(2,1)}, u32[]{:S(2)}) copy-start(bf16[128,704]{0,1:T(8,128)(2,1)} %param.35) | copy-start | bytes 540676
  133.8 13.1 %copy-start.6 = (bf16[128,704]{0,1:T(8,128)(2,1)S(1)}, bf16[128,704]{0,1:T(8,128)(2,1)}, u32[]{:S(2)}) copy-start(bf16[128,704]{0,1:T(8,128)(2,1)} %param.36) | copy-start | bytes 540676
  147.4 35.9 %copy-start.2 = (bf16[704,128]{1,0:T(8,128)(2,1)S(1)}, bf16[704,128]{1,0:T(8,128)(2,1)}, u32[]{:S(2)}) copy-start(bf16[704,128]{1,0:T(8,128)(2,1)} %refs_10_.1) | copy-start | bytes 540676

commit v4 on v3

v4 whole, which is shorter than its diff:
```python
import functools

import jax
import jax.numpy as jnp
from jax import lax
from jax.experimental import pallas as pl
from jax.experimental.pallas import tpu as pltpu
from jax.sharding import Mesh
from jax.sharding import PartitionSpec as P

D = 4096
DK = 128
W = 4
EPSILON = 1e-06
LANES = 128
GAIN_ROWS = 16

f32 = jnp.float32
bf16 = jnp.bfloat16
barrier = lax.optimization_barrier


def matmul(a, b):
    return jnp.dot(a, b, preferred_element_type=f32)


def in_vmem(value):
    return pltpu.with_memory_space_constraint(value, pltpu.VMEM)


def matmul_t(a, b):
    return lax.dot_general(a, b, (((1,), (1,)), ((), ())), preferred_element_type=f32)


def iota(shape, axis):
    return lax.broadcasted_iota(jnp.int32, shape, axis)


def tables_of(lengths, tokens, core):
    slots = tokens.shape[1]
    packed = slots // 2
    half = packed // 2
    seqs = lengths.shape[1]
    slot = iota((1, slots), 1)
    seq, seq_of = iota((seqs, slots), 0), iota((seqs, slots), 1) // W
    wide = jnp.broadcast_to(lengths, (8, seqs)).astype(bf16)
    before = matmul(wide, (seq < seq_of).astype(f32).astype(bf16))[:1]
    own = matmul(wide, (seq == seq_of).astype(f32).astype(bf16))[:1]
    within = (slot % W).astype(f32)
    targets = jnp.where(within < own, before + within, -1.0)
    rows = iota((packed, slots), 0).astype(f32)
    table = (rows == targets).astype(f32).astype(bf16)
    rows = (iota((half, slots), 0) + core * half).astype(f32)
    my_table = (rows == targets).astype(f32).astype(bf16)
    place = iota((packed, 1), 0)
    my_slot = place // 8 * 16 + core * 8 + place % 8
    before, own = counted(lengths, my_slot)
    within = (my_slot % W).astype(f32)
    targets = jnp.where(within < own, before + within, -1.0)
    row_ids = ((iota((1, packed), 1) + core * half) % packed).astype(f32)
    spread = (targets == row_ids).astype(f32).astype(bf16)
    entry = matmul_t(tokens, table).astype(bf16)
    return table, my_table, spread, entry


def counted(lengths, slots):
    seq = iota((slots.shape[0], lengths.shape[1]), 1)
    before = jnp.sum(jnp.where(seq < slots // W, lengths, 0.0), axis=1, keepdims=True)
    own = jnp.sum(jnp.where(seq == slots // W, lengths, 0.0), axis=1, keepdims=True)
    return before, own


def front_kernel(count, *refs):
    weights, gains, refs = refs[:count], refs[count : count + 3], refs[count + 3 :]
    lengths, tokens, out, table, my_table, spread, entry, sems = refs
    copies = []
    at = 0
    for i, ref in enumerate(weights):
        rows = ref.shape[0]
        copies.append(pltpu.make_async_copy(ref, out.at[pl.ds(at, rows)], sems.at[i]))
        copies[-1].start()
        at += rows
    pieces = []
    for ref in gains:
        value = ref[...]
        high = value.astype(bf16).astype(f32)
        rest = value - high
        mid = rest.astype(bf16).astype(f32)
        pieces += [high, mid, rest - mid]
    pieces.append(jnp.zeros((GAIN_ROWS - len(pieces), LANES), f32))
    out[at:, :] = jnp.concatenate(pieces, axis=0).astype(bf16)
    results = tables_of(lengths[...].astype(f32), tokens[...], lax.axis_index("c"))
    for ref, value in zip((table, my_table, spread, entry), results, strict=True):
        ref[...] = value
    for copy in copies:
        copy.wait()


def front(weights, gains, lengths, tokens):
    rows = sum(w.shape[0] for w in weights) + GAIN_ROWS
    slots = tokens.shape[1]
    packed = slots // 2
    shapes = (
        (rows, weights[0].shape[1]),
        (packed, slots),
        (packed // 2, slots),
        (packed, packed),
        (tokens.shape[0], packed),
    )
    vmem = pl.BlockSpec(memory_space=pltpu.VMEM)
    return pl.pallas_call(
        functools.partial(front_kernel, len(weights)),
        in_specs=[pl.BlockSpec(memory_space=pl.ANY)] * len(weights)
        + [vmem] * (len(gains) + 2),
        out_specs=[vmem] * len(shapes),
        out_shape=[pltpu.VMEM(shape, bf16) for shape in shapes],
        scratch_shapes=[pltpu.SemaphoreType.DMA((len(weights),))],
    )(*weights, *[gain[None, :] for gain in gains], lengths[None, :], tokens)


def recur_kernel(sums, lengths, floors, head_gain, states, heads, new_states, scratch, sems):
    total = jnp.sum(sums[...].astype(f32), axis=0)
    slots = total.shape[0]
    at = 4 * DK
    squares = total[:, at : at + 1] + total[:, at + 1 : at + 2]
    total = total[:, :at] * lax.rsqrt(squares / D + EPSILON)
    queries = total[:, :DK]
    queries = queries * jax.nn.sigmoid(queries)
    fresh = total[:, 2 * DK : 3 * DK]
    gating = total[:, 3 * DK :]
    first = (lax.axis_index("z") * 2 + lax.axis_index("c")) * slots
    slot = iota((slots, 1), 0) + first
    _, own = counted(lengths[...].astype(f32), slot)
    live = ((slot % W).astype(f32) < own).astype(f32)
    floor = floors[...]
    forgets = floor + (1.0 - floor) * jax.nn.sigmoid(total[:, DK : 2 * DK])
    forgets = jnp.where(live > 0, forgets, 1.0)
    both = jnp.concatenate([queries, forgets], axis=0).T
    readings, copies = [], []
    for seq in range(states.shape[0]):
        carried = states[seq]
        for offset in range(W):
            row = seq * W + offset
            query = both[:, row : row + 1]
            forget = both[:, slots + row : slots + row + 1]
            carried = forget * carried + (1.0 - forget) * fresh[row : row + 1]
            readings.append(jnp.sum(query * carried, axis=0, keepdims=True))
        scratch[seq] = carried
        copies.append(pltpu.make_async_copy(scratch.at[seq], new_states.at[seq], sems.at[seq]))
        copies[-1].start()
    read_out = jnp.concatenate(readings, axis=0)
    meansq = jnp.mean(read_out * read_out, axis=1, keepdims=True)
    gate = gating * jax.nn.sigmoid(gating)
    out = read_out * lax.rsqrt(meansq + EPSILON) * head_gain[...] * gate * live
    heads[...] = out.astype(bf16)
    for copy in copies:
        copy.wait()


def recurred(sums, lengths, floors, head_gain, states):
    vmem = pl.BlockSpec(memory_space=pltpu.VMEM)
    return pl.pallas_call(
        recur_kernel,
        in_specs=[vmem] * 5,
        out_specs=[vmem, pl.BlockSpec(memory_space=pl.ANY)],
        out_shape=[
            pltpu.VMEM((sums.shape[1], DK), bf16),
            jax.ShapeDtypeStruct(states.shape, f32),
        ],
        scratch_shapes=[
            pltpu.VMEM(states.shape, f32),
            pltpu.SemaphoreType.DMA((states.shape[0],)),
        ],
    )(*[in_vmem(value) for value in (sums, lengths, floors, head_gain, states)])


def gain_rows(bundle, which):
    at = bundle.shape[0] - GAIN_ROWS + 3 * which
    return jnp.sum(bundle[at : at + 3, :].astype(f32), axis=0, keepdims=True)


def stats_of(own, other):
    total = jnp.sum(own * own + other * other, axis=1, keepdims=True)
    upper = total.astype(bf16).astype(f32)
    lanes = iota((1, LANES), 1)
    return jnp.where(lanes == 0, upper, jnp.where(lanes == 1, total - upper, 0.0)).astype(bf16)


def products(sent, own, other, gains, weights, product, exact):
    parts = []
    for rows, gain in zip((own, other), gains, strict=True):
        wide = rows * gain
        whole = wide.astype(bf16)
        if exact:
            rest = (wide - whole.astype(f32)).astype(bf16)
            whole = jnp.concatenate([whole, rest], axis=0)
        parts.append(whole)
    count = own.shape[0]
    at = 0
    for ours, theirs in weights:
        both = product(parts[0], ours) + product(parts[1], theirs)
        if exact:
            both = both[:count] + both[count:]
        sent[:, at : at + both.shape[1]] = both.astype(bf16)
        at += both.shape[1]
    sent[:, at:] = stats_of(own, other)


def halves_of(weights, bundle, at):
    pairs = []
    for weight in weights:
        pairs.append((weight[...], bundle[at : at + weight.shape[0], :]))
        at += weight.shape[0]
    return pairs


def entry_kernel(gathered, gain, gate, up, bundle, sent, resid):
    cols = gain.shape[1]
    first = lax.axis_index("c") == 0
    low, high = gathered[:cols, :].astype(f32), gathered[cols:, :].astype(f32)
    own = jnp.where(first, low, high).T
    other = jnp.where(first, high, low).T
    resid[:, :cols] = own.astype(bf16)
    resid[:, cols:] = other.astype(bf16)
    weights = halves_of((gate, up), bundle, 0)
    gains = (gain[...], gain_rows(bundle, 0))
    products(sent, own, other, gains, weights, matmul_t, True)


def mix_kernel(spread, resid, swapped, gain, query, forget, value, outgate, bundle, at, sent):
    cols = gain.shape[1]
    rows = jnp.concatenate([resid[...], swapped[...]], axis=0)
    rows = matmul(spread[...], rows)
    weights = halves_of((query, forget, value, outgate), bundle, at)
    gains = (gain[...], gain_rows(bundle, 1))
    products(sent, rows[:, :cols], rows[:, cols:], gains, weights, matmul, True)


def post_kernel(received, before, gain, gate, up, bundle, at, sent, resid):
    cols = gain.shape[1]
    total = jnp.sum(received[...].astype(f32), axis=0)
    rows = (before[...].astype(f32) + total).astype(bf16)
    resid[...] = rows
    rows = rows.astype(f32)
    weights = halves_of((gate, up), bundle, at)
    gains = (gain[...], gain_rows(bundle, 2))
    products(sent, rows[:, :cols], rows[:, cols:], gains, weights, matmul_t, False)


def in_kernel(kernel, shapes, *values):
    vmem = pl.BlockSpec(memory_space=pltpu.VMEM)
    return pl.pallas_call(
        kernel,
        in_specs=[vmem] * len(values),
        out_specs=[vmem] * len(shapes),
        out_shape=[pltpu.VMEM(shape, bf16) for shape in shapes],
    )(*[in_vmem(value) for value in values])


def local(
    tokens,
    lengths,
    states,
    gain_pre,
    pre_gate,
    pre_up,
    pre_down,
    gain_mix,
    query_weight,
    forget_weight,
    input_weight,
    outgate_weight,
    forget_floor,
    head_gain,
    mix_weight,
    gain_post,
    post_gate,
    post_up,
    post_down,
):
    core = lax.axis_index("c")
    z_count = lax.axis_size("z")
    tp_count = lax.axis_size("tp")
    slot_count = tokens.shape[0]
    packed = slot_count // 2
    half = packed // 2
    per_z = half // z_count
    own_cols = gain_pre.shape[0]
    hidden = pre_gate.shape[1]
    ff_cols = 2 * hidden
    head_cols = query_weight.shape[1]
    seq_local, heads_local = states.shape[:2]
    swap = [(0, 1), (1, 0)]

    side = {}

    def exchanged(value, axis):
        value, tied = barrier((value, dict(side)))
        value = lax.all_to_all(value, axis, split_axis=0, concat_axis=0, tiled=True)
        value, tied = barrier((value, tied))
        side.update(tied)
        return value

    def sent_to_all(value, axis):
        return exchanged(jnp.broadcast_to(value, (lax.axis_size(axis), *value.shape)), axis)

    mine = (pre_gate.T, pre_up.T, post_gate.T, post_up.T)
    mine += (query_weight, forget_weight, input_weight, outgate_weight)
    mine += (mix_weight, pre_down, post_down)
    gains = (gain_pre, gain_mix, gain_post)
    packed_own, table, my_table, spread, entry = front(mine, gains, lengths, tokens.T)
    bundle = lax.ppermute(packed_own, "c", swap)

    side["table"] = table
    side["my_table"] = my_table
    side["spread"] = spread
    side["core"] = core
    side["first"] = (lax.axis_index("tp") == 0).astype(f32)

    pieces = jnp.stack([entry[:, :half], entry[:, half:]])
    pieces = jnp.broadcast_to(pieces[:, None], (2, tp_count, *pieces.shape[1:]))
    gathered = exchanged(pieces.reshape(2 * tp_count, *pieces.shape[2:]), ("c", "tp"))
    starts = [0]
    for weight in mine:
        starts.append(starts[-1] + weight.shape[0])

    def other(i):
        return side["bundle"][starts[i] : starts[i + 1]]

    side["bundle"] = bundle
    sent_shape = (half, ff_cols + LANES)
    resid_shape = (half, 2 * own_cols)
    sent, side["resid"] = in_kernel(
        entry_kernel,
        (sent_shape, resid_shape),
        gathered.reshape(2 * own_cols, half),
        gain_pre[None, :],
        mine[0],
        mine[1],
        bundle,
    )

    def ff_hidden(sent):
        sent = sent.reshape(z_count, per_z, ff_cols + LANES)
        owned = jnp.sum(exchanged(sent, "z").astype(f32), axis=0)
        total = owned[:, ff_cols : ff_cols + 1] + owned[:, ff_cols + 1 : ff_cols + 2]
        scale = lax.rsqrt(total / D + EPSILON)
        gate = owned[:, :hidden] * scale
        up = owned[:, hidden:ff_cols] * scale
        act = (jax.nn.silu(gate) * up).astype(bf16)
        return sent_to_all(act, "z").reshape(half, hidden)

    def tp_partials(value, i):
        partial = jnp.concatenate([matmul(value, mine[i]), matmul(value, other(i))], axis=1)
        return sent_to_all(partial.astype(bf16), "tp")

    act = ff_hidden(sent)
    summed = jnp.sum(tp_partials(act, 9).astype(f32), axis=0)
    resid = (side["resid"].astype(f32) + 0.5 * summed).astype(bf16)
    side["resid"] = resid

    turned = jnp.concatenate([resid[:, own_cols:], resid[:, :own_cols]], axis=1)
    swapped = lax.ppermute(turned, "c", swap)
    (sent,) = in_kernel(
        lambda *refs: mix_kernel(*refs[:-1], starts[4], refs[-1]),
        ((packed, 4 * head_cols + LANES),),
        side["spread"],
        resid,
        swapped,
        gain_mix[None, :],
        *mine[4:8],
        side["bundle"],
    )
    sent = sent.reshape(z_count, seq_local * W, 4 * head_cols + LANES)
    side["recur"] = (lengths[None, :], forget_floor[None, :], head_gain[None, :])
    side["states"] = states.reshape(seq_local * heads_local, DK, DK)
    received = exchanged(sent, "z")
    head_out, new_states = recurred(received, *side.pop("recur"), side.pop("states"))
    all_heads = sent_to_all(head_out, ("z", "c")).reshape(slot_count, DK)
    head_rows = matmul(side["my_table"], all_heads).astype(bf16)
    sent, side["resid"] = in_kernel(
        lambda *refs: post_kernel(*refs[:-2], starts[2], *refs[-2:]),
        (sent_shape, resid_shape),
        tp_partials(head_rows, 8),
        side["resid"],
        gain_post[None, :],
        mine[2],
        mine[3],
        side["bundle"],
    )
    act = ff_hidden(sent)
    contract = (((0,), (1,)), ((), ()))
    finish = jnp.stack(
        [
            lax.dot_general(down, act, contract, preferred_element_type=f32)
            for down in (post_down, other(10))
        ]
    )
    residual = side["resid"].astype(f32).T.reshape(2, own_cols, half)
    finish = 0.5 * finish + side["first"] * residual
    finish = jnp.where(side["core"] == 0, finish, finish[::-1])
    piece = own_cols // tp_count
    finish = finish.reshape(2 * tp_count, piece * half)
    finished = jnp.sum(exchanged(finish, ("c", "tp")).reshape(2, tp_count, -1), axis=1)
    finished = finished.reshape(2, piece, half)
    finished = jnp.concatenate([finished[0], finished[1]], axis=1).astype(bf16)
    outcome = matmul(finished, side["table"]).astype(bf16).T
    return (outcome, new_states.reshape(states.shape))


def solution(mesh):
    kv = mesh.shape["kv"]
    tp = mesh.shape["tp"]
    cut = Mesh(mesh.devices.reshape(kv // 2, 2, tp), ("z", "c", "tp"))
    kv_axes = ("z", "c")
    placed = (
        P(None, ("z", "c", "tp")),
        P(),
        P(kv_axes, "tp", None, None),
        P(kv_axes),
        P(kv_axes, "tp"),
        P(kv_axes, "tp"),
        P("tp", kv_axes),
        P(kv_axes),
        P(kv_axes, "tp"),
        P(kv_axes, "tp"),
        P(kv_axes, "tp"),
        P(kv_axes, "tp"),
        P("tp"),
        P(),
        P("tp", kv_axes),
        P(kv_axes),
        P(kv_axes, "tp"),
        P(kv_axes, "tp"),
        P("tp", kv_axes),
    )
    return jax.shard_map(
        local,
        mesh=cut,
        in_specs=placed,
        out_specs=(P(None, ("z", "c", "tp")), P(kv_axes, "tp", None, None)),
        check_vma=False,
    )
```

time: 200 us -> 195 us (0.975)
  other arithmetic: 5.63 us -> 0.93 us
  Pallas kernels: 2.19 us -> 5.23 us
    pallas_call x1 -> x5, Pallas kernels: 2.19 us -> 5.23 us  [the longest x1 2.35 us: front(): pl.pallas_call(functools.partial(front_kernel, len(weights)), in_specs=[p...]
  transfers between devices with their start and end apart: 2 -> 2, of which waited for: 1 -> 1; matrix products, arithmetic and copies ran while one was open for 1% -> 0% of each run, Pallas kernels for 0% -> 0%
where the time goes in v4:
time: 195 us
  blocking collectives  168 us (86%)
  starting transfers between devices  15 us (8%)
  Pallas kernels  5.23 us (3%)
    all_to_all x10, blocking collectives, exchanged(): value = lax.all_to_all(value, axis, split_axis=0, concat_axis=0, tiled=True)  168 us
    ppermute x1, starting transfers between devices, local(): bundle = lax.ppermute(packed_own, 'c', swap)  8.75 us
    ppermute x1, starting transfers between devices, local(): swapped = lax.ppermute(turned, 'c', swap)  6.22 us
  transfers between devices with their start and end apart: 2, of which 1 were waited for; matrix products, arithmetic and copies ran while one was open for 0% of the time, Pallas kernels for 0%

profile of v4, /device:TPU:1, one launch (start us, length us, event | category | flops | bytes accessed | tf_op | source)
XLA Modules:
  0.0 194.6 jit_solution(17819811509669073907)
XLA Ops:
  0.7 2.3 %shard_map.194 = (bf16[4880,128]{1,0:T(8,128)(2,1)S(1)}, bf16[128,256]{1,0:T(8,128)(2,1)S(1)}, bf16[64,256]{1,0:T(8,128)(2,1)S(1)}, bf16[128,128]{1,0:T(8,128)(2,1)S(1)}, bf16[8,128]{1,0:T(8,128)(2,1)S(1)}) custom-call(bf16[704,128]{1,0:T(8,128)(2,1)} %bitcast.54, bf16[704,128]{1,0:T(8,128)(2,1)} %bitcast.56, bf16[704,128]{1,0:T(8,128)(2,1)} %bitcast.58, ...), custom_call_target="tpu_custom_call" | custom-call | tf_op jit(solution)/shard_map/pallas_call | solution.py:111
  3.0 8.7 %collective-permute-start = (bf16[4880,128]{1,0:T(8,128)(2,1)S(1)}, bf16[4880,128]{1,0:T(8,128)(2,1)S(1)}, u32[]{:S(2)}, u32[]{:S(2)}) collective-permute-start(bf16[4880,128]{1,0:T(8,128)(2,1)S(1)} %get-tuple-element.160), channel_id=1, source_target_pairs={{0,16},{16,0},{1,17},{17,1},{2,18},{18,2},{3,19},{19,3},{4,20},{20... | collective-permute-start | bytes 3747848 | tf_op jit(solution)/shard_map/ppermute | solution.py:312
  11.8 0.1 slice_bitcast_fusion.1
  11.9 0.1 reshape.67
  12.0 9.7 %all_to_all.57 = bf16[32,2,256]{2,1,0:T(2,128)(2,1)S(1)} all-to-all(bf16[32,2,256]{2,1,0:T(2,128)(2,1)S(1)} %reshape.67), channel_id=1, replica_groups=mesh['z'=16,'c'=2,'tp'=16] {'c','tp'}, dimensions={0} | all-to-all | bytes 65536 | tf_op jit(solution)/shard_map/all_to_all | solution.py:299
  21.7 0.1 reshape.68
  21.8 0.0 collective-permute-done.bundle.refs_8_.refs_5_
  21.9 0.0 copy-start.19
  21.9 0.6 shard_map.195
  22.4 0.1 reshape.53
  22.5 26.2 %all_to_all.58 = bf16[16,4,1536]{2,1,0:T(4,128)(2,1)S(1)} all-to-all(bf16[16,4,1536]{2,1,0:T(4,128)(2,1)S(1)} %reshape.53), channel_id=1, replica_groups=mesh['z'=16,'c'=2,'tp'=16] {'z'}, dimensions={0} | all-to-all | bytes 393216 | tf_op jit(solution)/shard_map/all_to_all | solution.py:299
  48.7 0.1 convert_reduce_fusion.2
  48.7 0.2 fusion.15
  48.9 0.1 fusion.7
  49.1 20.5 %all_to_all.59 = bf16[16,4,704]{2,1,0:T(4,128)(2,1)S(1)} all-to-all(bf16[16,4,704]{2,1,0:T(4,128)(2,1)S(1)} %broadcast_in_dim.48), channel_id=1, replica_groups=mesh['z'=16,'c'=2,'tp'=16] {'z'}, dimensions={0} | all-to-all | bytes 180224 | tf_op jit(solution)/shard_map/all_to_all | solution.py:299
  69.7 0.2 convolution_convert_fusion.4
  69.8 0.2 convolution_convert_fusion.3
  70.0 0.0 copy-start.6
  70.0 0.0 copy-start.7
  70.0 0.0 copy-start.8
  70.1 0.0 copy-start.9
  70.1 0.0 copy-start.14
  70.1 12.0 %all_to_all.60 = bf16[16,64,256]{2,1,0:T(8,128)(2,1)S(1)} all-to-all(bf16[16,64,256]{2,1,0:T(8,128)(2,1)S(1)} %broadcast_in_dim.49), channel_id=1, replica_groups=mesh['z'=16,'c'=2,'tp'=16] {'tp'}, dimensions={0} | all-to-all | bytes 1048576 | tf_op jit(solution)/shard_map/all_to_all | solution.py:299
  82.1 0.1 convert_reduce_fusion
  82.2 0.0 copy-start.10
  82.2 0.0 copy-start.15
  82.2 0.0 copy-start.17
  82.2 0.0 copy-start.18
  82.3 0.0 copy-start.21
  82.3 6.2 %collective-permute-start.1 = (bf16[64,256]{1,0:T(8,128)(2,1)S(1)}, bf16[64,256]{1,0:T(8,128)(2,1)S(1)}, u32[]{:S(2)}, u32[]{:S(2)}) collective-permute-start(bf16[64,256]{1,0:T(8,128)(2,1)S(1)} %pad_maximum_fusion.1), channel_id=1, source_target_pairs={{0,16},{16,0},{1,17},{17,1},{2,18},{18,2},{3,19},{19,3},{4,20},{20... | collective-permute-start | bytes 98312 | tf_op jit(solution)/shard_map/ppermute | solution.py:363
  88.5 0.8 collective-permute-done.1.refs_2_
  89.4 0.0 copy-done.9
  89.4 0.4 shard_map.196
  89.8 16.2 %all_to_all.61.sums = bf16[16,8,640]{2,1,0:T(8,128)(2,1)S(1)} all-to-all(bf16[16,8,640]{2,1,0:T(8,128)(2,1)S(1)} %bitcast.62), channel_id=1, replica_groups=mesh['z'=16,'c'=2,'tp'=16] {'z'}, dimensions={0} | all-to-all | bytes 327680 | tf_op jit(solution)/shard_map/all_to_all | solution.py:299
  106.0 0.0 copy-done.17
  106.0 0.0 copy-done.18
  106.1 0.0 copy-start.4
  106.1 0.0 copy-start.5
  106.1 0.0 copy-start.16
  106.1 1.4 shard_map.197
  107.5 21.5 %all_to_all.62 = bf16[32,8,128]{2,1,0:T(8,128)(2,1)S(1)} all-to-all(bf16[32,8,128]{2,1,0:T(8,128)(2,1)S(1)} %broadcast_in_dim.52), channel_id=1, replica_groups=mesh['z'=16,'c'=2,'tp'=16] {'z','c'}, dimensions={0} | all-to-all | bytes 131072 | tf_op jit(solution)/shard_map/all_to_all | solution.py:299
  129.0 0.1 convolution_convert_fusion.2
  129.1 0.0 copy-done.21
  129.1 0.1 convolution_convert_fusion.1
  129.3 0.1 convolution_convert_fusion
  129.5 12.7 %all_to_all.63.refs_0_ = bf16[16,64,256]{2,1,0:T(8,128)(2,1)S(1)} all-to-all(bf16[16,64,256]{2,1,0:T(8,128)(2,1)S(1)} %broadcast_in_dim.53), channel_id=1, replica_groups=mesh['z'=16,'c'=2,'tp'=16] {'tp'}, dimensions={0} | all-to-all | bytes 1048576 | tf_op jit(solution)/shard_map/all_to_all | solution.py:299
  142.3 0.5 shard_map.198
  142.8 0.0 copy-start.20
  142.8 0.1 reshape.58
  142.8 15.8 %all_to_all.64 = bf16[16,4,1536]{2,1,0:T(4,128)(2,1)S(1)} all-to-all(bf16[16,4,1536]{2,1,0:T(4,128)(2,1)S(1)} %reshape.58), channel_id=1, replica_groups=mesh['z'=16,'c'=2,'tp'=16] {'z'}, dimensions={0} | all-to-all | bytes 393216 | tf_op jit(solution)/shard_map/all_to_all | solution.py:299
  158.6 0.1 convert_reduce_fusion.1
  158.7 0.2 fusion.11
  158.9 0.1 fusion.6
  159.0 19.6 %all_to_all.65 = bf16[16,4,704]{2,1,0:T(4,128)(2,1)S(1)} all-to-all(bf16[16,4,704]{2,1,0:T(4,128)(2,1)S(1)} %broadcast_in_dim.54), channel_id=1, replica_groups=mesh['z'=16,'c'=2,'tp'=16] {'z'}, dimensions={0} | all-to-all | bytes 180224 | tf_op jit(solution)/shard_map/all_to_all | solution.py:299
  178.6 0.0 copy-done.20
  178.6 0.2 convolution_bitcast_fusion.1
  178.8 0.2 convolution_bitcast_fusion
  179.1 0.1 copy.39
  179.2 0.1 reshape.60
  179.2 0.1 copy.40
  179.3 14.3 %all_to_all.66 = f32[32,1,512]{2,1,0:T(1,128)S(1)} all-to-all(f32[32,1,512]{2,1,0:T(1,128)S(1)} %copy.40), channel_id=1, replica_groups=mesh['z'=16,'c'=2,'tp'=16] {'c','tp'}, dimensions={0} | all-to-all | bytes 131072 | tf_op jit(solution)/shard_map/all_to_all | solution.py:299
  193.6 0.1 squeeze.8
  193.7 0.1 squeeze.9
  193.8 0.8 convolution_convert_fusion.5
  (43 shorter events, 0.4 us)
Async XLA Ops:
  0.6 21.2 %copy-start.3 = (bf16[128,704]{0,1:T(8,128)(2,1)S(1)}, bf16[128,704]{0,1:T(8,128)(2,1)}, u32[]{:S(2)}) copy-start(bf16[128,704]{0,1:T(8,128)(2,1)} %param.24) | copy-start | bytes 540676
  0.6 21.2 %copy-start.2 = (bf16[128,704]{0,1:T(8,128)(2,1)S(1)}, bf16[128,704]{0,1:T(8,128)(2,1)}, u32[]{:S(2)}) copy-start(bf16[128,704]{0,1:T(8,128)(2,1)} %param.23) | copy-start | bytes 540676
  0.7 21.2 %copy-start.13 = (f32[128]{0:T(128)S(1)}, f32[128]{0:T(128)}, u32[]{:S(2)}) copy-start(f32[128]{0:T(128)} %param.22) | copy-start | bytes 1540
  3.0 45.6 %copy-start.11 = (bf16[128,256]{1,0:T(8,128)(2,1)}, bf16[128,256]{1,0:T(8,128)(2,1)S(1)}, u32[]{:S(2)}) copy-start(bf16[128,256]{1,0:T(8,128)(2,1)S(1)} %get-tuple-element.293) | copy-start | bytes 196612
  3.0 18.8 %collective-permute-start = (bf16[4880,128]{1,0:T(8,128)(2,1)S(1)}, bf16[4880,128]{1,0:T(8,128)(2,1)S(1)}, u32[]{:S(2)}, u32[]{:S(2)}) collective-permute-start(bf16[4880,128]{1,0:T(8,128)(2,1)S(1)} %get-tuple-element.160), channel_id=1, source_target_pairs={{0,16},{16,0},{1,17},{17,1},{2,18},{18,2},{3,19},{19,3},{4,20},{20... | collective-permute-start | bytes 3747848 | tf_op jit(solution)/shard_map/ppermute | solution.py:312
  21.8 107.4 %copy-start = (bf16[4880,128]{1,0:T(8,128)(2,1)}, bf16[4880,128]{1,0:T(8,128)(2,1)S(1)}, u32[]{:S(2)}) copy-start(bf16[4880,128]{1,0:T(8,128)(2,1)S(1)} %collective-permute-done.bundle.refs_8_.refs_5_) | copy-start | bytes 3747844
  21.9 47.8 %copy-start.19 = (bf16[704,128]{1,0:T(8,128)(2,1)S(1)}, bf16[704,128]{1,0:T(8,128)(2,1)}, u32[]{:S(2)}) copy-start(bf16[704,128]{1,0:T(8,128)(2,1)} %refs_9_.1) | copy-start | bytes 540676
  70.0 19.3 %copy-start.6 = (bf16[128,128]{1,0:T(8,128)(2,1)S(1)}, bf16[128,128]{1,0:T(8,128)(2,1)}, u32[]{:S(2)}) copy-start(bf16[128,128]{1,0:T(8,128)(2,1)} %refs_4_.3) | copy-start | bytes 98308
  70.0 19.3 %copy-start.7 = (bf16[128,128]{1,0:T(8,128)(2,1)S(1)}, bf16[128,128]{1,0:T(8,128)(2,1)}, u32[]{:S(2)}) copy-start(bf16[128,128]{1,0:T(8,128)(2,1)} %refs_5_.3) | copy-start | bytes 98308
  70.0 19.3 %copy-start.8 = (bf16[128,128]{1,0:T(8,128)(2,1)S(1)}, bf16[128,128]{1,0:T(8,128)(2,1)}, u32[]{:S(2)}) copy-start(bf16[128,128]{1,0:T(8,128)(2,1)} %refs_6_.3) | copy-start | bytes 98308
  70.1 19.3 %copy-start.9 = (bf16[128,128]{1,0:T(8,128)(2,1)S(1)}, bf16[128,128]{1,0:T(8,128)(2,1)}, u32[]{:S(2)}) copy-start(bf16[128,128]{1,0:T(8,128)(2,1)} %refs_7_.3) | copy-start | bytes 98308
  70.1 19.3 %copy-start.14 = (f32[128]{0:T(128)S(1)}, f32[128]{0:T(128)}, u32[]{:S(2)}) copy-start(f32[128]{0:T(128)} %param.26) | copy-start | bytes 1540
  82.2 23.9 %copy-start.10 = (f32[2,1,128,128]{3,2,1,0:T(8,128)S(1)}, f32[2,1,128,128]{3,2,1,0:T(8,128)}, u32[]{:S(2)}) copy-start(f32[2,1,128,128]{3,2,1,0:T(8,128)} %param.21) | copy-start | bytes 393220
  82.2 23.8 %copy-start.15 = (s32[64]{0:T(128)S(1)}, s32[64]{0:T(128)}, u32[]{:S(2)}) copy-start(s32[64]{0:T(128)} %param.20) | copy-start | bytes 772
  82.2 23.8 %copy-start.17 = (f32[128]{0:T(128)S(1)}, f32[128]{0:T(128)}, u32[]{:S(2)}) copy-start(f32[128]{0:T(128)} %param.31) | copy-start | bytes 1540
  82.2 23.8 %copy-start.18 = (f32[128]{0:T(128)S(1)}, f32[128]{0:T(128)}, u32[]{:S(2)}) copy-start(f32[128]{0:T(128)} %param.32) | copy-start | bytes 1540
  82.3 46.9 %copy-start.21 = (bf16[128,128]{1,0:T(8,128)(2,1)S(1)}, bf16[128,128]{1,0:T(8,128)(2,1)}, u32[]{:S(2)}) copy-start(bf16[128,128]{1,0:T(8,128)(2,1)} %refs_8_.1) | copy-start | bytes 98308
  82.3 7.1 %collective-permute-start.1 = (bf16[64,256]{1,0:T(8,128)(2,1)S(1)}, bf16[64,256]{1,0:T(8,128)(2,1)S(1)}, u32[]{:S(2)}, u32[]{:S(2)}) collective-permute-start(bf16[64,256]{1,0:T(8,128)(2,1)S(1)} %pad_maximum_fusion.1), channel_id=1, source_target_pairs={{0,16},{16,0},{1,17},{17,1},{2,18},{18,2},{3,19},{19,3},{4,20},{20... | collective-permute-start | bytes 98312 | tf_op jit(solution)/shard_map/ppermute | solution.py:363
  106.1 36.2 %copy-start.4 = (bf16[128,704]{0,1:T(8,128)(2,1)S(1)}, bf16[128,704]{0,1:T(8,128)(2,1)}, u32[]{:S(2)}) copy-start(bf16[128,704]{0,1:T(8,128)(2,1)} %param.35) | copy-start | bytes 540676
  106.1 36.2 %copy-start.5 = (bf16[128,704]{0,1:T(8,128)(2,1)S(1)}, bf16[128,704]{0,1:T(8,128)(2,1)}, u32[]{:S(2)}) copy-start(bf16[128,704]{0,1:T(8,128)(2,1)} %param.36) | copy-start | bytes 540676
  106.1 36.2 %copy-start.16 = (f32[128]{0:T(128)S(1)}, f32[128]{0:T(128)}, u32[]{:S(2)}) copy-start(f32[128]{0:T(128)} %param.34) | copy-start | bytes 1540
  129.4 12.8 %copy-start.1 = (bf16[4880,128]{1,0:T(8,128)(2,1)S(1)}, bf16[4880,128]{1,0:T(8,128)(2,1)}, u32[]{:S(2)}) copy-start(bf16[4880,128]{1,0:T(8,128)(2,1)} %copy-done) | copy-start | bytes 3747844
  142.8 35.9 %copy-start.20 = (bf16[704,128]{1,0:T(8,128)(2,1)S(1)}, bf16[704,128]{1,0:T(8,128)(2,1)}, u32[]{:S(2)}) copy-start(bf16[704,128]{1,0:T(8,128)(2,1)} %refs_10_.1) | copy-start | bytes 540676
  158.6 35.2 %copy-start.12 = (bf16[128,256]{1,0:T(8,128)(2,1)S(1)}, bf16[128,256]{1,0:T(8,128)(2,1)}, u32[]{:S(2)}) copy-start(bf16[128,256]{1,0:T(8,128)(2,1)} %copy-done.11) | copy-start | bytes 196612

commit v5 on v4

--- a/solution.py
+++ b/solution.py
@@ -18,6 +18,7 @@
 f32 = jnp.float32
 bf16 = jnp.bfloat16
 barrier = lax.optimization_barrier
+SMALL = pltpu.CompilerParams(vmem_limit_bytes=16 * 2**20)
 
 
 def matmul(a, b):
@@ -118,7 +119,7 @@
     )(*weights, *[gain[None, :] for gain in gains], lengths[None, :], tokens)
 
 
-def recur_kernel(sums, lengths, floors, head_gain, states, heads, new_states, scratch, sems):
+def recur_kernel(sums, lengths, floors, head_gain, states, heads, new_states):
     total = jnp.sum(sums[...].astype(f32), axis=0)
     slots = total.shape[0]
     at = 4 * DK
@@ -136,7 +137,7 @@
     forgets = floor + (1.0 - floor) * jax.nn.sigmoid(total[:, DK : 2 * DK])
     forgets = jnp.where(live > 0, forgets, 1.0)
     both = jnp.concatenate([queries, forgets], axis=0).T
-    readings, copies = [], []
+    readings = []
     for seq in range(states.shape[0]):
         carried = states[seq]
         for offset in range(W):
@@ -145,16 +146,12 @@
             forget = both[:, slots + row : slots + row + 1]
             carried = forget * carried + (1.0 - forget) * fresh[row : row + 1]
             readings.append(jnp.sum(query * carried, axis=0, keepdims=True))
-        scratch[seq] = carried
-        copies.append(pltpu.make_async_copy(scratch.at[seq], new_states.at[seq], sems.at[seq]))
-        copies[-1].start()
+        new_states[seq] = carried
     read_out = jnp.concatenate(readings, axis=0)
     meansq = jnp.mean(read_out * read_out, axis=1, keepdims=True)
     gate = gating * jax.nn.sigmoid(gating)
     out = read_out * lax.rsqrt(meansq + EPSILON) * head_gain[...] * gate * live
     heads[...] = out.astype(bf16)
-    for copy in copies:
-        copy.wait()
 
 
 def recurred(sums, lengths, floors, head_gain, states):
@@ -162,15 +159,9 @@
     return pl.pallas_call(
         recur_kernel,
         in_specs=[vmem] * 5,
-        out_specs=[vmem, pl.BlockSpec(memory_space=pl.ANY)],
-        out_shape=[
-            pltpu.VMEM((sums.shape[1], DK), bf16),
-            jax.ShapeDtypeStruct(states.shape, f32),
-        ],
-        scratch_shapes=[
-            pltpu.VMEM(states.shape, f32),
-            pltpu.SemaphoreType.DMA((states.shape[0],)),
-        ],
+        out_specs=[vmem, vmem],
+        out_shape=[pltpu.VMEM((sums.shape[1], DK), bf16), pltpu.VMEM(states.shape, f32)],
+        compiler_params=SMALL,
     )(*[in_vmem(value) for value in (sums, lengths, floors, head_gain, states)])
 
 
@@ -247,13 +238,60 @@
     products(sent, rows[:, :cols], rows[:, cols:], gains, weights, matmul_t, False)
 
 
-def in_kernel(kernel, shapes, *values):
+def put_partials(rows, weight, other, out):
+    cols = weight.shape[1]
+    own = matmul(rows, weight[...]).astype(bf16)
+    other = matmul(rows, other).astype(bf16)
+    for i in range(out.shape[0]):
+        out[i, :, :cols] = own
+        out[i, :, cols:] = other
+
+
+def down_kernel(rows, weight, bundle, at, out):
+    put_partials(rows[...], weight, bundle[at : at + weight.shape[0], :], out)
+
+
+def heads_kernel(heads, table, weight, states, bundle, at, out, new_states, sem):
+    copy = pltpu.make_async_copy(states, new_states, sem)
+    copy.start()
+    rows = matmul(table[...], heads[...]).astype(bf16)
+    put_partials(rows, weight, bundle[at : at + weight.shape[0], :], out)
+    copy.wait()
+
+
+def head_partials(heads, table, weight, states, bundle, at, shape):
+    vmem = pl.BlockSpec(memory_space=pltpu.VMEM)
+    values = [in_vmem(value) for value in (heads, table, weight, states, bundle)]
+    return pl.pallas_call(
+        lambda *refs: heads_kernel(*refs[:5], at, *refs[5:]),
+        in_specs=[vmem] * len(values),
+        out_specs=[vmem, pl.BlockSpec(memory_space=pl.ANY)],
+        out_shape=[pltpu.VMEM(shape, bf16), jax.ShapeDtypeStruct(states.shape, f32)],
+        scratch_shapes=[pltpu.SemaphoreType.DMA],
+        compiler_params=SMALL,
+    )(*values)
+
+
+def finish_kernel(rows, resid, weight, bundle, at, out):
+    cols = weight.shape[1]
+    first = (lax.axis_index("tp") == 0).astype(f32)
+    own = 0.5 * matmul(rows[...], weight[...]) + first * resid[:, :cols].astype(f32)
+    other = matmul(rows[...], bundle[at : at + weight.shape[0], :])
+    other = 0.5 * other + first * resid[:, cols:].astype(f32)
+    own, other = own.T, other.T
+    leads = lax.axis_index("c") == 0
+    out[:cols, :] = jnp.where(leads, own, other)
+    out[cols:, :] = jnp.where(leads, other, own)
+
+
+def in_kernel(kernel, shapes, *values, dtype=bf16):
     vmem = pl.BlockSpec(memory_space=pltpu.VMEM)
     return pl.pallas_call(
         kernel,
         in_specs=[vmem] * len(values),
         out_specs=[vmem] * len(shapes),
-        out_shape=[pltpu.VMEM(shape, bf16) for shape in shapes],
+        out_shape=[pltpu.VMEM(shape, dtype) for shape in shapes],
+        compiler_params=SMALL,
     )(*[in_vmem(value) for value in values])
 
 
@@ -278,7 +316,6 @@
     post_up,
     post_down,
 ):
-    core = lax.axis_index("c")
     z_count = lax.axis_size("z")
     tp_count = lax.axis_size("tp")
     slot_count = tokens.shape[0]
@@ -314,8 +351,6 @@
     side["table"] = table
     side["my_table"] = my_table
     side["spread"] = spread
-    side["core"] = core
-    side["first"] = (lax.axis_index("tp") == 0).astype(f32)
 
     pieces = jnp.stack([entry[:, :half], entry[:, half:]])
     pieces = jnp.broadcast_to(pieces[:, None], (2, tp_count, *pieces.shape[1:]))
@@ -323,9 +358,6 @@
     starts = [0]
     for weight in mine:
         starts.append(starts[-1] + weight.shape[0])
-
-    def other(i):
-        return side["bundle"][starts[i] : starts[i + 1]]
 
     side["bundle"] = bundle
     sent_shape = (half, ff_cols + LANES)
@@ -350,12 +382,16 @@
         act = (jax.nn.silu(gate) * up).astype(bf16)
         return sent_to_all(act, "z").reshape(half, hidden)
 
-    def tp_partials(value, i):
-        partial = jnp.concatenate([matmul(value, mine[i]), matmul(value, other(i))], axis=1)
-        return sent_to_all(partial.astype(bf16), "tp")
-
+    partial_shape = (tp_count, *resid_shape)
     act = ff_hidden(sent)
-    summed = jnp.sum(tp_partials(act, 9).astype(f32), axis=0)
+    (partials,) = in_kernel(
+        lambda *refs: down_kernel(*refs[:-1], starts[9], refs[-1]),
+        (partial_shape,),
+        act,
+        pre_down,
+        side["bundle"],
+    )
+    summed = jnp.sum(exchanged(partials, "tp").astype(f32), axis=0)
     resid = (side["resid"].astype(f32) + 0.5 * summed).astype(bf16)
     side["resid"] = resid
 
@@ -375,13 +411,21 @@
     side["recur"] = (lengths[None, :], forget_floor[None, :], head_gain[None, :])
     side["states"] = states.reshape(seq_local * heads_local, DK, DK)
     received = exchanged(sent, "z")
-    head_out, new_states = recurred(received, *side.pop("recur"), side.pop("states"))
+    head_out, side["states"] = recurred(received, *side.pop("recur"), side["states"])
     all_heads = sent_to_all(head_out, ("z", "c")).reshape(slot_count, DK)
-    head_rows = matmul(side["my_table"], all_heads).astype(bf16)
+    partials, new_states = head_partials(
+        all_heads,
+        side["my_table"],
+        mix_weight,
+        side.pop("states"),
+        side["bundle"],
+        starts[8],
+        partial_shape,
+    )
     sent, side["resid"] = in_kernel(
         lambda *refs: post_kernel(*refs[:-2], starts[2], *refs[-2:]),
         (sent_shape, resid_shape),
-        tp_partials(head_rows, 8),
+        exchanged(partials, "tp"),
         side["resid"],
         gain_post[None, :],
         mine[2],
@@ -389,16 +433,15 @@
         side["bundle"],
     )
     act = ff_hidden(sent)
-    contract = (((0,), (1,)), ((), ()))
-    finish = jnp.stack(
-        [
-            lax.dot_general(down, act, contract, preferred_element_type=f32)
-            for down in (post_down, other(10))
-        ]
-    )
-    residual = side["resid"].astype(f32).T.reshape(2, own_cols, half)
-    finish = 0.5 * finish + side["first"] * residual
-    finish = jnp.where(side["core"] == 0, finish, finish[::-1])
+    (finish,) = in_kernel(
+        lambda *refs: finish_kernel(*refs[:-1], starts[10], refs[-1]),
+        ((2 * own_cols, half),),
+        act,
+        side["resid"],
+        post_down,
+        side["bundle"],
+        dtype=f32,
+    )
     piece = own_cols // tp_count
     finish = finish.reshape(2 * tp_count, piece * half)
     finished = jnp.sum(exchanged(finish, ("c", "tp")).reshape(2, tp_count, -1), axis=1)

time: 195 us -> 194 us (level)
  no operation moved by 1% of the time
where the time goes in v5:
time: 194 us
  blocking collectives  168 us (87%)
  starting transfers between devices  15 us (8%)
  Pallas kernels  5.94 us (3%)
    all_to_all x10, blocking collectives, exchanged(): value = lax.all_to_all(value, axis, split_axis=0, concat_axis=0, tiled=True)  168 us
    ppermute x1, starting transfers between devices, local(): bundle = lax.ppermute(packed_own, 'c', swap)  8.75 us
    ppermute x1, starting transfers between devices, local(): swapped = lax.ppermute(turned, 'c', swap)  6.22 us
  transfers between devices with their start and end apart: 2, of which 1 were waited for; matrix products, arithmetic and copies ran while one was open for 0% of the time, Pallas kernels for 0%

profile of v5, /device:TPU:1, one launch (start us, length us, event | category | flops | bytes accessed | tf_op | source)
XLA Modules:
  0.0 193.8 jit_solution(998847858316753171)
XLA Ops:
  0.6 0.0 copy-start.1
  0.6 0.0 copy-start
  0.7 0.0 copy-start.12
  0.7 2.3 %shard_map.194 = (bf16[4880,128]{1,0:T(8,128)(2,1)S(1)}, bf16[128,256]{1,0:T(8,128)(2,1)S(1)}, bf16[64,256]{1,0:T(8,128)(2,1)S(1)}, bf16[128,128]{1,0:T(8,128)(2,1)S(1)}, bf16[8,128]{1,0:T(8,128)(2,1)S(1)}) custom-call(bf16[704,128]{1,0:T(8,128)(2,1)} %bitcast.30, bf16[704,128]{1,0:T(8,128)(2,1)} %bitcast.32, bf16[704,128]{1,0:T(8,128)(2,1)} %bitcast.34, ...), custom_call_target="tpu_custom_call" | custom-call | tf_op jit(solution)/shard_map/pallas_call | solution.py:112
  3.0 8.7 %collective-permute-start = (bf16[4880,128]{1,0:T(8,128)(2,1)S(1)}, bf16[4880,128]{1,0:T(8,128)(2,1)S(1)}, u32[]{:S(2)}, u32[]{:S(2)}) collective-permute-start(bf16[4880,128]{1,0:T(8,128)(2,1)S(1)} %get-tuple-element.126), channel_id=1, source_target_pairs={{0,16},{16,0},{1,17},{17,1},{2,18},{18,2},{3,19},{19,3},{4,20},{20... | collective-permute-start | bytes 3747848 | tf_op jit(solution)/shard_map/ppermute | solution.py:349
  11.8 0.1 slice_bitcast_fusion.1
  11.9 0.1 reshape.64
  12.0 9.7 %all_to_all.57 = bf16[32,2,256]{2,1,0:T(2,128)(2,1)S(1)} all-to-all(bf16[32,2,256]{2,1,0:T(2,128)(2,1)S(1)} %reshape.64), channel_id=1, replica_groups=mesh['z'=16,'c'=2,'tp'=16] {'c','tp'}, dimensions={0} | all-to-all | bytes 65536 | tf_op jit(solution)/shard_map/all_to_all | solution.py:336
  21.7 0.1 reshape.65
  21.8 0.0 collective-permute-done.bundle.refs_2_.refs_8_.refs_4_.refs_5_.refs_3_
  21.8 0.0 copy-done.1
  21.8 0.0 copy-done
  21.8 0.0 copy-done.12
  21.8 0.0 copy-start.5
  21.9 0.6 shard_map.195
  22.4 0.1 reshape.50
  22.5 26.2 %all_to_all.58 = bf16[16,4,1536]{2,1,0:T(4,128)(2,1)S(1)} all-to-all(bf16[16,4,1536]{2,1,0:T(4,128)(2,1)S(1)} %reshape.50), channel_id=1, replica_groups=mesh['z'=16,'c'=2,'tp'=16] {'z'}, dimensions={0} | all-to-all | bytes 393216 | tf_op jit(solution)/shard_map/all_to_all | solution.py:336
  48.6 0.1 convert_reduce_fusion.2
  48.7 0.2 fusion.11
  48.9 0.1 fusion.3
  49.0 20.5 %all_to_all.59 = bf16[16,4,704]{2,1,0:T(4,128)(2,1)S(1)} all-to-all(bf16[16,4,704]{2,1,0:T(4,128)(2,1)S(1)} %broadcast_in_dim.42), channel_id=1, replica_groups=mesh['z'=16,'c'=2,'tp'=16] {'z'}, dimensions={0} | all-to-all | bytes 180224 | tf_op jit(solution)/shard_map/all_to_all | solution.py:336
  69.6 0.0 copy-done.5
  69.6 0.3 shard_map.196
  69.9 0.0 copy-start.6
  69.9 0.0 copy-start.7
  69.9 0.0 copy-start.8
  69.9 0.0 copy-start.9
  70.0 0.0 copy-start.13
  70.0 12.1 %all_to_all.60 = bf16[16,64,256]{2,1,0:T(8,128)(2,1)S(1)} all-to-all(bf16[16,64,256]{2,1,0:T(8,128)(2,1)S(1)} %shard_map.196), channel_id=1, replica_groups=mesh['z'=16,'c'=2,'tp'=16] {'tp'}, dimensions={0} | all-to-all | bytes 1048576 | tf_op jit(solution)/shard_map/all_to_all | solution.py:336
  82.1 0.1 convert_reduce_fusion
  82.1 0.0 copy-start.11
  82.1 0.0 copy-start.14
  82.2 0.0 copy-start.16
  82.2 0.0 copy-start.17
  82.2 0.0 copy-start.10
  82.2 6.2 %collective-permute-start.1 = (bf16[64,256]{1,0:T(8,128)(2,1)S(1)}, bf16[64,256]{1,0:T(8,128)(2,1)S(1)}, u32[]{:S(2)}, u32[]{:S(2)}) collective-permute-start(bf16[64,256]{1,0:T(8,128)(2,1)S(1)} %pad_maximum_fusion), channel_id=1, source_target_pairs={{0,16},{16,0},{1,17},{17,1},{2,18},{18,2},{3,19},{19,3},{4,20},{20... | collective-permute-start | bytes 98312 | tf_op jit(solution)/shard_map/ppermute | solution.py:399
  88.5 0.8 collective-permute-done.1.refs_2_
  89.3 0.0 copy-done.6
  89.3 0.0 copy-done.7
  89.3 0.0 copy-done.8
  89.3 0.0 copy-done.9
  89.3 0.0 copy-done.13
  89.3 0.4 shard_map.197
  89.8 16.2 %all_to_all.61.sums = bf16[16,8,640]{2,1,0:T(8,128)(2,1)S(1)} all-to-all(bf16[16,8,640]{2,1,0:T(8,128)(2,1)S(1)} %bitcast.38), channel_id=1, replica_groups=mesh['z'=16,'c'=2,'tp'=16] {'z'}, dimensions={0} | all-to-all | bytes 327680 | tf_op jit(solution)/shard_map/all_to_all | solution.py:336
  106.0 0.0 copy-done.11
  106.0 0.9 shard_map.198
  106.9 21.5 %all_to_all.62 = bf16[32,8,128]{2,1,0:T(8,128)(2,1)S(1)} all-to-all(bf16[32,8,128]{2,1,0:T(8,128)(2,1)S(1)} %broadcast_in_dim.45), channel_id=1, replica_groups=mesh['z'=16,'c'=2,'tp'=16] {'z','c'}, dimensions={0} | all-to-all | bytes 131072 | tf_op jit(solution)/shard_map/all_to_all | solution.py:336
  128.4 0.7 shard_map.199
  129.1 12.6 %all_to_all.63.refs_0_ = bf16[16,64,256]{2,1,0:T(8,128)(2,1)S(1)} all-to-all(bf16[16,64,256]{2,1,0:T(8,128)(2,1)S(1)} %get-tuple-element.201), channel_id=1, replica_groups=mesh['z'=16,'c'=2,'tp'=16] {'tp'}, dimensions={0} | all-to-all | bytes 1048576 | tf_op jit(solution)/shard_map/all_to_all | solution.py:336
  141.7 0.5 shard_map.200
  142.2 0.0 copy-start.2
  142.2 0.1 reshape.55
  142.3 15.8 %all_to_all.64 = bf16[16,4,1536]{2,1,0:T(4,128)(2,1)S(1)} all-to-all(bf16[16,4,1536]{2,1,0:T(4,128)(2,1)S(1)} %reshape.55), channel_id=1, replica_groups=mesh['z'=16,'c'=2,'tp'=16] {'z'}, dimensions={0} | all-to-all | bytes 393216 | tf_op jit(solution)/shard_map/all_to_all | solution.py:336
  158.1 0.1 convert_reduce_fusion.1
  158.2 0.2 fusion.7
  158.3 0.1 fusion.2
  158.5 19.6 %all_to_all.65 = bf16[16,4,704]{2,1,0:T(4,128)(2,1)S(1)} all-to-all(bf16[16,4,704]{2,1,0:T(4,128)(2,1)S(1)} %broadcast_in_dim.46), channel_id=1, replica_groups=mesh['z'=16,'c'=2,'tp'=16] {'z'}, dimensions={0} | all-to-all | bytes 180224 | tf_op jit(solution)/shard_map/all_to_all | solution.py:336
  178.1 0.3 shard_map.201
  178.4 0.1 reshape.57
  178.5 0.1 copy.29
  178.6 14.2 %all_to_all.66 = f32[32,1,512]{2,1,0:T(1,128)S(1)} all-to-all(f32[32,1,512]{2,1,0:T(1,128)S(1)} %copy.29), channel_id=1, replica_groups=mesh['z'=16,'c'=2,'tp'=16] {'c','tp'}, dimensions={0} | all-to-all | bytes 131072 | tf_op jit(solution)/shard_map/all_to_all | solution.py:336
  192.9 0.1 squeeze.8
  192.9 0.1 squeeze.9
  193.0 0.8 convolution_convert_fusion
  (24 shorter events, 0.3 us)
Async XLA Ops:
  0.6 21.2 %copy-start.1 = (bf16[128,704]{0,1:T(8,128)(2,1)S(1)}, bf16[128,704]{0,1:T(8,128)(2,1)}, u32[]{:S(2)}) copy-start(bf16[128,704]{0,1:T(8,128)(2,1)} %param.24) | copy-start | bytes 540676
  0.6 21.2 %copy-start = (bf16[128,704]{0,1:T(8,128)(2,1)S(1)}, bf16[128,704]{0,1:T(8,128)(2,1)}, u32[]{:S(2)}) copy-start(bf16[128,704]{0,1:T(8,128)(2,1)} %param.23) | copy-start | bytes 540676
  0.7 21.2 %copy-start.12 = (f32[128]{0:T(128)S(1)}, f32[128]{0:T(128)}, u32[]{:S(2)}) copy-start(f32[128]{0:T(128)} %param.22) | copy-start | bytes 1540
  3.0 18.8 %collective-permute-start = (bf16[4880,128]{1,0:T(8,128)(2,1)S(1)}, bf16[4880,128]{1,0:T(8,128)(2,1)S(1)}, u32[]{:S(2)}, u32[]{:S(2)}) collective-permute-start(bf16[4880,128]{1,0:T(8,128)(2,1)S(1)} %get-tuple-element.126), channel_id=1, source_target_pairs={{0,16},{16,0},{1,17},{17,1},{2,18},{18,2},{3,19},{19,3},{4,20},{20... | collective-permute-start | bytes 3747848 | tf_op jit(solution)/shard_map/ppermute | solution.py:349
  21.8 47.8 %copy-start.5 = (bf16[704,128]{1,0:T(8,128)(2,1)S(1)}, bf16[704,128]{1,0:T(8,128)(2,1)}, u32[]{:S(2)}) copy-start(bf16[704,128]{1,0:T(8,128)(2,1)} %refs_1_.1) | copy-start | bytes 540676
  69.9 19.4 %copy-start.6 = (bf16[128,128]{1,0:T(8,128)(2,1)S(1)}, bf16[128,128]{1,0:T(8,128)(2,1)}, u32[]{:S(2)}) copy-start(bf16[128,128]{1,0:T(8,128)(2,1)} %refs_4_.3) | copy-start | bytes 98308
  69.9 19.4 %copy-start.7 = (bf16[128,128]{1,0:T(8,128)(2,1)S(1)}, bf16[128,128]{1,0:T(8,128)(2,1)}, u32[]{:S(2)}) copy-start(bf16[128,128]{1,0:T(8,128)(2,1)} %refs_5_.3) | copy-start | bytes 98308
  69.9 19.4 %copy-start.8 = (bf16[128,128]{1,0:T(8,128)(2,1)S(1)}, bf16[128,128]{1,0:T(8,128)(2,1)}, u32[]{:S(2)}) copy-start(bf16[128,128]{1,0:T(8,128)(2,1)} %refs_6_.3) | copy-start | bytes 98308
  69.9 19.4 %copy-start.9 = (bf16[128,128]{1,0:T(8,128)(2,1)S(1)}, bf16[128,128]{1,0:T(8,128)(2,1)}, u32[]{:S(2)}) copy-start(bf16[128,128]{1,0:T(8,128)(2,1)} %refs_7_.3) | copy-start | bytes 98308
  70.0 19.4 %copy-start.13 = (f32[128]{0:T(128)S(1)}, f32[128]{0:T(128)}, u32[]{:S(2)}) copy-start(f32[128]{0:T(128)} %param.26) | copy-start | bytes 1540
  82.1 23.9 %copy-start.11 = (f32[2,1,128,128]{3,2,1,0:T(8,128)S(1)}, f32[2,1,128,128]{3,2,1,0:T(8,128)}, u32[]{:S(2)}) copy-start(f32[2,1,128,128]{3,2,1,0:T(8,128)} %param.21) | copy-start | bytes 393220
  82.1 23.8 %copy-start.14 = (s32[64]{0:T(128)S(1)}, s32[64]{0:T(128)}, u32[]{:S(2)}) copy-start(s32[64]{0:T(128)} %param.20) | copy-start | bytes 772
  82.2 23.8 %copy-start.16 = (f32[128]{0:T(128)S(1)}, f32[128]{0:T(128)}, u32[]{:S(2)}) copy-start(f32[128]{0:T(128)} %param.31) | copy-start | bytes 1540
  82.2 23.8 %copy-start.17 = (f32[128]{0:T(128)S(1)}, f32[128]{0:T(128)}, u32[]{:S(2)}) copy-start(f32[128]{0:T(128)} %param.32) | copy-start | bytes 1540
  82.2 46.2 %copy-start.10 = (bf16[128,128]{1,0:T(8,128)(2,1)S(1)}, bf16[128,128]{1,0:T(8,128)(2,1)}, u32[]{:S(2)}) copy-start(bf16[128,128]{1,0:T(8,128)(2,1)} %refs_2_.2) | copy-start | bytes 98308
  82.2 7.1 %collective-permute-start.1 = (bf16[64,256]{1,0:T(8,128)(2,1)S(1)}, bf16[64,256]{1,0:T(8,128)(2,1)S(1)}, u32[]{:S(2)}, u32[]{:S(2)}) collective-permute-start(bf16[64,256]{1,0:T(8,128)(2,1)S(1)} %pad_maximum_fusion), channel_id=1, source_target_pairs={{0,16},{16,0},{1,17},{17,1},{2,18},{18,2},{3,19},{19,3},{4,20},{20... | collective-permute-start | bytes 98312 | tf_op jit(solution)/shard_map/ppermute | solution.py:399
  128.4 13.3 %copy-start.3 = (bf16[128,704]{0,1:T(8,128)(2,1)S(1)}, bf16[128,704]{0,1:T(8,128)(2,1)}, u32[]{:S(2)}) copy-start(bf16[128,704]{0,1:T(8,128)(2,1)} %param.35) | copy-start | bytes 540676
  128.4 13.3 %copy-start.4 = (bf16[128,704]{0,1:T(8,128)(2,1)S(1)}, bf16[128,704]{0,1:T(8,128)(2,1)}, u32[]{:S(2)}) copy-start(bf16[128,704]{0,1:T(8,128)(2,1)} %param.36) | copy-start | bytes 540676
  128.4 13.3 %copy-start.15 = (f32[128]{0:T(128)S(1)}, f32[128]{0:T(128)}, u32[]{:S(2)}) copy-start(f32[128]{0:T(128)} %param.34) | copy-start | bytes 1540
  142.2 35.9 %copy-start.2 = (bf16[704,128]{1,0:T(8,128)(2,1)S(1)}, bf16[704,128]{1,0:T(8,128)(2,1)}, u32[]{:S(2)}) copy-start(bf16[704,128]{1,0:T(8,128)(2,1)} %refs_2_.3) | copy-start | bytes 540676

commit v6 on v5

--- a/solution.py
+++ b/solution.py
@@ -72,8 +72,13 @@
 
 
 def front_kernel(count, *refs):
-    weights, gains, refs = refs[:count], refs[count : count + 3], refs[count + 3 :]
-    lengths, tokens, out, table, my_table, spread, entry, sems = refs
+    weights, small, refs = refs[:count], refs[count : count + 5], refs[count + 5 :]
+    out, table, my_table, spread, entry, sems, *held = refs
+    first = []
+    for i, (ref, copied) in enumerate(zip(small, held, strict=True)):
+        first.append(pltpu.make_async_copy(ref, copied, sems.at[count + i]))
+        first[-1].start()
+    gains, (lengths, tokens) = held[:3], held[3:]
     copies = []
     at = 0
     for i, ref in enumerate(weights):
@@ -81,6 +86,8 @@
         copies.append(pltpu.make_async_copy(ref, out.at[pl.ds(at, rows)], sems.at[i]))
         copies[-1].start()
         at += rows
+    for copy in first:
+        copy.wait()
     pieces = []
     for ref in gains:
         value = ref[...]
@@ -108,23 +115,30 @@
         (packed, packed),
         (tokens.shape[0], packed),
     )
-    vmem = pl.BlockSpec(memory_space=pltpu.VMEM)
+    small = (*[gain[None, :] for gain in gains], lengths[None, :], tokens)
+    count = len(weights) + len(small)
     return pl.pallas_call(
         functools.partial(front_kernel, len(weights)),
-        in_specs=[pl.BlockSpec(memory_space=pl.ANY)] * len(weights)
-        + [vmem] * (len(gains) + 2),
-        out_specs=[vmem] * len(shapes),
+        in_specs=[pl.BlockSpec(memory_space=pl.ANY)] * count,
+        out_specs=[pl.BlockSpec(memory_space=pltpu.VMEM)] * len(shapes),
         out_shape=[pltpu.VMEM(shape, bf16) for shape in shapes],
-        scratch_shapes=[pltpu.SemaphoreType.DMA((len(weights),))],
-    )(*weights, *[gain[None, :] for gain in gains], lengths[None, :], tokens)
+        scratch_shapes=[
+            pltpu.SemaphoreType.DMA((count,)),
+            *[pltpu.VMEM(value.shape, value.dtype) for value in small],
+        ],
+    )(*weights, *small)
 
 
 def recur_kernel(sums, lengths, floors, head_gain, states, heads, new_states):
     total = jnp.sum(sums[...].astype(f32), axis=0)
+    at = 4 * DK
+    stats = total[:, 2 * at :]
+    squares = jnp.concatenate(
+        [stats[:, 0:1] + stats[:, 1:2], stats[:, 2:3] + stats[:, 3:4]], axis=0
+    )
+    total = jnp.concatenate([total[:, :at], total[:, at : 2 * at]], axis=0)
     slots = total.shape[0]
-    at = 4 * DK
-    squares = total[:, at : at + 1] + total[:, at + 1 : at + 2]
-    total = total[:, :at] * lax.rsqrt(squares / D + EPSILON)
+    total = total * lax.rsqrt(squares / D + EPSILON)
     queries = total[:, :DK]
     queries = queries * jax.nn.sigmoid(queries)
     fresh = total[:, 2 * DK : 3 * DK]
@@ -160,7 +174,7 @@
         recur_kernel,
         in_specs=[vmem] * 5,
         out_specs=[vmem, vmem],
-        out_shape=[pltpu.VMEM((sums.shape[1], DK), bf16), pltpu.VMEM(states.shape, f32)],
+        out_shape=[pltpu.VMEM((2 * sums.shape[1], DK), bf16), pltpu.VMEM(states.shape, f32)],
         compiler_params=SMALL,
     )(*[in_vmem(value) for value in (sums, lengths, floors, head_gain, states)])
 
@@ -170,14 +184,14 @@
     return jnp.sum(bundle[at : at + 3, :].astype(f32), axis=0, keepdims=True)
 
 
-def stats_of(own, other):
+def stats_of(own, other, at):
     total = jnp.sum(own * own + other * other, axis=1, keepdims=True)
     upper = total.astype(bf16).astype(f32)
     lanes = iota((1, LANES), 1)
-    return jnp.where(lanes == 0, upper, jnp.where(lanes == 1, total - upper, 0.0)).astype(bf16)
-
-
-def products(sent, own, other, gains, weights, product, exact):
+    return jnp.where(lanes == at, upper, jnp.where(lanes == at + 1, total - upper, 0.0))
+
+
+def products(own, other, gains, weights, product, exact):
     parts = []
     for rows, gain in zip((own, other), gains, strict=True):
         wide = rows * gain
@@ -187,14 +201,34 @@
             whole = jnp.concatenate([whole, rest], axis=0)
         parts.append(whole)
     count = own.shape[0]
-    at = 0
+    results = []
     for ours, theirs in weights:
         both = product(parts[0], ours) + product(parts[1], theirs)
         if exact:
             both = both[:count] + both[count:]
-        sent[:, at : at + both.shape[1]] = both.astype(bf16)
-        at += both.shape[1]
-    sent[:, at:] = stats_of(own, other)
+        results.append(both)
+    return results
+
+
+def put_rows(sent, results, stats):
+    at = 0
+    for result in (*results, stats):
+        sent[:, at : at + result.shape[1]] = result.astype(bf16)
+        at += result.shape[1]
+
+
+def put_slots(sent, results, stats):
+    groups = sent.shape[0]
+    width = sum(result.shape[1] for result in results)
+    at = 0
+    for result in results:
+        cols = result.shape[1]
+        slots = result.reshape(groups, 2 * W, cols)
+        sent[:, :, at : at + cols] = slots[:, :W].astype(bf16)
+        sent[:, :, width + at : width + at + cols] = slots[:, W:].astype(bf16)
+        at += cols
+    low, high = [value.reshape(groups, 2 * W, LANES) for value in stats]
+    sent[:, :, 2 * width :] = (low[:, :W] + high[:, W:]).astype(bf16)
 
 
 def halves_of(weights, bundle, at):
@@ -215,7 +249,8 @@
     resid[:, cols:] = other.astype(bf16)
     weights = halves_of((gate, up), bundle, 0)
     gains = (gain[...], gain_rows(bundle, 0))
-    products(sent, own, other, gains, weights, matmul_t, True)
+    results = products(own, other, gains, weights, matmul_t, True)
+    put_rows(sent, results, stats_of(own, other, 0))
 
 
 def mix_kernel(spread, resid, swapped, gain, query, forget, value, outgate, bundle, at, sent):
@@ -224,7 +259,9 @@
     rows = matmul(spread[...], rows)
     weights = halves_of((query, forget, value, outgate), bundle, at)
     gains = (gain[...], gain_rows(bundle, 1))
-    products(sent, rows[:, :cols], rows[:, cols:], gains, weights, matmul, True)
+    own, other = rows[:, :cols], rows[:, cols:]
+    results = products(own, other, gains, weights, matmul, True)
+    put_slots(sent, results, (stats_of(own, other, 0), stats_of(own, other, 2)))
 
 
 def post_kernel(received, before, gain, gate, up, bundle, at, sent, resid):
@@ -235,7 +272,9 @@
     rows = rows.astype(f32)
     weights = halves_of((gate, up), bundle, at)
     gains = (gain[...], gain_rows(bundle, 2))
-    products(sent, rows[:, :cols], rows[:, cols:], gains, weights, matmul_t, False)
+    own, other = rows[:, :cols], rows[:, cols:]
+    results = products(own, other, gains, weights, matmul_t, False)
+    put_rows(sent, results, stats_of(own, other, 0))
 
 
 def put_partials(rows, weight, other, out):
@@ -282,6 +321,29 @@
     leads = lax.axis_index("c") == 0
     out[:cols, :] = jnp.where(leads, own, other)
     out[cols:, :] = jnp.where(leads, other, own)
+
+
+def last_kernel(received, table, out):
+    groups, size = received.shape
+    half = table.shape[0] // 2
+    low = jnp.sum(received[: groups // 2, :], axis=0, keepdims=True)
+    high = jnp.sum(received[groups // 2 :, :], axis=0, keepdims=True)
+    rows = [
+        jnp.concatenate([low[:, at : at + half], high[:, at : at + half]], axis=1)
+        for at in range(0, size, half)
+    ]
+    out[...] = matmul(jnp.concatenate(rows, axis=0).astype(bf16), table[...]).astype(bf16)
+
+
+def last_spread(received, table, cols):
+    vmem = pl.BlockSpec(memory_space=pltpu.VMEM)
+    return pl.pallas_call(
+        last_kernel,
+        in_specs=[vmem, vmem],
+        out_specs=vmem,
+        out_shape=jax.ShapeDtypeStruct((cols, table.shape[1]), bf16),
+        compiler_params=SMALL,
+    )(in_vmem(received), in_vmem(table))
 
 
 def in_kernel(kernel, shapes, *values, dtype=bf16):
@@ -399,7 +461,7 @@
     swapped = lax.ppermute(turned, "c", swap)
     (sent,) = in_kernel(
         lambda *refs: mix_kernel(*refs[:-1], starts[4], refs[-1]),
-        ((packed, 4 * head_cols + LANES),),
+        ((z_count, W, 8 * head_cols + LANES),),
         side["spread"],
         resid,
         swapped,
@@ -407,7 +469,6 @@
         *mine[4:8],
         side["bundle"],
     )
-    sent = sent.reshape(z_count, seq_local * W, 4 * head_cols + LANES)
     side["recur"] = (lengths[None, :], forget_floor[None, :], head_gain[None, :])
     side["states"] = states.reshape(seq_local * heads_local, DK, DK)
     received = exchanged(sent, "z")
@@ -444,10 +505,7 @@
     )
     piece = own_cols // tp_count
     finish = finish.reshape(2 * tp_count, piece * half)
-    finished = jnp.sum(exchanged(finish, ("c", "tp")).reshape(2, tp_count, -1), axis=1)
-    finished = finished.reshape(2, piece, half)
-    finished = jnp.concatenate([finished[0], finished[1]], axis=1).astype(bf16)
-    outcome = matmul(finished, side["table"]).astype(bf16).T
+    outcome = last_spread(exchanged(finish, ("c", "tp")), side["table"], piece).T
     return (outcome, new_states.reshape(states.shape))
 
 

time: 194 us -> 193 us (level)
  no operation moved by 1% of the time
where the time goes in v6:
time: 193 us; the launch traced here: 192 us
  blocking collectives  168 us (87%)
  starting transfers between devices  14.8 us (8%)
  Pallas kernels  6.14 us (3%)
    all_to_all x10, blocking collectives, exchanged(): value = lax.all_to_all(value, axis, split_axis=0, concat_axis=0, tiled=True)  168 us
    ppermute x1, starting transfers between devices, local(): bundle = lax.ppermute(packed_own, 'c', swap)  8.75 us
    ppermute x1, starting transfers between devices, local(): swapped = lax.ppermute(turned, 'c', swap)  6.09 us
  transfers between devices with their start and end apart: 2, of which 1 were waited for; matrix products, arithmetic and copies ran while one was open for 0% of the time, Pallas kernels for 0%

profile of v6, /device:TPU:1, one launch (start us, length us, event | category | flops | bytes accessed | tf_op | source)
XLA Modules:
  0.0 192.1 jit_solution(10313374401785906751)
XLA Ops:
  0.6 0.0 copy-start.1
  0.6 0.0 copy-start
  0.7 0.0 copy-start.12
  0.7 1.6 shard_map.194
  2.3 8.7 %collective-permute-start = (bf16[4880,128]{1,0:T(8,128)(2,1)S(1)}, bf16[4880,128]{1,0:T(8,128)(2,1)S(1)}, u32[]{:S(2)}, u32[]{:S(2)}) collective-permute-start(bf16[4880,128]{1,0:T(8,128)(2,1)S(1)} %get-tuple-element.126), channel_id=1, source_target_pairs={{0,16},{16,0},{1,17},{17,1},{2,18},{18,2},{3,19},{19,3},{4,20},{20... | collective-permute-start | bytes 3747848 | tf_op jit(solution)/shard_map/ppermute | solution.py:411
  11.1 0.1 slice_bitcast_fusion.1
  11.1 0.1 reshape.49
  11.3 9.7 %all_to_all.57 = bf16[32,2,256]{2,1,0:T(2,128)(2,1)S(1)} all-to-all(bf16[32,2,256]{2,1,0:T(2,128)(2,1)S(1)} %reshape.49), channel_id=1, replica_groups=mesh['z'=16,'c'=2,'tp'=16] {'c','tp'}, dimensions={0} | all-to-all | bytes 65536 | tf_op jit(solution)/shard_map/all_to_all | solution.py:398
  21.0 0.1 reshape.50
  21.1 0.0 collective-permute-done.bundle.refs_2_.refs_8_.refs_4_.refs_5_.refs_3_
  21.1 0.0 copy-done.1
  21.1 0.0 copy-done
  21.1 0.0 copy-done.12
  21.1 0.0 copy-start.5
  21.1 0.6 shard_map.195
  21.7 0.1 reshape.39
  21.8 26.2 %all_to_all.58 = bf16[16,4,1536]{2,1,0:T(4,128)(2,1)S(1)} all-to-all(bf16[16,4,1536]{2,1,0:T(4,128)(2,1)S(1)} %reshape.39), channel_id=1, replica_groups=mesh['z'=16,'c'=2,'tp'=16] {'z'}, dimensions={0} | all-to-all | bytes 393216 | tf_op jit(solution)/shard_map/all_to_all | solution.py:398
  47.9 0.1 convert_reduce_fusion.2
  48.0 0.2 fusion.11
  48.2 0.1 fusion.3
  48.3 20.5 %all_to_all.59 = bf16[16,4,704]{2,1,0:T(4,128)(2,1)S(1)} all-to-all(bf16[16,4,704]{2,1,0:T(4,128)(2,1)S(1)} %broadcast_in_dim.42), channel_id=1, replica_groups=mesh['z'=16,'c'=2,'tp'=16] {'z'}, dimensions={0} | all-to-all | bytes 180224 | tf_op jit(solution)/shard_map/all_to_all | solution.py:398
  68.9 0.0 copy-done.5
  68.9 0.3 shard_map.196
  69.2 0.0 copy-start.6
  69.2 0.0 copy-start.7
  69.2 0.0 copy-start.8
  69.2 0.0 copy-start.9
  69.2 0.0 copy-start.13
  69.3 12.1 %all_to_all.60 = bf16[16,64,256]{2,1,0:T(8,128)(2,1)S(1)} all-to-all(bf16[16,64,256]{2,1,0:T(8,128)(2,1)S(1)} %shard_map.196), channel_id=1, replica_groups=mesh['z'=16,'c'=2,'tp'=16] {'tp'}, dimensions={0} | all-to-all | bytes 1048576 | tf_op jit(solution)/shard_map/all_to_all | solution.py:398
  81.3 0.1 convert_reduce_fusion
  81.5 0.0 copy-start.10
  81.5 6.1 %collective-permute-start.1 = (bf16[64,256]{1,0:T(8,128)(2,1)S(1)}, bf16[64,256]{1,0:T(8,128)(2,1)S(1)}, u32[]{:S(2)}, u32[]{:S(2)}) collective-permute-start(bf16[64,256]{1,0:T(8,128)(2,1)S(1)} %pad_maximum_fusion), channel_id=1, source_target_pairs={{0,16},{16,0},{1,17},{17,1},{2,18},{18,2},{3,19},{19,3},{4,20},{20... | collective-permute-start | bytes 98312 | tf_op jit(solution)/shard_map/ppermute | solution.py:461
  87.6 0.8 collective-permute-done.1.refs_2_
  88.4 0.0 copy-done.6
  88.4 0.0 copy-done.7
  88.4 0.0 copy-done.8
  88.4 0.0 copy-done.9
  88.4 0.0 copy-done.13
  88.5 0.4 shard_map.197
  88.9 16.2 %all_to_all.61.sums = bf16[16,4,1152]{2,1,0:T(4,128)(2,1)S(1)} all-to-all(bf16[16,4,1152]{2,1,0:T(4,128)(2,1)S(1)} %shard_map.197), channel_id=1, replica_groups=mesh['z'=16,'c'=2,'tp'=16] {'z'}, dimensions={0} | all-to-all | bytes 294912 | tf_op jit(solution)/shard_map/all_to_all | solution.py:398
  105.0 0.0 copy-done.11
  105.1 0.0 copy-done.14
  105.1 0.0 copy-done.16
  105.1 0.0 copy-done.17
  105.1 1.0 shard_map.198
  106.1 20.8 %all_to_all.62 = bf16[32,8,128]{2,1,0:T(8,128)(2,1)S(1)} all-to-all(bf16[32,8,128]{2,1,0:T(8,128)(2,1)S(1)} %broadcast_in_dim.45), channel_id=1, replica_groups=mesh['z'=16,'c'=2,'tp'=16] {'z','c'}, dimensions={0} | all-to-all | bytes 131072 | tf_op jit(solution)/shard_map/all_to_all | solution.py:398
  126.9 0.0 copy-done.10
  126.9 0.7 shard_map.199
  127.6 12.6 %all_to_all.63.refs_0_ = bf16[16,64,256]{2,1,0:T(8,128)(2,1)S(1)} all-to-all(bf16[16,64,256]{2,1,0:T(8,128)(2,1)S(1)} %get-tuple-element.201), channel_id=1, replica_groups=mesh['z'=16,'c'=2,'tp'=16] {'tp'}, dimensions={0} | all-to-all | bytes 1048576 | tf_op jit(solution)/shard_map/all_to_all | solution.py:398
  140.2 0.0 copy-done.3
  140.2 0.0 copy-done.4
  140.2 0.5 shard_map.200
  140.8 0.0 copy-start.2
  140.8 0.1 reshape.43
  140.8 15.8 %all_to_all.64 = bf16[16,4,1536]{2,1,0:T(4,128)(2,1)S(1)} all-to-all(bf16[16,4,1536]{2,1,0:T(4,128)(2,1)S(1)} %reshape.43), channel_id=1, replica_groups=mesh['z'=16,'c'=2,'tp'=16] {'z'}, dimensions={0} | all-to-all | bytes 393216 | tf_op jit(solution)/shard_map/all_to_all | solution.py:398
  156.6 0.1 convert_reduce_fusion.1
  156.7 0.2 fusion.7
  156.9 0.1 fusion.2
  157.0 19.6 %all_to_all.65 = bf16[16,4,704]{2,1,0:T(4,128)(2,1)S(1)} all-to-all(bf16[16,4,704]{2,1,0:T(4,128)(2,1)S(1)} %broadcast_in_dim.46), channel_id=1, replica_groups=mesh['z'=16,'c'=2,'tp'=16] {'z'}, dimensions={0} | all-to-all | bytes 180224 | tf_op jit(solution)/shard_map/all_to_all | solution.py:398
  176.6 0.3 shard_map.201
  176.9 0.1 reshape.45
  177.0 0.1 copy.29
  177.1 14.2 %all_to_all.66 = f32[32,1,512]{2,1,0:T(1,128)S(1)} all-to-all(f32[32,1,512]{2,1,0:T(1,128)S(1)} %copy.29), channel_id=1, replica_groups=mesh['z'=16,'c'=2,'tp'=16] {'c','tp'}, dimensions={0} | all-to-all | bytes 131072 | tf_op jit(solution)/shard_map/all_to_all | solution.py:398
  191.4 0.8 shard_map.202
  (20 shorter events, 0.2 us)
Async XLA Ops:
  0.6 20.5 %copy-start.1 = (bf16[128,704]{0,1:T(8,128)(2,1)S(1)}, bf16[128,704]{0,1:T(8,128)(2,1)}, u32[]{:S(2)}) copy-start(bf16[128,704]{0,1:T(8,128)(2,1)} %param.24) | copy-start | bytes 540676
  0.6 20.5 %copy-start = (bf16[128,704]{0,1:T(8,128)(2,1)S(1)}, bf16[128,704]{0,1:T(8,128)(2,1)}, u32[]{:S(2)}) copy-start(bf16[128,704]{0,1:T(8,128)(2,1)} %param.23) | copy-start | bytes 540676
  0.7 20.5 %copy-start.12 = (f32[128]{0:T(128)S(1)}, f32[128]{0:T(128)}, u32[]{:S(2)}) copy-start(f32[128]{0:T(128)} %param.22) | copy-start | bytes 1540
  2.3 18.8 %collective-permute-start = (bf16[4880,128]{1,0:T(8,128)(2,1)S(1)}, bf16[4880,128]{1,0:T(8,128)(2,1)S(1)}, u32[]{:S(2)}, u32[]{:S(2)}) collective-permute-start(bf16[4880,128]{1,0:T(8,128)(2,1)S(1)} %get-tuple-element.126), channel_id=1, source_target_pairs={{0,16},{16,0},{1,17},{17,1},{2,18},{18,2},{3,19},{19,3},{4,20},{20... | collective-permute-start | bytes 3747848 | tf_op jit(solution)/shard_map/ppermute | solution.py:411
  21.1 47.8 %copy-start.5 = (bf16[704,128]{1,0:T(8,128)(2,1)S(1)}, bf16[704,128]{1,0:T(8,128)(2,1)}, u32[]{:S(2)}) copy-start(bf16[704,128]{1,0:T(8,128)(2,1)} %refs_1_.1) | copy-start | bytes 540676
  69.2 19.2 %copy-start.6 = (bf16[128,128]{1,0:T(8,128)(2,1)S(1)}, bf16[128,128]{1,0:T(8,128)(2,1)}, u32[]{:S(2)}) copy-start(bf16[128,128]{1,0:T(8,128)(2,1)} %refs_4_.3) | copy-start | bytes 98308
  69.2 19.2 %copy-start.7 = (bf16[128,128]{1,0:T(8,128)(2,1)S(1)}, bf16[128,128]{1,0:T(8,128)(2,1)}, u32[]{:S(2)}) copy-start(bf16[128,128]{1,0:T(8,128)(2,1)} %refs_5_.3) | copy-start | bytes 98308
  69.2 19.2 %copy-start.8 = (bf16[128,128]{1,0:T(8,128)(2,1)S(1)}, bf16[128,128]{1,0:T(8,128)(2,1)}, u32[]{:S(2)}) copy-start(bf16[128,128]{1,0:T(8,128)(2,1)} %refs_6_.3) | copy-start | bytes 98308
  69.2 19.2 %copy-start.9 = (bf16[128,128]{1,0:T(8,128)(2,1)S(1)}, bf16[128,128]{1,0:T(8,128)(2,1)}, u32[]{:S(2)}) copy-start(bf16[128,128]{1,0:T(8,128)(2,1)} %refs_7_.3) | copy-start | bytes 98308
  69.2 19.2 %copy-start.13 = (f32[128]{0:T(128)S(1)}, f32[128]{0:T(128)}, u32[]{:S(2)}) copy-start(f32[128]{0:T(128)} %param.26) | copy-start | bytes 1540
  81.3 23.7 %copy-start.11 = (f32[2,1,128,128]{3,2,1,0:T(8,128)S(1)}, f32[2,1,128,128]{3,2,1,0:T(8,128)}, u32[]{:S(2)}) copy-start(f32[2,1,128,128]{3,2,1,0:T(8,128)} %param.21) | copy-start | bytes 393220
  81.3 23.7 %copy-start.14 = (s32[64]{0:T(128)S(1)}, s32[64]{0:T(128)}, u32[]{:S(2)}) copy-start(s32[64]{0:T(128)} %param.20) | copy-start | bytes 772
  81.3 23.7 %copy-start.16 = (f32[128]{0:T(128)S(1)}, f32[128]{0:T(128)}, u32[]{:S(2)}) copy-start(f32[128]{0:T(128)} %param.31) | copy-start | bytes 1540
  81.3 23.7 %copy-start.17 = (f32[128]{0:T(128)S(1)}, f32[128]{0:T(128)}, u32[]{:S(2)}) copy-start(f32[128]{0:T(128)} %param.32) | copy-start | bytes 1540
  81.5 45.5 %copy-start.10 = (bf16[128,128]{1,0:T(8,128)(2,1)S(1)}, bf16[128,128]{1,0:T(8,128)(2,1)}, u32[]{:S(2)}) copy-start(bf16[128,128]{1,0:T(8,128)(2,1)} %refs_2_.2) | copy-start | bytes 98308
  81.5 6.9 %collective-permute-start.1 = (bf16[64,256]{1,0:T(8,128)(2,1)S(1)}, bf16[64,256]{1,0:T(8,128)(2,1)S(1)}, u32[]{:S(2)}, u32[]{:S(2)}) collective-permute-start(bf16[64,256]{1,0:T(8,128)(2,1)S(1)} %pad_maximum_fusion), channel_id=1, source_target_pairs={{0,16},{16,0},{1,17},{17,1},{2,18},{18,2},{3,19},{19,3},{4,20},{20... | collective-permute-start | bytes 98312 | tf_op jit(solution)/shard_map/ppermute | solution.py:461
  126.9 13.3 %copy-start.3 = (bf16[128,704]{0,1:T(8,128)(2,1)S(1)}, bf16[128,704]{0,1:T(8,128)(2,1)}, u32[]{:S(2)}) copy-start(bf16[128,704]{0,1:T(8,128)(2,1)} %param.35) | copy-start | bytes 540676
  126.9 13.3 %copy-start.4 = (bf16[128,704]{0,1:T(8,128)(2,1)S(1)}, bf16[128,704]{0,1:T(8,128)(2,1)}, u32[]{:S(2)}) copy-start(bf16[128,704]{0,1:T(8,128)(2,1)} %param.36) | copy-start | bytes 540676
  126.9 13.3 %copy-start.15 = (f32[128]{0:T(128)S(1)}, f32[128]{0:T(128)}, u32[]{:S(2)}) copy-start(f32[128]{0:T(128)} %param.34) | copy-start | bytes 1540
  140.8 35.9 %copy-start.2 = (bf16[704,128]{1,0:T(8,128)(2,1)S(1)}, bf16[704,128]{1,0:T(8,128)(2,1)}, u32[]{:S(2)}) copy-start(bf16[704,128]{1,0:T(8,128)(2,1)} %refs_2_.3) | copy-start | bytes 540676

commit v7 on v6

--- a/solution.py
+++ b/solution.py
@@ -60,7 +60,14 @@
     targets = jnp.where(within < own, before + within, -1.0)
     row_ids = ((iota((1, packed), 1) + core * half) % packed).astype(f32)
     spread = (targets == row_ids).astype(f32).astype(bf16)
-    entry = matmul_t(tokens, table).astype(bf16)
+    entry = matmul_t(tokens, table)
+    cols = entry.shape[0] // 2
+    entry = jnp.stack(
+        [
+            jnp.concatenate([entry[:cols, at : at + half], entry[cols:, at : at + half]], axis=1)
+            for at in (0, half)
+        ]
+    ).astype(bf16)
     return table, my_table, spread, entry
 
 
@@ -113,7 +120,7 @@
         (packed, slots),
         (packed // 2, slots),
         (packed, packed),
-        (tokens.shape[0], packed),
+        (2, tokens.shape[0] // 2, packed),
     )
     small = (*[gain[None, :] for gain in gains], lengths[None, :], tokens)
     count = len(weights) + len(small)
@@ -242,7 +249,14 @@
 def entry_kernel(gathered, gain, gate, up, bundle, sent, resid):
     cols = gain.shape[1]
     first = lax.axis_index("c") == 0
-    low, high = gathered[:cols, :].astype(f32), gathered[cols:, :].astype(f32)
+    groups = gathered.shape[0] // 2
+    halves = []
+    for at in (0, groups):
+        pairs = gathered[at : at + groups].astype(f32)
+        rows = pairs.shape[2] // 2
+        pairs = jnp.concatenate([pairs[:, :, :rows], pairs[:, :, rows:]], axis=1)
+        halves.append(pairs.reshape(cols, rows))
+    low, high = halves
     own = jnp.where(first, low, high).T
     other = jnp.where(first, high, low).T
     resid[:, :cols] = own.astype(bf16)
@@ -286,6 +300,19 @@
         out[i, :, cols:] = other
 
 
+def hidden_kernel(received, out):
+    total = jnp.sum(received[...].astype(f32), axis=0)
+    hidden = out.shape[2]
+    at = 2 * hidden
+    squares = total[:, at : at + 1] + total[:, at + 1 : at + 2]
+    scale = lax.rsqrt(squares / D + EPSILON)
+    gate = total[:, :hidden] * scale
+    up = total[:, hidden:at] * scale
+    act = (gate * jax.nn.sigmoid(gate) * up).astype(bf16)
+    for i in range(out.shape[0]):
+        out[i] = act
+
+
 def down_kernel(rows, weight, bundle, at, out):
     put_partials(rows[...], weight, bundle[at : at + weight.shape[0], :], out)
 
@@ -311,6 +338,14 @@
     )(*values)
 
 
+def put_pairs(out, at, cols, groups):
+    count, rows = cols.shape
+    pairs = cols.reshape(groups, count // groups, rows)
+    half = count // groups // 2
+    paired = jnp.concatenate([pairs[:, :half], pairs[:, half:]], axis=2)
+    out[at : at + groups] = paired.astype(out.dtype)
+
+
 def finish_kernel(rows, resid, weight, bundle, at, out):
     cols = weight.shape[1]
     first = (lax.axis_index("tp") == 0).astype(f32)
@@ -319,18 +354,19 @@
     other = 0.5 * other + first * resid[:, cols:].astype(f32)
     own, other = own.T, other.T
     leads = lax.axis_index("c") == 0
-    out[:cols, :] = jnp.where(leads, own, other)
-    out[cols:, :] = jnp.where(leads, other, own)
+    groups = out.shape[0] // 2
+    put_pairs(out, 0, jnp.where(leads, own, other), groups)
+    put_pairs(out, groups, jnp.where(leads, other, own), groups)
 
 
 def last_kernel(received, table, out):
-    groups, size = received.shape
+    groups = received.shape[0] // 2
     half = table.shape[0] // 2
-    low = jnp.sum(received[: groups // 2, :], axis=0, keepdims=True)
-    high = jnp.sum(received[groups // 2 :, :], axis=0, keepdims=True)
+    low = jnp.sum(received[:groups], axis=0)
+    high = jnp.sum(received[groups:], axis=0)
     rows = [
         jnp.concatenate([low[:, at : at + half], high[:, at : at + half]], axis=1)
-        for at in range(0, size, half)
+        for at in (0, half)
     ]
     out[...] = matmul(jnp.concatenate(rows, axis=0).astype(bf16), table[...]).astype(bf16)
 
@@ -414,9 +450,8 @@
     side["my_table"] = my_table
     side["spread"] = spread
 
-    pieces = jnp.stack([entry[:, :half], entry[:, half:]])
-    pieces = jnp.broadcast_to(pieces[:, None], (2, tp_count, *pieces.shape[1:]))
-    gathered = exchanged(pieces.reshape(2 * tp_count, *pieces.shape[2:]), ("c", "tp"))
+    pieces = jnp.broadcast_to(entry[:, None], (2, tp_count, *entry.shape[1:]))
+    gathered = exchanged(pieces.reshape(2 * tp_count, *entry.shape[1:]), ("c", "tp"))
     starts = [0]
     for weight in mine:
         starts.append(starts[-1] + weight.shape[0])
@@ -427,7 +462,7 @@
     sent, side["resid"] = in_kernel(
         entry_kernel,
         (sent_shape, resid_shape),
-        gathered.reshape(2 * own_cols, half),
+        gathered,
         gain_pre[None, :],
         mine[0],
         mine[1],
@@ -436,13 +471,10 @@
 
     def ff_hidden(sent):
         sent = sent.reshape(z_count, per_z, ff_cols + LANES)
-        owned = jnp.sum(exchanged(sent, "z").astype(f32), axis=0)
-        total = owned[:, ff_cols : ff_cols + 1] + owned[:, ff_cols + 1 : ff_cols + 2]
-        scale = lax.rsqrt(total / D + EPSILON)
-        gate = owned[:, :hidden] * scale
-        up = owned[:, hidden:ff_cols] * scale
-        act = (jax.nn.silu(gate) * up).astype(bf16)
-        return sent_to_all(act, "z").reshape(half, hidden)
+        (acts,) = in_kernel(
+            hidden_kernel, ((z_count, per_z, hidden),), exchanged(sent, "z")
+        )
+        return exchanged(acts, "z").reshape(half, hidden)
 
     partial_shape = (tp_count, *resid_shape)
     act = ff_hidden(sent)
@@ -496,7 +528,7 @@
     act = ff_hidden(sent)
     (finish,) = in_kernel(
         lambda *refs: finish_kernel(*refs[:-1], starts[10], refs[-1]),
-        ((2 * own_cols, half),),
+        ((2 * tp_count, own_cols // tp_count // 2, 2 * half),),
         act,
         side["resid"],
         post_down,
@@ -504,7 +536,6 @@
         dtype=f32,
     )
     piece = own_cols // tp_count
-    finish = finish.reshape(2 * tp_count, piece * half)
     outcome = last_spread(exchanged(finish, ("c", "tp")), side["table"], piece).T
     return (outcome, new_states.reshape(states.shape))
 

time: 193 us -> 192 us (level)
  no operation moved by 1% of the time
where the time goes in v7:
time: 192 us; the launch traced here: 191 us
  blocking collectives  168 us (88%)
  starting transfers between devices  14.8 us (8%)
  Pallas kernels  6.77 us (4%)
    all_to_all x10, blocking collectives, exchanged(): value = lax.all_to_all(value, axis, split_axis=0, concat_axis=0, tiled=True)  168 us
    ppermute x1, starting transfers between devices, local(): bundle = lax.ppermute(packed_own, 'c', swap)  8.75 us
    ppermute x1, starting transfers between devices, local(): swapped = lax.ppermute(turned, 'c', swap)  6.09 us
  transfers between devices with their start and end apart: 2, of which 1 were waited for; matrix products, arithmetic and copies ran while one was open for 0% of the time, Pallas kernels for 0%

profile of v7, /device:TPU:1, one launch (start us, length us, event | category | flops | bytes accessed | tf_op | source)
XLA Modules:
  0.0 191.4 jit_solution(9530022516118709933)
XLA Ops:
  0.6 0.0 copy-start.1
  0.6 0.0 copy-start
  0.7 0.0 copy-start.12
  0.7 1.6 shard_map.194
  2.3 8.7 %collective-permute-start = (bf16[4880,128]{1,0:T(8,128)(2,1)S(1)}, bf16[4880,128]{1,0:T(8,128)(2,1)S(1)}, u32[]{:S(2)}, u32[]{:S(2)}) collective-permute-start(bf16[4880,128]{1,0:T(8,128)(2,1)S(1)} %get-tuple-element.126), channel_id=1, source_target_pairs={{0,16},{16,0},{1,17},{17,1},{2,18},{18,2},{3,19},{19,3},{4,20},{20... | collective-permute-start | bytes 3747848 | tf_op jit(solution)/shard_map/ppermute | solution.py:447
  11.1 9.7 %all_to_all.50.gathered = bf16[32,4,128]{2,1,0:T(4,128)(2,1)S(1)} all-to-all(bf16[32,4,128]{2,1,0:T(4,128)(2,1)S(1)} %bitcast.38), channel_id=1, replica_groups=mesh['z'=16,'c'=2,'tp'=16] {'c','tp'}, dimensions={0} | all-to-all | bytes 65536 | tf_op jit(solution)/shard_map/all_to_all | solution.py:434
  20.8 0.0 copy-start.5
  20.8 0.0 collective-permute-done.bundle.refs_2_.refs_8_.refs_4_.refs_5_.refs_3_
  20.8 0.0 copy-done.1
  20.8 0.0 copy-done
  20.8 0.0 copy-done.12
  20.8 0.6 shard_map.195
  21.4 0.1 reshape.30
  21.5 26.2 %all_to_all.51.received = bf16[16,4,1536]{2,1,0:T(4,128)(2,1)S(1)} all-to-all(bf16[16,4,1536]{2,1,0:T(4,128)(2,1)S(1)} %reshape.30), channel_id=1, replica_groups=mesh['z'=16,'c'=2,'tp'=16] {'z'}, dimensions={0} | all-to-all | bytes 393216 | tf_op jit(solution)/shard_map/all_to_all | solution.py:434
  47.6 0.2 shard_map.196
  47.9 20.5 %all_to_all.52 = bf16[16,4,704]{2,1,0:T(4,128)(2,1)S(1)} all-to-all(bf16[16,4,704]{2,1,0:T(4,128)(2,1)S(1)} %shard_map.196), channel_id=1, replica_groups=mesh['z'=16,'c'=2,'tp'=16] {'z'}, dimensions={0} | all-to-all | bytes 180224 | tf_op jit(solution)/shard_map/all_to_all | solution.py:434
  68.5 0.0 copy-done.5
  68.5 0.3 shard_map.197
  68.8 0.0 copy-start.6
  68.8 0.0 copy-start.7
  68.8 0.0 copy-start.8
  68.8 0.0 copy-start.9
  68.8 0.0 copy-start.13
  68.8 12.1 %all_to_all.53 = bf16[16,64,256]{2,1,0:T(8,128)(2,1)S(1)} all-to-all(bf16[16,64,256]{2,1,0:T(8,128)(2,1)S(1)} %shard_map.197), channel_id=1, replica_groups=mesh['z'=16,'c'=2,'tp'=16] {'tp'}, dimensions={0} | all-to-all | bytes 1048576 | tf_op jit(solution)/shard_map/all_to_all | solution.py:434
  80.9 0.0 copy-start.11
  80.9 0.0 copy-start.14
  80.9 0.0 copy-start.16
  80.9 0.0 copy-start.17
  80.9 0.1 convert_reduce_fusion
  81.0 0.0 copy-start.10
  81.1 6.1 %collective-permute-start.1 = (bf16[64,256]{1,0:T(8,128)(2,1)S(1)}, bf16[64,256]{1,0:T(8,128)(2,1)S(1)}, u32[]{:S(2)}, u32[]{:S(2)}) collective-permute-start(bf16[64,256]{1,0:T(8,128)(2,1)S(1)} %pad_maximum_fusion), channel_id=1, source_target_pairs={{0,16},{16,0},{1,17},{17,1},{2,18},{18,2},{3,19},{19,3},{4,20},{20... | collective-permute-start | bytes 98312 | tf_op jit(solution)/shard_map/ppermute | solution.py:493
  87.1 0.8 collective-permute-done.1.refs_2_
  88.0 0.0 copy-done.6
  88.0 0.0 copy-done.7
  88.0 0.0 copy-done.8
  88.0 0.0 copy-done.9
  88.0 0.0 copy-done.13
  88.0 0.4 shard_map.198
  88.4 16.2 %all_to_all.54.sums = bf16[16,4,1152]{2,1,0:T(4,128)(2,1)S(1)} all-to-all(bf16[16,4,1152]{2,1,0:T(4,128)(2,1)S(1)} %shard_map.198), channel_id=1, replica_groups=mesh['z'=16,'c'=2,'tp'=16] {'z'}, dimensions={0} | all-to-all | bytes 294912 | tf_op jit(solution)/shard_map/all_to_all | solution.py:434
  104.6 0.0 copy-done.11
  104.6 0.0 copy-done.14
  104.6 0.0 copy-done.16
  104.6 0.0 copy-done.17
  104.6 1.0 shard_map.199
  105.6 20.8 %all_to_all.55 = bf16[32,8,128]{2,1,0:T(8,128)(2,1)S(1)} all-to-all(bf16[32,8,128]{2,1,0:T(8,128)(2,1)S(1)} %broadcast_in_dim.38), channel_id=1, replica_groups=mesh['z'=16,'c'=2,'tp'=16] {'z','c'}, dimensions={0} | all-to-all | bytes 131072 | tf_op jit(solution)/shard_map/all_to_all | solution.py:434
  126.5 0.0 copy-done.10
  126.5 0.0 copy-start.3
  126.5 0.0 copy-start.4
  126.5 0.0 copy-start.15
  126.5 0.7 shard_map.200
  127.2 12.6 %all_to_all.56.refs_0_ = bf16[16,64,256]{2,1,0:T(8,128)(2,1)S(1)} all-to-all(bf16[16,64,256]{2,1,0:T(8,128)(2,1)S(1)} %get-tuple-element.201), channel_id=1, replica_groups=mesh['z'=16,'c'=2,'tp'=16] {'tp'}, dimensions={0} | all-to-all | bytes 1048576 | tf_op jit(solution)/shard_map/all_to_all | solution.py:434
  139.8 0.0 copy-done.3
  139.8 0.0 copy-done.4
  139.8 0.0 copy-done.15
  139.8 0.5 shard_map.201
  140.3 0.0 copy-start.2
  140.3 0.1 reshape.34
  140.4 15.8 %all_to_all.57.received = bf16[16,4,1536]{2,1,0:T(4,128)(2,1)S(1)} all-to-all(bf16[16,4,1536]{2,1,0:T(4,128)(2,1)S(1)} %reshape.34), channel_id=1, replica_groups=mesh['z'=16,'c'=2,'tp'=16] {'z'}, dimensions={0} | all-to-all | bytes 393216 | tf_op jit(solution)/shard_map/all_to_all | solution.py:434
  156.2 0.2 shard_map.202
  156.4 19.6 %all_to_all.58 = bf16[16,4,704]{2,1,0:T(4,128)(2,1)S(1)} all-to-all(bf16[16,4,704]{2,1,0:T(4,128)(2,1)S(1)} %shard_map.202), channel_id=1, replica_groups=mesh['z'=16,'c'=2,'tp'=16] {'z'}, dimensions={0} | all-to-all | bytes 180224 | tf_op jit(solution)/shard_map/all_to_all | solution.py:434
  176.0 0.0 copy-done.2
  176.0 0.4 shard_map.203
  176.4 14.2 %all_to_all.59.received = f32[32,4,128]{2,1,0:T(4,128)S(1)} all-to-all(f32[32,4,128]{2,1,0:T(4,128)S(1)} %shard_map.203), channel_id=1, replica_groups=mesh['z'=16,'c'=2,'tp'=16] {'c','tp'}, dimensions={0} | all-to-all | bytes 131072 | tf_op jit(solution)/shard_map/all_to_all | solution.py:434
  190.6 0.8 shard_map.204
  (7 shorter events, 0.1 us)
Async XLA Ops:
  0.6 20.2 %copy-start.1 = (bf16[128,704]{0,1:T(8,128)(2,1)S(1)}, bf16[128,704]{0,1:T(8,128)(2,1)}, u32[]{:S(2)}) copy-start(bf16[128,704]{0,1:T(8,128)(2,1)} %param.24) | copy-start | bytes 540676
  0.6 20.1 %copy-start = (bf16[128,704]{0,1:T(8,128)(2,1)S(1)}, bf16[128,704]{0,1:T(8,128)(2,1)}, u32[]{:S(2)}) copy-start(bf16[128,704]{0,1:T(8,128)(2,1)} %param.23) | copy-start | bytes 540676
  0.7 20.1 %copy-start.12 = (f32[128]{0:T(128)S(1)}, f32[128]{0:T(128)}, u32[]{:S(2)}) copy-start(f32[128]{0:T(128)} %param.22) | copy-start | bytes 1540
  2.3 18.5 %collective-permute-start = (bf16[4880,128]{1,0:T(8,128)(2,1)S(1)}, bf16[4880,128]{1,0:T(8,128)(2,1)S(1)}, u32[]{:S(2)}, u32[]{:S(2)}) collective-permute-start(bf16[4880,128]{1,0:T(8,128)(2,1)S(1)} %get-tuple-element.126), channel_id=1, source_target_pairs={{0,16},{16,0},{1,17},{17,1},{2,18},{18,2},{3,19},{19,3},{4,20},{20... | collective-permute-start | bytes 3747848 | tf_op jit(solution)/shard_map/ppermute | solution.py:447
  20.8 47.7 %copy-start.5 = (bf16[704,128]{1,0:T(8,128)(2,1)S(1)}, bf16[704,128]{1,0:T(8,128)(2,1)}, u32[]{:S(2)}) copy-start(bf16[704,128]{1,0:T(8,128)(2,1)} %refs_1_.1) | copy-start | bytes 540676
  68.8 19.2 %copy-start.6 = (bf16[128,128]{1,0:T(8,128)(2,1)S(1)}, bf16[128,128]{1,0:T(8,128)(2,1)}, u32[]{:S(2)}) copy-start(bf16[128,128]{1,0:T(8,128)(2,1)} %refs_4_.3) | copy-start | bytes 98308
  68.8 19.2 %copy-start.7 = (bf16[128,128]{1,0:T(8,128)(2,1)S(1)}, bf16[128,128]{1,0:T(8,128)(2,1)}, u32[]{:S(2)}) copy-start(bf16[128,128]{1,0:T(8,128)(2,1)} %refs_5_.3) | copy-start | bytes 98308
  68.8 19.2 %copy-start.8 = (bf16[128,128]{1,0:T(8,128)(2,1)S(1)}, bf16[128,128]{1,0:T(8,128)(2,1)}, u32[]{:S(2)}) copy-start(bf16[128,128]{1,0:T(8,128)(2,1)} %refs_6_.3) | copy-start | bytes 98308
  68.8 19.2 %copy-start.9 = (bf16[128,128]{1,0:T(8,128)(2,1)S(1)}, bf16[128,128]{1,0:T(8,128)(2,1)}, u32[]{:S(2)}) copy-start(bf16[128,128]{1,0:T(8,128)(2,1)} %refs_7_.3) | copy-start | bytes 98308
  68.8 19.2 %copy-start.13 = (f32[128]{0:T(128)S(1)}, f32[128]{0:T(128)}, u32[]{:S(2)}) copy-start(f32[128]{0:T(128)} %param.26) | copy-start | bytes 1540
  80.9 23.7 %copy-start.11 = (f32[2,1,128,128]{3,2,1,0:T(8,128)S(1)}, f32[2,1,128,128]{3,2,1,0:T(8,128)}, u32[]{:S(2)}) copy-start(f32[2,1,128,128]{3,2,1,0:T(8,128)} %param.21) | copy-start | bytes 393220
  80.9 23.7 %copy-start.14 = (s32[64]{0:T(128)S(1)}, s32[64]{0:T(128)}, u32[]{:S(2)}) copy-start(s32[64]{0:T(128)} %param.20) | copy-start | bytes 772
  80.9 23.7 %copy-start.16 = (f32[128]{0:T(128)S(1)}, f32[128]{0:T(128)}, u32[]{:S(2)}) copy-start(f32[128]{0:T(128)} %param.31) | copy-start | bytes 1540
  80.9 23.7 %copy-start.17 = (f32[128]{0:T(128)S(1)}, f32[128]{0:T(128)}, u32[]{:S(2)}) copy-start(f32[128]{0:T(128)} %param.32) | copy-start | bytes 1540
  81.0 45.5 %copy-start.10 = (bf16[128,128]{1,0:T(8,128)(2,1)S(1)}, bf16[128,128]{1,0:T(8,128)(2,1)}, u32[]{:S(2)}) copy-start(bf16[128,128]{1,0:T(8,128)(2,1)} %refs_2_.2) | copy-start | bytes 98308
  81.1 6.9 %collective-permute-start.1 = (bf16[64,256]{1,0:T(8,128)(2,1)S(1)}, bf16[64,256]{1,0:T(8,128)(2,1)S(1)}, u32[]{:S(2)}, u32[]{:S(2)}) collective-permute-start(bf16[64,256]{1,0:T(8,128)(2,1)S(1)} %pad_maximum_fusion), channel_id=1, source_target_pairs={{0,16},{16,0},{1,17},{17,1},{2,18},{18,2},{3,19},{19,3},{4,20},{20... | collective-permute-start | bytes 98312 | tf_op jit(solution)/shard_map/ppermute | solution.py:493
  126.5 13.3 %copy-start.3 = (bf16[128,704]{0,1:T(8,128)(2,1)S(1)}, bf16[128,704]{0,1:T(8,128)(2,1)}, u32[]{:S(2)}) copy-start(bf16[128,704]{0,1:T(8,128)(2,1)} %param.35) | copy-start | bytes 540676
  126.5 13.3 %copy-start.4 = (bf16[128,704]{0,1:T(8,128)(2,1)S(1)}, bf16[128,704]{0,1:T(8,128)(2,1)}, u32[]{:S(2)}) copy-start(bf16[128,704]{0,1:T(8,128)(2,1)} %param.36) | copy-start | bytes 540676
  126.5 13.3 %copy-start.15 = (f32[128]{0:T(128)S(1)}, f32[128]{0:T(128)}, u32[]{:S(2)}) copy-start(f32[128]{0:T(128)} %param.34) | copy-start | bytes 1540
  140.3 35.7 %copy-start.2 = (bf16[704,128]{1,0:T(8,128)(2,1)S(1)}, bf16[704,128]{1,0:T(8,128)(2,1)}, u32[]{:S(2)}) copy-start(bf16[704,128]{1,0:T(8,128)(2,1)} %refs_2_.3) | copy-start | bytes 540676

commit v8 on v7

--- a/solution.py
+++ b/solution.py
@@ -278,7 +278,9 @@
     put_slots(sent, results, (stats_of(own, other, 0), stats_of(own, other, 2)))
 
 
-def post_kernel(received, before, gain, gate, up, bundle, at, sent, resid):
+def post_kernel(received, before, gain, gate, up, bundle, states, at, sent, resid, out, sem):
+    copy = pltpu.make_async_copy(states, out, sem)
+    copy.start()
     cols = gain.shape[1]
     total = jnp.sum(received[...].astype(f32), axis=0)
     rows = (before[...].astype(f32) + total).astype(bf16)
@@ -289,6 +291,22 @@
     own, other = rows[:, :cols], rows[:, cols:]
     results = products(own, other, gains, weights, matmul_t, False)
     put_rows(sent, results, stats_of(own, other, 0))
+    copy.wait()
+
+
+def post_products(values, states, at, shapes):
+    vmem = pl.BlockSpec(memory_space=pltpu.VMEM)
+    values = [in_vmem(value) for value in (*values, states)]
+    count = len(values)
+    return pl.pallas_call(
+        lambda *refs: post_kernel(*refs[:count], at, *refs[count:]),
+        in_specs=[vmem] * count,
+        out_specs=[vmem, vmem, pl.BlockSpec(memory_space=pl.ANY)],
+        out_shape=[pltpu.VMEM(shape, bf16) for shape in shapes]
+        + [jax.ShapeDtypeStruct(states.shape, f32)],
+        scratch_shapes=[pltpu.SemaphoreType.DMA],
+        compiler_params=SMALL,
+    )(*values)
 
 
 def put_partials(rows, weight, other, out):
@@ -317,25 +335,9 @@
     put_partials(rows[...], weight, bundle[at : at + weight.shape[0], :], out)
 
 
-def heads_kernel(heads, table, weight, states, bundle, at, out, new_states, sem):
-    copy = pltpu.make_async_copy(states, new_states, sem)
-    copy.start()
+def heads_kernel(heads, table, weight, bundle, at, out):
     rows = matmul(table[...], heads[...]).astype(bf16)
     put_partials(rows, weight, bundle[at : at + weight.shape[0], :], out)
-    copy.wait()
-
-
-def head_partials(heads, table, weight, states, bundle, at, shape):
-    vmem = pl.BlockSpec(memory_space=pltpu.VMEM)
-    values = [in_vmem(value) for value in (heads, table, weight, states, bundle)]
-    return pl.pallas_call(
-        lambda *refs: heads_kernel(*refs[:5], at, *refs[5:]),
-        in_specs=[vmem] * len(values),
-        out_specs=[vmem, pl.BlockSpec(memory_space=pl.ANY)],
-        out_shape=[pltpu.VMEM(shape, bf16), jax.ShapeDtypeStruct(states.shape, f32)],
-        scratch_shapes=[pltpu.SemaphoreType.DMA],
-        compiler_params=SMALL,
-    )(*values)
 
 
 def put_pairs(out, at, cols, groups):
@@ -506,24 +508,18 @@
     received = exchanged(sent, "z")
     head_out, side["states"] = recurred(received, *side.pop("recur"), side["states"])
     all_heads = sent_to_all(head_out, ("z", "c")).reshape(slot_count, DK)
-    partials, new_states = head_partials(
+    (partials,) = in_kernel(
+        lambda *refs: heads_kernel(*refs[:-1], starts[8], refs[-1]),
+        (partial_shape,),
         all_heads,
         side["my_table"],
         mix_weight,
-        side.pop("states"),
         side["bundle"],
-        starts[8],
-        partial_shape,
-    )
-    sent, side["resid"] = in_kernel(
-        lambda *refs: post_kernel(*refs[:-2], starts[2], *refs[-2:]),
-        (sent_shape, resid_shape),
-        exchanged(partials, "tp"),
-        side["resid"],
-        gain_post[None, :],
-        mine[2],
-        mine[3],
-        side["bundle"],
+    )
+    received = exchanged(partials, "tp")
+    values = (received, side["resid"], gain_post[None, :], mine[2], mine[3], side["bundle"])
+    sent, side["resid"], new_states = post_products(
+        values, side.pop("states"), starts[2], (sent_shape, resid_shape)
     )
     act = ff_hidden(sent)
     (finish,) = in_kernel(

time: 192 us -> 192 us (level)
  no operation moved by 1% of the time
where the time goes in v8:
time: 192 us; the launch traced here: 191 us
  blocking collectives  168 us (88%)
  starting transfers between devices  14.8 us (8%)
  Pallas kernels  6.62 us (3%)
    all_to_all x10, blocking collectives, exchanged(): value = lax.all_to_all(value, axis, split_axis=0, concat_axis=0, tiled=True)  168 us
    ppermute x1, starting transfers between devices, local(): bundle = lax.ppermute(packed_own, 'c', swap)  8.75 us
    ppermute x1, starting transfers between devices, local(): swapped = lax.ppermute(turned, 'c', swap)  6.09 us
  transfers between devices with their start and end apart: 2, of which 1 were waited for; matrix products, arithmetic and copies ran while one was open for 0% of the time, Pallas kernels for 0%

profile of v8, /device:TPU:1, one launch (start us, length us, event | category | flops | bytes accessed | tf_op | source)
XLA Modules:
  0.0 191.3 jit_solution(4190019722811250400)
XLA Ops:
  0.6 0.0 copy-start.1
  0.6 0.0 copy-start
  0.7 0.0 copy-start.12
  0.7 1.6 shard_map.194
  2.3 8.7 %collective-permute-start = (bf16[4880,128]{1,0:T(8,128)(2,1)S(1)}, bf16[4880,128]{1,0:T(8,128)(2,1)S(1)}, u32[]{:S(2)}, u32[]{:S(2)}) collective-permute-start(bf16[4880,128]{1,0:T(8,128)(2,1)S(1)} %get-tuple-element.127), channel_id=1, source_target_pairs={{0,16},{16,0},{1,17},{17,1},{2,18},{18,2},{3,19},{19,3},{4,20},{20... | collective-permute-start | bytes 3747848 | tf_op jit(solution)/shard_map/ppermute | solution.py:449
  11.1 9.7 %all_to_all.50.gathered = bf16[32,4,128]{2,1,0:T(4,128)(2,1)S(1)} all-to-all(bf16[32,4,128]{2,1,0:T(4,128)(2,1)S(1)} %bitcast.38), channel_id=1, replica_groups=mesh['z'=16,'c'=2,'tp'=16] {'c','tp'}, dimensions={0} | all-to-all | bytes 65536 | tf_op jit(solution)/shard_map/all_to_all | solution.py:436
  20.8 0.0 copy-start.5
  20.8 0.0 collective-permute-done.bundle.refs_2_.refs_8_.refs_3_.refs_5_
  20.8 0.0 copy-done.1
  20.8 0.0 copy-done
  20.8 0.0 copy-done.12
  20.8 0.6 shard_map.195
  21.4 0.1 reshape.30
  21.5 26.2 %all_to_all.51.received = bf16[16,4,1536]{2,1,0:T(4,128)(2,1)S(1)} all-to-all(bf16[16,4,1536]{2,1,0:T(4,128)(2,1)S(1)} %reshape.30), channel_id=1, replica_groups=mesh['z'=16,'c'=2,'tp'=16] {'z'}, dimensions={0} | all-to-all | bytes 393216 | tf_op jit(solution)/shard_map/all_to_all | solution.py:436
  47.6 0.2 shard_map.196
  47.9 20.5 %all_to_all.52 = bf16[16,4,704]{2,1,0:T(4,128)(2,1)S(1)} all-to-all(bf16[16,4,704]{2,1,0:T(4,128)(2,1)S(1)} %shard_map.196), channel_id=1, replica_groups=mesh['z'=16,'c'=2,'tp'=16] {'z'}, dimensions={0} | all-to-all | bytes 180224 | tf_op jit(solution)/shard_map/all_to_all | solution.py:436
  68.5 0.0 copy-done.5
  68.5 0.3 shard_map.197
  68.8 0.0 copy-start.6
  68.8 0.0 copy-start.7
  68.8 0.0 copy-start.8
  68.8 0.0 copy-start.9
  68.8 0.0 copy-start.13
  68.8 12.1 %all_to_all.53 = bf16[16,64,256]{2,1,0:T(8,128)(2,1)S(1)} all-to-all(bf16[16,64,256]{2,1,0:T(8,128)(2,1)S(1)} %shard_map.197), channel_id=1, replica_groups=mesh['z'=16,'c'=2,'tp'=16] {'tp'}, dimensions={0} | all-to-all | bytes 1048576 | tf_op jit(solution)/shard_map/all_to_all | solution.py:436
  80.9 0.0 copy-start.10
  80.9 0.0 copy-start.14
  80.9 0.0 copy-start.16
  80.9 0.0 copy-start.17
  80.9 0.1 convert_reduce_fusion
  81.0 0.0 copy-start.11
  81.1 6.1 %collective-permute-start.1 = (bf16[64,256]{1,0:T(8,128)(2,1)S(1)}, bf16[64,256]{1,0:T(8,128)(2,1)S(1)}, u32[]{:S(2)}, u32[]{:S(2)}) collective-permute-start(bf16[64,256]{1,0:T(8,128)(2,1)S(1)} %pad_maximum_fusion), channel_id=1, source_target_pairs={{0,16},{16,0},{1,17},{17,1},{2,18},{18,2},{3,19},{19,3},{4,20},{20... | collective-permute-start | bytes 98312 | tf_op jit(solution)/shard_map/ppermute | solution.py:495
  87.1 0.8 collective-permute-done.1.refs_2_
  88.0 0.0 copy-done.6
  88.0 0.0 copy-done.7
  88.0 0.0 copy-done.8
  88.0 0.0 copy-done.9
  88.0 0.0 copy-done.13
  88.0 0.4 shard_map.198
  88.4 16.2 %all_to_all.54.sums = bf16[16,4,1152]{2,1,0:T(4,128)(2,1)S(1)} all-to-all(bf16[16,4,1152]{2,1,0:T(4,128)(2,1)S(1)} %shard_map.198), channel_id=1, replica_groups=mesh['z'=16,'c'=2,'tp'=16] {'z'}, dimensions={0} | all-to-all | bytes 294912 | tf_op jit(solution)/shard_map/all_to_all | solution.py:436
  104.6 0.0 copy-done.10
  104.6 0.0 copy-done.14
  104.6 0.0 copy-done.16
  104.6 0.0 copy-done.17
  104.6 1.0 shard_map.199
  105.6 20.8 %all_to_all.55 = bf16[32,8,128]{2,1,0:T(8,128)(2,1)S(1)} all-to-all(bf16[32,8,128]{2,1,0:T(8,128)(2,1)S(1)} %broadcast_in_dim.38), channel_id=1, replica_groups=mesh['z'=16,'c'=2,'tp'=16] {'z','c'}, dimensions={0} | all-to-all | bytes 131072 | tf_op jit(solution)/shard_map/all_to_all | solution.py:436
  126.5 0.0 copy-done.11
  126.5 0.0 copy-start.3
  126.5 0.0 copy-start.4
  126.5 0.0 copy-start.15
  126.5 0.3 shard_map.200
  126.9 12.6 %all_to_all.56.refs_0_ = bf16[16,64,256]{2,1,0:T(8,128)(2,1)S(1)} all-to-all(bf16[16,64,256]{2,1,0:T(8,128)(2,1)S(1)} %shard_map.200), channel_id=1, replica_groups=mesh['z'=16,'c'=2,'tp'=16] {'tp'}, dimensions={0} | all-to-all | bytes 1048576 | tf_op jit(solution)/shard_map/all_to_all | solution.py:436
  139.5 0.0 copy-done.3
  139.5 0.0 copy-done.4
  139.5 0.0 copy-done.15
  139.5 0.7 shard_map.201
  140.2 0.0 copy-start.2
  140.2 0.1 reshape.34
  140.2 15.8 %all_to_all.57.received = bf16[16,4,1536]{2,1,0:T(4,128)(2,1)S(1)} all-to-all(bf16[16,4,1536]{2,1,0:T(4,128)(2,1)S(1)} %reshape.34), channel_id=1, replica_groups=mesh['z'=16,'c'=2,'tp'=16] {'z'}, dimensions={0} | all-to-all | bytes 393216 | tf_op jit(solution)/shard_map/all_to_all | solution.py:436
  156.0 0.2 shard_map.202
  156.3 19.6 %all_to_all.58 = bf16[16,4,704]{2,1,0:T(4,128)(2,1)S(1)} all-to-all(bf16[16,4,704]{2,1,0:T(4,128)(2,1)S(1)} %shard_map.202), channel_id=1, replica_groups=mesh['z'=16,'c'=2,'tp'=16] {'z'}, dimensions={0} | all-to-all | bytes 180224 | tf_op jit(solution)/shard_map/all_to_all | solution.py:436
  175.9 0.0 copy-done.2
  175.9 0.4 shard_map.203
  176.2 14.3 %all_to_all.59.received = f32[32,4,128]{2,1,0:T(4,128)S(1)} all-to-all(f32[32,4,128]{2,1,0:T(4,128)S(1)} %shard_map.203), channel_id=1, replica_groups=mesh['z'=16,'c'=2,'tp'=16] {'c','tp'}, dimensions={0} | all-to-all | bytes 131072 | tf_op jit(solution)/shard_map/all_to_all | solution.py:436
  190.5 0.8 shard_map.204
  (7 shorter events, 0.1 us)
Async XLA Ops:
  0.6 20.2 %copy-start.1 = (bf16[128,704]{0,1:T(8,128)(2,1)S(1)}, bf16[128,704]{0,1:T(8,128)(2,1)}, u32[]{:S(2)}) copy-start(bf16[128,704]{0,1:T(8,128)(2,1)} %param.24) | copy-start | bytes 540676
  0.6 20.1 %copy-start = (bf16[128,704]{0,1:T(8,128)(2,1)S(1)}, bf16[128,704]{0,1:T(8,128)(2,1)}, u32[]{:S(2)}) copy-start(bf16[128,704]{0,1:T(8,128)(2,1)} %param.23) | copy-start | bytes 540676
  0.7 20.1 %copy-start.12 = (f32[128]{0:T(128)S(1)}, f32[128]{0:T(128)}, u32[]{:S(2)}) copy-start(f32[128]{0:T(128)} %param.22) | copy-start | bytes 1540
  2.3 18.5 %collective-permute-start = (bf16[4880,128]{1,0:T(8,128)(2,1)S(1)}, bf16[4880,128]{1,0:T(8,128)(2,1)S(1)}, u32[]{:S(2)}, u32[]{:S(2)}) collective-permute-start(bf16[4880,128]{1,0:T(8,128)(2,1)S(1)} %get-tuple-element.127), channel_id=1, source_target_pairs={{0,16},{16,0},{1,17},{17,1},{2,18},{18,2},{3,19},{19,3},{4,20},{20... | collective-permute-start | bytes 3747848 | tf_op jit(solution)/shard_map/ppermute | solution.py:449
  20.8 47.7 %copy-start.5 = (bf16[704,128]{1,0:T(8,128)(2,1)S(1)}, bf16[704,128]{1,0:T(8,128)(2,1)}, u32[]{:S(2)}) copy-start(bf16[704,128]{1,0:T(8,128)(2,1)} %refs_1_.1) | copy-start | bytes 540676
  68.8 19.2 %copy-start.6 = (bf16[128,128]{1,0:T(8,128)(2,1)S(1)}, bf16[128,128]{1,0:T(8,128)(2,1)}, u32[]{:S(2)}) copy-start(bf16[128,128]{1,0:T(8,128)(2,1)} %refs_4_.3) | copy-start | bytes 98308
  68.8 19.2 %copy-start.7 = (bf16[128,128]{1,0:T(8,128)(2,1)S(1)}, bf16[128,128]{1,0:T(8,128)(2,1)}, u32[]{:S(2)}) copy-start(bf16[128,128]{1,0:T(8,128)(2,1)} %refs_5_.3) | copy-start | bytes 98308
  68.8 19.2 %copy-start.8 = (bf16[128,128]{1,0:T(8,128)(2,1)S(1)}, bf16[128,128]{1,0:T(8,128)(2,1)}, u32[]{:S(2)}) copy-start(bf16[128,128]{1,0:T(8,128)(2,1)} %refs_6_.3) | copy-start | bytes 98308
  68.8 19.2 %copy-start.9 = (bf16[128,128]{1,0:T(8,128)(2,1)S(1)}, bf16[128,128]{1,0:T(8,128)(2,1)}, u32[]{:S(2)}) copy-start(bf16[128,128]{1,0:T(8,128)(2,1)} %refs_7_.3) | copy-start | bytes 98308
  68.8 19.2 %copy-start.13 = (f32[128]{0:T(128)S(1)}, f32[128]{0:T(128)}, u32[]{:S(2)}) copy-start(f32[128]{0:T(128)} %param.26) | copy-start | bytes 1540
  80.9 23.7 %copy-start.10 = (f32[2,1,128,128]{3,2,1,0:T(8,128)S(1)}, f32[2,1,128,128]{3,2,1,0:T(8,128)}, u32[]{:S(2)}) copy-start(f32[2,1,128,128]{3,2,1,0:T(8,128)} %param.21) | copy-start | bytes 393220
  80.9 23.7 %copy-start.14 = (s32[64]{0:T(128)S(1)}, s32[64]{0:T(128)}, u32[]{:S(2)}) copy-start(s32[64]{0:T(128)} %param.20) | copy-start | bytes 772
  80.9 23.7 %copy-start.16 = (f32[128]{0:T(128)S(1)}, f32[128]{0:T(128)}, u32[]{:S(2)}) copy-start(f32[128]{0:T(128)} %param.31) | copy-start | bytes 1540
  80.9 23.7 %copy-start.17 = (f32[128]{0:T(128)S(1)}, f32[128]{0:T(128)}, u32[]{:S(2)}) copy-start(f32[128]{0:T(128)} %param.32) | copy-start | bytes 1540
  81.0 45.5 %copy-start.11 = (bf16[128,128]{1,0:T(8,128)(2,1)S(1)}, bf16[128,128]{1,0:T(8,128)(2,1)}, u32[]{:S(2)}) copy-start(bf16[128,128]{1,0:T(8,128)(2,1)} %refs_2_.2) | copy-start | bytes 98308
  81.1 6.9 %collective-permute-start.1 = (bf16[64,256]{1,0:T(8,128)(2,1)S(1)}, bf16[64,256]{1,0:T(8,128)(2,1)S(1)}, u32[]{:S(2)}, u32[]{:S(2)}) collective-permute-start(bf16[64,256]{1,0:T(8,128)(2,1)S(1)} %pad_maximum_fusion), channel_id=1, source_target_pairs={{0,16},{16,0},{1,17},{17,1},{2,18},{18,2},{3,19},{19,3},{4,20},{20... | collective-permute-start | bytes 98312 | tf_op jit(solution)/shard_map/ppermute | solution.py:495
  126.5 13.0 %copy-start.3 = (bf16[128,704]{0,1:T(8,128)(2,1)S(1)}, bf16[128,704]{0,1:T(8,128)(2,1)}, u32[]{:S(2)}) copy-start(bf16[128,704]{0,1:T(8,128)(2,1)} %param.35) | copy-start | bytes 540676
  126.5 13.0 %copy-start.4 = (bf16[128,704]{0,1:T(8,128)(2,1)S(1)}, bf16[128,704]{0,1:T(8,128)(2,1)}, u32[]{:S(2)}) copy-start(bf16[128,704]{0,1:T(8,128)(2,1)} %param.36) | copy-start | bytes 540676
  126.5 13.0 %copy-start.15 = (f32[128]{0:T(128)S(1)}, f32[128]{0:T(128)}, u32[]{:S(2)}) copy-start(f32[128]{0:T(128)} %param.34) | copy-start | bytes 1540
  140.2 35.7 %copy-start.2 = (bf16[704,128]{1,0:T(8,128)(2,1)S(1)}, bf16[704,128]{1,0:T(8,128)(2,1)}, u32[]{:S(2)}) copy-start(bf16[704,128]{1,0:T(8,128)(2,1)} %refs_2_.3) | copy-start | bytes 540676

commit v9 on v8

--- a/solution.py
+++ b/solution.py
@@ -267,15 +267,26 @@
     put_rows(sent, results, stats_of(own, other, 0))
 
 
-def mix_kernel(spread, resid, swapped, gain, query, forget, value, outgate, bundle, at, sent):
+def mix_rows(rows, gain, weights, bundle, at):
     cols = gain.shape[1]
-    rows = jnp.concatenate([resid[...], swapped[...]], axis=0)
-    rows = matmul(spread[...], rows)
-    weights = halves_of((query, forget, value, outgate), bundle, at)
+    rows = rows[...].astype(f32)
+    own, other = rows[:, :cols], rows[:, cols:]
     gains = (gain[...], gain_rows(bundle, 1))
-    own, other = rows[:, :cols], rows[:, cols:]
-    results = products(own, other, gains, weights, matmul, True)
-    put_slots(sent, results, (stats_of(own, other, 0), stats_of(own, other, 2)))
+    results = products(own, other, gains, halves_of(weights, bundle, at), matmul, True)
+    stats = [stats_of(own, other, 0), stats_of(own, other, 2)]
+    return jnp.concatenate([value.astype(bf16) for value in (*results, *stats)], axis=1)
+
+
+def own_kernel(rows, gain, query, forget, value, outgate, bundle, at, out):
+    out[...] = mix_rows(rows, gain, (query, forget, value, outgate), bundle, at)
+
+
+def mix_kernel(spread, ready, rows, gain, query, forget, value, outgate, bundle, at, sent):
+    others = mix_rows(rows, gain, (query, forget, value, outgate), bundle, at)
+    slots = matmul(spread[...], jnp.concatenate([ready[...], others], axis=0))
+    width = slots.shape[1] - 2 * LANES
+    stats = (slots[:, width : width + LANES], slots[:, width + LANES :])
+    put_slots(sent, [slots[:, :width]], stats)
 
 
 def post_kernel(received, before, gain, gate, up, bundle, states, at, sent, resid, out, sem):
@@ -493,15 +504,20 @@
 
     turned = jnp.concatenate([resid[:, own_cols:], resid[:, :own_cols]], axis=1)
     swapped = lax.ppermute(turned, "c", swap)
+    mix_values = (gain_mix[None, :], *mine[4:8], side["bundle"])
+    (ready,) = in_kernel(
+        lambda *refs: own_kernel(*refs[:-1], starts[4], refs[-1]),
+        ((half, 4 * head_cols + 2 * LANES),),
+        resid,
+        *mix_values,
+    )
     (sent,) = in_kernel(
         lambda *refs: mix_kernel(*refs[:-1], starts[4], refs[-1]),
         ((z_count, W, 8 * head_cols + LANES),),
         side["spread"],
-        resid,
+        ready,
         swapped,
-        gain_mix[None, :],
-        *mine[4:8],
-        side["bundle"],
+        *mix_values,
     )
     side["recur"] = (lengths[None, :], forget_floor[None, :], head_gain[None, :])
     side["states"] = states.reshape(seq_local * heads_local, DK, DK)

time: 192 us -> 192 us (level)
  no operation moved by 1% of the time
where the time goes in v9:
time: 192 us; the launch traced here: 191 us
  blocking collectives  168 us (88%)
  starting transfers between devices  14.8 us (8%)
  Pallas kernels  6.8 us (4%)
    all_to_all x10, blocking collectives, exchanged(): value = lax.all_to_all(value, axis, split_axis=0, concat_axis=0, tiled=True)  168 us
    ppermute x1, starting transfers between devices, local(): bundle = lax.ppermute(packed_own, 'c', swap)  8.75 us
    ppermute x1, starting transfers between devices, local(): swapped = lax.ppermute(turned, 'c', swap)  6.09 us
  transfers between devices with their start and end apart: 2, of which 1 were waited for; matrix products, arithmetic and copies ran while one was open for 0% of the time, Pallas kernels for 0%

profile of v9, /device:TPU:1, one launch (start us, length us, event | category | flops | bytes accessed | tf_op | source)
XLA Modules:
  0.0 191.2 jit_solution(5304707033346056345)
XLA Ops:
  0.6 0.0 copy-start.1
  0.6 0.0 copy-start
  0.7 0.0 copy-start.13
  0.7 1.6 shard_map.194
  2.3 8.7 %collective-permute-start = (bf16[4880,128]{1,0:T(8,128)(2,1)S(1)}, bf16[4880,128]{1,0:T(8,128)(2,1)S(1)}, u32[]{:S(2)}, u32[]{:S(2)}) collective-permute-start(bf16[4880,128]{1,0:T(8,128)(2,1)S(1)} %get-tuple-element.127), channel_id=1, source_target_pairs={{0,16},{16,0},{1,17},{17,1},{2,18},{18,2},{3,19},{19,3},{4,20},{20... | collective-permute-start | bytes 3747848 | tf_op jit(solution)/shard_map/ppermute | solution.py:460
  11.1 9.7 %all_to_all.50.gathered = bf16[32,4,128]{2,1,0:T(4,128)(2,1)S(1)} all-to-all(bf16[32,4,128]{2,1,0:T(4,128)(2,1)S(1)} %bitcast.39), channel_id=1, replica_groups=mesh['z'=16,'c'=2,'tp'=16] {'c','tp'}, dimensions={0} | all-to-all | bytes 65536 | tf_op jit(solution)/shard_map/all_to_all | solution.py:447
  20.8 0.0 copy-start.5
  20.8 0.0 collective-permute-done.bundle.refs_2_.refs_6_.refs_8_.refs_3_.refs_5_
  20.8 0.0 copy-done.1
  20.8 0.0 copy-done
  20.8 0.0 copy-done.13
  20.8 0.6 shard_map.195
  21.4 0.1 reshape.30
  21.5 26.2 %all_to_all.51.received = bf16[16,4,1536]{2,1,0:T(4,128)(2,1)S(1)} all-to-all(bf16[16,4,1536]{2,1,0:T(4,128)(2,1)S(1)} %reshape.30), channel_id=1, replica_groups=mesh['z'=16,'c'=2,'tp'=16] {'z'}, dimensions={0} | all-to-all | bytes 393216 | tf_op jit(solution)/shard_map/all_to_all | solution.py:447
  47.6 0.2 shard_map.196
  47.9 20.5 %all_to_all.52 = bf16[16,4,704]{2,1,0:T(4,128)(2,1)S(1)} all-to-all(bf16[16,4,704]{2,1,0:T(4,128)(2,1)S(1)} %shard_map.196), channel_id=1, replica_groups=mesh['z'=16,'c'=2,'tp'=16] {'z'}, dimensions={0} | all-to-all | bytes 180224 | tf_op jit(solution)/shard_map/all_to_all | solution.py:447
  68.5 0.0 copy-done.5
  68.5 0.3 shard_map.197
  68.8 0.0 copy-start.6
  68.8 0.0 copy-start.7
  68.8 0.0 copy-start.8
  68.8 0.0 copy-start.9
  68.8 0.0 copy-start.12
  68.8 12.1 %all_to_all.53 = bf16[16,64,256]{2,1,0:T(8,128)(2,1)S(1)} all-to-all(bf16[16,64,256]{2,1,0:T(8,128)(2,1)S(1)} %shard_map.197), channel_id=1, replica_groups=mesh['z'=16,'c'=2,'tp'=16] {'tp'}, dimensions={0} | all-to-all | bytes 1048576 | tf_op jit(solution)/shard_map/all_to_all | solution.py:447
  80.9 0.1 convert_reduce_fusion
  81.0 6.1 %collective-permute-start.1 = (bf16[64,256]{1,0:T(8,128)(2,1)S(1)}, bf16[64,256]{1,0:T(8,128)(2,1)S(1)}, u32[]{:S(2)}, u32[]{:S(2)}) collective-permute-start(bf16[64,256]{1,0:T(8,128)(2,1)S(1)} %pad_maximum_fusion), channel_id=1, source_target_pairs={{0,16},{16,0},{1,17},{17,1},{2,18},{18,2},{3,19},{19,3},{4,20},{20... | collective-permute-start | bytes 98312 | tf_op jit(solution)/shard_map/ppermute | solution.py:506
  87.1 0.0 copy-done.6
  87.1 0.0 copy-done.7
  87.1 0.0 copy-done.8
  87.2 0.0 copy-done.9
  87.2 0.0 copy-done.12
  87.2 0.2 shard_map.198.refs_1_
  87.4 0.0 copy-start.10
  87.4 0.0 copy-start.14
  87.4 0.0 copy-start.16
  87.4 0.0 copy-start.17
  87.4 0.0 copy-start.11
  87.4 0.5 collective-permute-done.1.refs_2_
  88.0 0.4 shard_map.199
  88.4 16.2 %all_to_all.54.sums = bf16[16,4,1152]{2,1,0:T(4,128)(2,1)S(1)} all-to-all(bf16[16,4,1152]{2,1,0:T(4,128)(2,1)S(1)} %shard_map.199), channel_id=1, replica_groups=mesh['z'=16,'c'=2,'tp'=16] {'z'}, dimensions={0} | all-to-all | bytes 294912 | tf_op jit(solution)/shard_map/all_to_all | solution.py:447
  104.5 0.0 copy-done.10
  104.5 0.0 copy-done.14
  104.5 0.0 copy-done.16
  104.5 0.0 copy-done.17
  104.5 1.0 shard_map.200
  105.6 20.8 %all_to_all.55 = bf16[32,8,128]{2,1,0:T(8,128)(2,1)S(1)} all-to-all(bf16[32,8,128]{2,1,0:T(8,128)(2,1)S(1)} %broadcast_in_dim.38), channel_id=1, replica_groups=mesh['z'=16,'c'=2,'tp'=16] {'z','c'}, dimensions={0} | all-to-all | bytes 131072 | tf_op jit(solution)/shard_map/all_to_all | solution.py:447
  126.4 0.0 copy-done.11
  126.4 0.0 copy-start.3
  126.4 0.0 copy-start.4
  126.4 0.3 shard_map.201
  126.8 12.6 %all_to_all.56.refs_0_ = bf16[16,64,256]{2,1,0:T(8,128)(2,1)S(1)} all-to-all(bf16[16,64,256]{2,1,0:T(8,128)(2,1)S(1)} %shard_map.201), channel_id=1, replica_groups=mesh['z'=16,'c'=2,'tp'=16] {'tp'}, dimensions={0} | all-to-all | bytes 1048576 | tf_op jit(solution)/shard_map/all_to_all | solution.py:447
  139.4 0.0 copy-done.3
  139.4 0.0 copy-done.4
  139.4 0.0 copy-done.15
  139.4 0.7 shard_map.202
  140.1 0.0 copy-start.2
  140.1 0.1 reshape.34
  140.1 15.8 %all_to_all.57.received = bf16[16,4,1536]{2,1,0:T(4,128)(2,1)S(1)} all-to-all(bf16[16,4,1536]{2,1,0:T(4,128)(2,1)S(1)} %reshape.34), channel_id=1, replica_groups=mesh['z'=16,'c'=2,'tp'=16] {'z'}, dimensions={0} | all-to-all | bytes 393216 | tf_op jit(solution)/shard_map/all_to_all | solution.py:447
  155.9 0.2 shard_map.203
  156.2 19.6 %all_to_all.58 = bf16[16,4,704]{2,1,0:T(4,128)(2,1)S(1)} all-to-all(bf16[16,4,704]{2,1,0:T(4,128)(2,1)S(1)} %shard_map.203), channel_id=1, replica_groups=mesh['z'=16,'c'=2,'tp'=16] {'z'}, dimensions={0} | all-to-all | bytes 180224 | tf_op jit(solution)/shard_map/all_to_all | solution.py:447
  175.8 0.0 copy-done.2
  175.8 0.4 shard_map.204
  176.2 14.3 %all_to_all.59.received = f32[32,4,128]{2,1,0:T(4,128)S(1)} all-to-all(f32[32,4,128]{2,1,0:T(4,128)S(1)} %shard_map.204), channel_id=1, replica_groups=mesh['z'=16,'c'=2,'tp'=16] {'c','tp'}, dimensions={0} | all-to-all | bytes 131072 | tf_op jit(solution)/shard_map/all_to_all | solution.py:447
  190.4 0.8 shard_map.205
  (8 shorter events, 0.1 us)
Async XLA Ops:
  0.6 20.2 %copy-start.1 = (bf16[128,704]{0,1:T(8,128)(2,1)S(1)}, bf16[128,704]{0,1:T(8,128)(2,1)}, u32[]{:S(2)}) copy-start(bf16[128,704]{0,1:T(8,128)(2,1)} %param.24) | copy-start | bytes 540676
  0.6 20.1 %copy-start = (bf16[128,704]{0,1:T(8,128)(2,1)S(1)}, bf16[128,704]{0,1:T(8,128)(2,1)}, u32[]{:S(2)}) copy-start(bf16[128,704]{0,1:T(8,128)(2,1)} %param.23) | copy-start | bytes 540676
  0.7 20.1 %copy-start.13 = (f32[128]{0:T(128)S(1)}, f32[128]{0:T(128)}, u32[]{:S(2)}) copy-start(f32[128]{0:T(128)} %param.22) | copy-start | bytes 1540
  2.3 18.5 %collective-permute-start = (bf16[4880,128]{1,0:T(8,128)(2,1)S(1)}, bf16[4880,128]{1,0:T(8,128)(2,1)S(1)}, u32[]{:S(2)}, u32[]{:S(2)}) collective-permute-start(bf16[4880,128]{1,0:T(8,128)(2,1)S(1)} %get-tuple-element.127), channel_id=1, source_target_pairs={{0,16},{16,0},{1,17},{17,1},{2,18},{18,2},{3,19},{19,3},{4,20},{20... | collective-permute-start | bytes 3747848 | tf_op jit(solution)/shard_map/ppermute | solution.py:460
  20.8 47.7 %copy-start.5 = (bf16[704,128]{1,0:T(8,128)(2,1)S(1)}, bf16[704,128]{1,0:T(8,128)(2,1)}, u32[]{:S(2)}) copy-start(bf16[704,128]{1,0:T(8,128)(2,1)} %refs_1_.1) | copy-start | bytes 540676
  68.8 18.4 %copy-start.6 = (bf16[128,128]{1,0:T(8,128)(2,1)S(1)}, bf16[128,128]{1,0:T(8,128)(2,1)}, u32[]{:S(2)}) copy-start(bf16[128,128]{1,0:T(8,128)(2,1)} %refs_4_.5) | copy-start | bytes 98308
  68.8 18.4 %copy-start.7 = (bf16[128,128]{1,0:T(8,128)(2,1)S(1)}, bf16[128,128]{1,0:T(8,128)(2,1)}, u32[]{:S(2)}) copy-start(bf16[128,128]{1,0:T(8,128)(2,1)} %refs_5_.5) | copy-start | bytes 98308
  68.8 18.4 %copy-start.8 = (bf16[128,128]{1,0:T(8,128)(2,1)S(1)}, bf16[128,128]{1,0:T(8,128)(2,1)}, u32[]{:S(2)}) copy-start(bf16[128,128]{1,0:T(8,128)(2,1)} %refs_6_.3) | copy-start | bytes 98308
  68.8 18.4 %copy-start.9 = (bf16[128,128]{1,0:T(8,128)(2,1)S(1)}, bf16[128,128]{1,0:T(8,128)(2,1)}, u32[]{:S(2)}) copy-start(bf16[128,128]{1,0:T(8,128)(2,1)} %refs_7_.3) | copy-start | bytes 98308
  68.8 18.4 %copy-start.12 = (f32[128]{0:T(128)S(1)}, f32[128]{0:T(128)}, u32[]{:S(2)}) copy-start(f32[128]{0:T(128)} %param.26) | copy-start | bytes 1540
  81.0 6.9 %collective-permute-start.1 = (bf16[64,256]{1,0:T(8,128)(2,1)S(1)}, bf16[64,256]{1,0:T(8,128)(2,1)S(1)}, u32[]{:S(2)}, u32[]{:S(2)}) collective-permute-start(bf16[64,256]{1,0:T(8,128)(2,1)S(1)} %pad_maximum_fusion), channel_id=1, source_target_pairs={{0,16},{16,0},{1,17},{17,1},{2,18},{18,2},{3,19},{19,3},{4,20},{20... | collective-permute-start | bytes 98312 | tf_op jit(solution)/shard_map/ppermute | solution.py:506
  87.4 17.1 %copy-start.10 = (f32[2,1,128,128]{3,2,1,0:T(8,128)S(1)}, f32[2,1,128,128]{3,2,1,0:T(8,128)}, u32[]{:S(2)}) copy-start(f32[2,1,128,128]{3,2,1,0:T(8,128)} %param.21) | copy-start | bytes 393220
  87.4 17.1 %copy-start.14 = (s32[64]{0:T(128)S(1)}, s32[64]{0:T(128)}, u32[]{:S(2)}) copy-start(s32[64]{0:T(128)} %param.20) | copy-start | bytes 772
  87.4 17.1 %copy-start.16 = (f32[128]{0:T(128)S(1)}, f32[128]{0:T(128)}, u32[]{:S(2)}) copy-start(f32[128]{0:T(128)} %param.31) | copy-start | bytes 1540
  87.4 17.1 %copy-start.17 = (f32[128]{0:T(128)S(1)}, f32[128]{0:T(128)}, u32[]{:S(2)}) copy-start(f32[128]{0:T(128)} %param.32) | copy-start | bytes 1540
  87.4 39.0 %copy-start.11 = (bf16[128,128]{1,0:T(8,128)(2,1)S(1)}, bf16[128,128]{1,0:T(8,128)(2,1)}, u32[]{:S(2)}) copy-start(bf16[128,128]{1,0:T(8,128)(2,1)} %refs_2_.4) | copy-start | bytes 98308
  126.4 13.0 %copy-start.3 = (bf16[128,704]{0,1:T(8,128)(2,1)S(1)}, bf16[128,704]{0,1:T(8,128)(2,1)}, u32[]{:S(2)}) copy-start(bf16[128,704]{0,1:T(8,128)(2,1)} %param.35) | copy-start | bytes 540676
  126.4 13.0 %copy-start.4 = (bf16[128,704]{0,1:T(8,128)(2,1)S(1)}, bf16[128,704]{0,1:T(8,128)(2,1)}, u32[]{:S(2)}) copy-start(bf16[128,704]{0,1:T(8,128)(2,1)} %param.36) | copy-start | bytes 540676
  126.4 13.0 %copy-start.15 = (f32[128]{0:T(128)S(1)}, f32[128]{0:T(128)}, u32[]{:S(2)}) copy-start(f32[128]{0:T(128)} %param.34) | copy-start | bytes 1540
  140.1 35.7 %copy-start.2 = (bf16[704,128]{1,0:T(8,128)(2,1)S(1)}, bf16[704,128]{1,0:T(8,128)(2,1)}, u32[]{:S(2)}) copy-start(bf16[704,128]{1,0:T(8,128)(2,1)} %refs_2_.5) | copy-start | bytes 540676
